TPU v7x, 32 devices: a whole 2x2x4 slice. The times are simulated.
32 devices in a mesh: grp: 2 (over y), sp: 4 (over z), tp: 4 (over x, core).
Axes of the slice: x: 2, y: 2, z: 4, core: 2. Of those that a mesh axis runs over, the one named last changes fastest.
Arguments:
- residual: bfloat16 [6144, 2048], P(('grp', 'sp', 'tp')), parts along dimension 0, may hold values from -6 to 6
- value_projected: bfloat16 [6144, 4096], P(('grp', 'sp'), 'tp'), parts along dimension 0, may hold values from -6 to 6
- gate_projected: bfloat16 [6144, 4096], P(('grp', 'sp'), 'tp'), parts along dimension 0, may hold values from -6 to 6
- wide_key_rows: bfloat16 [6144, 1024], P(('grp', 'sp'), 'tp'), parts along dimension 0, may hold values from -6 to 6
- wide_query_rows: bfloat16 [6144, 1024], P(('grp', 'sp'), 'tp'), parts along dimension 0, may hold values from -6 to 6
- narrow_key_rows: bfloat16 [6144, 512], P(('grp', 'sp'), 'tp'), parts along dimension 0, may hold values from -6 to 6
- narrow_query_rows: bfloat16 [6144, 512], P(('grp', 'sp'), 'tp'), parts along dimension 0, may hold values from -6 to 6
- step_before_softplus: float32 [6144, 64], P(('grp', 'sp'), 'tp'), parts along dimension 0, may hold values from -5 to 5
- extra_log_decay: float32 [6144, 64], P(('grp', 'sp'), 'tp'), parts along dimension 0, may hold values from -0.7 to 0
- log_decay_rate: float32 [64], P('tp'), may hold values from -12.3 to -2.99
- value_kernel: bfloat16 [4, 4096], P(None, 'tp'), may hold values from -3 to 3
- wide_key_kernel: bfloat16 [4, 1024], P(None, 'tp'), may hold values from -3 to 3
- wide_query_kernel: bfloat16 [4, 1024], P(None, 'tp'), may hold values from -3 to 3
- narrow_key_kernel: bfloat16 [4, 512], P(None, 'tp'), may hold values from -3 to 3
- narrow_query_kernel: bfloat16 [4, 512], P(None, 'tp'), may hold values from -3 to 3
- head_norm_gain: bfloat16 [4096], P('tp'), may hold values from 0.099609375 to 1.8984375
- output_matrix: bfloat16 [4096, 2048], P('tp'), may hold values from -0.09375 to 0.09375
- feedforward_norm_gain: bfloat16 [2048], replicated, may hold values from 0.099609375 to 1.8984375
- gate_matrix: bfloat16 [2048, 3072], P('sp', 'tp'), may hold values from -0.125 to 0.125
- up_matrix: bfloat16 [2048, 3072], P('sp', 'tp'), may hold values from -0.125 to 0.125
- down_matrix: bfloat16 [2048, 3072], P('sp', 'tp'), may hold values from -0.3125 to 0.3125
Outputs:
- mixed: bfloat16 [6144, 2048], P(('grp', 'sp', 'tp')), parts along dimension 0
There are 2 independent parts, one for each index of `grp`. A program takes and returns all parts, laid end to end along the dimension named above; an argument that names none is the same for every part. Nothing has to cross between parts.
All inputs are finite; a program needn't handle non-finite values.
Results may differ from a plain program's by a relative error of at most 0.015.
Values may be sent and summed in bfloat16 or wider, within the bound.
No kernel may reach another device: no remote copies, remote signals or barrier semaphores. Data moves between devices by JAX's collectives and lax.ppermute only.
A program may use at most 128 MiB of HBM per device.

v0:
```python
import jax
import jax.numpy as jnp
from jax import lax
from jax.sharding import PartitionSpec as P

HEADS = 64
HEAD_DIM = 64
GROUPS = 16
STATE_WIDE = 128
STATE_NARROW = 64
CONV_W = 4
BLK = 64


def passed_along(value, axis, steps):
    count = lax.axis_size(axis)
    initial, last = (max(0, -steps), min(count, count - steps))
    return lax.ppermute(value, axis, [(source, source + steps) for source in range(initial, last)])


def entering_2(shard, axis, join, neutral):
    place = lax.axis_index(axis)
    gathered = jax.tree.map(
        lambda a, kind: lax.all_gather(a.astype(kind), axis),
        shard,
        (jnp.bfloat16, jnp.bfloat16, jnp.bfloat16),
    )
    state = jax.tree.map(lambda a, e: jnp.zeros_like(a) + jnp.asarray(e, a.dtype), shard, neutral)

    def one(turn, state):
        return join(
            state,
            jax.tree.map(
                lambda a, own: lax.dynamic_index_in_dim(a, turn, 0, False).astype(own.dtype),
                gathered,
                shard,
            ),
        )

    return lax.fori_loop(0, place, one, state)


def collect_weights(gate_matrix, up_matrix, down_matrix):
    return (
        lax.all_gather(gate_matrix, "sp", axis=0, tiled=True),
        lax.all_gather(up_matrix, "sp", axis=0, tiled=True),
        lax.all_gather(down_matrix, "sp", axis=0, tiled=True),
    )


def conv_local(inputs, rim, kernel):
    width = kernel.shape[0]
    length = inputs.shape[0]
    padded = jnp.concatenate([rim, inputs], axis=0).astype(jnp.float32)
    total = jnp.zeros(inputs.shape, jnp.float32)
    for offset in range(width):
        total = total + padded[offset : offset + length] * kernel[offset].astype(jnp.float32)
    return jax.nn.silu(total).astype(jnp.bfloat16)


def family_local(values, step_sizes, decay_factor, keys, queries):
    length, groups, per_group, width = values.shape
    states = keys.shape[2]
    count = length // BLK
    block_values = values.reshape(count, BLK, groups, per_group, width)
    block_steps = step_sizes.reshape(count, BLK, groups, per_group)
    block_keys = keys.reshape(count, BLK, groups, states)
    block_queries = queries.reshape(count, BLK, groups, states)
    running = jnp.cumsum(decay_factor.reshape(count, BLK, groups, per_group), axis=1)
    lower = jnp.tril(jnp.ones((BLK, BLK), dtype=bool))
    scores = jnp.einsum(
        "clgn,csgn->clsg", block_queries, block_keys, preferred_element_type=jnp.float32
    )
    spread = jnp.where(
        lower[None, :, :, None, None], running[:, :, None] - running[:, None, :], -jnp.inf
    )
    weights = (scores[..., None] * jnp.exp(spread) * block_steps[:, None]).astype(jnp.bfloat16)
    inside = jnp.einsum(
        "clsgr,csgrp->clgrp", weights, block_values, preferred_element_type=jnp.float32
    )
    fade = block_steps * jnp.exp(running[:, -1:] - running)
    scaled = (block_values.astype(jnp.float32) * fade[..., None]).astype(jnp.bfloat16)
    block_states = jnp.einsum(
        "clgrp,clgn->cgrpn", scaled, block_keys, preferred_element_type=jnp.float32
    )
    return (inside, running, block_states, running[:, -1], block_queries)


def device_summary(block_states, totals):
    inclusive = jnp.cumsum(totals, axis=0)
    whole = inclusive[-1]
    fades = jnp.exp(whole[None] - inclusive)
    summary = jnp.einsum("cgr,cgrpn->grpn", fades, block_states, precision=lax.Precision.HIGHEST)
    return (whole, summary)


def family_output(parts, entering):
    inside, running, block_states, totals, block_queries = parts
    count = inside.shape[0]
    inclusive = jnp.cumsum(totals, axis=0)
    exclusive = inclusive - totals
    earlier = jnp.tril(jnp.ones((count, count), dtype=bool), -1)
    pairs = jnp.where(earlier[:, :, None, None], exclusive[:, None] - inclusive[None, :], -jnp.inf)
    local = jnp.einsum(
        "cbgr,bgrpn->cgrpn", jnp.exp(pairs), block_states, precision=lax.Precision.HIGHEST
    )
    entering_blocks = jnp.exp(exclusive)[..., None, None] * entering[None] + local
    outside = jnp.exp(running)[..., None] * jnp.einsum(
        "clgn,cgrpn->clgrp",
        block_queries,
        entering_blocks.astype(jnp.bfloat16),
        preferred_element_type=jnp.float32,
    )
    combined = inside + outside
    return combined.reshape(count * BLK, combined.shape[2], combined.shape[3], combined.shape[4])


def on_device(
    residual,
    value_projected,
    gate_projected,
    wide_key_rows,
    wide_query_rows,
    narrow_key_rows,
    narrow_query_rows,
    step_before_softplus,
    extra_log_decay,
    log_decay_rate,
    value_kernel,
    wide_key_kernel,
    wide_query_kernel,
    narrow_key_kernel,
    narrow_query_kernel,
    head_norm_gain,
    output_matrix,
    feedforward_norm_gain,
    gate_matrix,
    up_matrix,
    down_matrix,
):
    margin = CONV_W - 1
    rims = passed_along(
        (
            value_projected[-margin:],
            wide_key_rows[-margin:],
            wide_query_rows[-margin:],
            narrow_key_rows[-margin:],
            narrow_query_rows[-margin:],
        ),
        "sp",
        1,
    )
    length = value_projected.shape[0]
    per_group = HEADS // GROUPS
    half = value_projected.shape[1] // (per_group * HEAD_DIM) // 2
    values = conv_local(value_projected, rims[0], value_kernel).reshape(
        length, half, 2, per_group, HEAD_DIM
    )
    keys_w = conv_local(wide_key_rows, rims[1], wide_key_kernel).reshape(length, half, STATE_WIDE)
    queries_w = conv_local(wide_query_rows, rims[2], wide_query_kernel).reshape(
        length, half, STATE_WIDE
    )
    keys_n = conv_local(narrow_key_rows, rims[3], narrow_key_kernel).reshape(
        length, half, STATE_NARROW
    )
    queries_n = conv_local(narrow_query_rows, rims[4], narrow_query_kernel).reshape(
        length, half, STATE_NARROW
    )
    step_sizes = jax.nn.softplus(step_before_softplus)
    decay_factor = -jnp.exp(log_decay_rate)[None, :] * step_sizes + extra_log_decay
    step_sizes = step_sizes.reshape(length, half, 2, per_group)
    decay_factor = decay_factor.reshape(length, half, 2, per_group)
    wide_parts = family_local(
        values[:, :, 0], step_sizes[:, :, 0], decay_factor[:, :, 0], keys_w, queries_w
    )
    narrow_parts = family_local(
        values[:, :, 1], step_sizes[:, :, 1], decay_factor[:, :, 1], keys_n, queries_n
    )
    whole_w, summary_w = device_summary(wide_parts[2], wide_parts[3])
    whole_n, summary_n = device_summary(narrow_parts[2], narrow_parts[3])
    stacked = jnp.stack([whole_w, whole_n])

    def combine(earlier, later):
        return (
            earlier[0] + later[0],
            jnp.exp(later[0][0])[..., None, None] * earlier[1] + later[1],
            jnp.exp(later[0][1])[..., None, None] * earlier[2] + later[2],
        )

    identity = (jnp.zeros_like(stacked), jnp.zeros_like(summary_w), jnp.zeros_like(summary_n))
    prefix = entering_2((stacked, summary_w, summary_n), "sp", combine, identity)
    entering_w = prefix[1]
    entering_n = prefix[2]
    mixed_w = family_output(wide_parts, entering_w)
    mixed_n = family_output(narrow_parts, entering_n)
    heads_out = jnp.stack([mixed_w, mixed_n], axis=2).reshape(length, -1, HEAD_DIM)
    gated = heads_out * jax.nn.silu(gate_projected.astype(jnp.float32)).reshape(
        length, -1, HEAD_DIM
    )
    gated = gated * lax.rsqrt(jnp.mean(gated * gated, axis=-1, keepdims=True) + 1e-06)
    normed = (gated.reshape(length, -1) * head_norm_gain.astype(jnp.float32)).astype(jnp.bfloat16)
    projected = lax.psum_scatter(
        jnp.dot(normed, output_matrix, preferred_element_type=jnp.float32).astype(jnp.bfloat16),
        "tp",
        scatter_dimension=0,
        tiled=True,
    ).astype(jnp.float32)
    after_mixer = (residual.astype(jnp.float32) + projected).astype(jnp.bfloat16)
    rows = after_mixer.astype(jnp.float32)
    x_norm = (
        rows
        * lax.rsqrt(jnp.mean(rows * rows, axis=-1, keepdims=True) + 1e-06)
        * feedforward_norm_gain.astype(jnp.float32)
    ).astype(jnp.bfloat16)
    gate_full, up_full, down_full = collect_weights(gate_matrix, up_matrix, down_matrix)
    piece = lax.all_gather(x_norm, "tp", axis=0, tiled=True)
    gate_values = jnp.dot(piece, gate_full, preferred_element_type=jnp.float32)
    up_values = jnp.dot(piece, up_full, preferred_element_type=jnp.float32)
    hidden = (jax.nn.silu(gate_values) * up_values).astype(jnp.bfloat16)
    channel = lax.psum_scatter(
        lax.dot_general(
            hidden, down_full, (((1,), (1,)), ((), ())), preferred_element_type=jnp.float32
        ).astype(jnp.bfloat16),
        "tp",
        scatter_dimension=0,
        tiled=True,
    ).astype(jnp.float32)
    return (after_mixer.astype(jnp.float32) + 0.5 * channel).astype(jnp.bfloat16)


def solution(mesh):
    in_specs = (
        P(("grp", "sp", "tp"), None),
        P(("grp", "sp"), "tp"),
        P(("grp", "sp"), "tp"),
        P(("grp", "sp"), "tp"),
        P(("grp", "sp"), "tp"),
        P(("grp", "sp"), "tp"),
        P(("grp", "sp"), "tp"),
        P(("grp", "sp"), "tp"),
        P(("grp", "sp"), "tp"),
        P("tp"),
        P(None, "tp"),
        P(None, "tp"),
        P(None, "tp"),
        P(None, "tp"),
        P(None, "tp"),
        P("tp"),
        P("tp", None),
        P(),
        P("sp", "tp"),
        P("sp", "tp"),
        P("sp", "tp"),
    )
    out_specs = P(("grp", "sp", "tp"), None)
    return jax.shard_map(
        on_device, mesh=mesh, in_specs=in_specs, out_specs=out_specs, check_vma=False
    )
```

profile of v0, /device:TPU:0, one launch (start us, length us, event | category | flops | bytes accessed | tf_op | source)
XLA Modules:
  0.0 493.6 jit_solution(6619962394763698357)
XLA Ops:
  9.0 5.7 %collective-permute-start = (bf16[3,1024]{0,1:T(8,128)(2,1)}, bf16[3,1024]{0,1:T(8,128)(2,1)}, u32[]{:S(2)}, u32[]{:S(2)}) collective-permute-start(bf16[3,1024]{0,1:T(8,128)(2,1)} %copy.149), channel_id=1, source_target_pairs={{0,4},{4,8},{8,12},{1,5},{5,9},{9,13},{2,6},{6,10},{10,14},{3,7},{... | collective-permute-start | bytes 18440 | tf_op jit(solution)/shard_map/ppermute | solution.py:18
  15.4 2.8 collective-permute-start.1
  18.8 3.5 collective-permute-start.3
  22.3 1.3 slice.223
  23.6 1.9 collective-permute-start.4
  25.5 1.3 slice.196
  26.8 2.5 collective-permute-start.2
  29.3 2.6 copy.150
  32.6 13.2 %fusion.102 = f32[12,64,2,4]{3,0,1,2:T(8,128)S(1)} fusion(f32[12,64,2,4]{3,0,1,2:T(8,128)S(1)} %copy.155), kind=kOutput, calls=%fused_computation.202 | output fusion | flops 387072 | bytes 49152 | tf_op jit(solution)/shard_map/jit(cumsum)/reduce_window_sum | solution.py:69
  46.5 1.5 copy.164
  47.9 1.4 fusion.103
  51.1 1.0 copy.184
  52.2 1.5 copy.173
  55.5 1.0 copy.156
  56.6 1.5 copy.167
  61.3 2.8 fusion.101
  64.1 1.7 copy.168
  65.8 7.9 %all_gather.28 = bf16[4,2,2,4]{3,2,1,0:T(2,128)(2,1)S(1)} all-gather(bf16[1,2,2,4]{3,2,1,0:T(2,128)(2,1)S(1)} %pad_maximum_fusion), channel_id=1, replica_groups=mesh['grp'=2,'sp'=4,'tp'=4] {'sp'}, dimensions={0}, use_global_device_ids=true | all-gather | bytes 160 | tf_op jit(solution)/shard_map/all_gather | solution.py:24
  74.3 1.7 copy.194
  76.1 2.5 convert_multiply_fusion
  78.6 1.7 fusion.100
  80.3 2.3 copy.174
  82.6 2.2 copy.188
  84.7 2.2 copy.161
  88.9 1.2 copy.183
  92.5 1.2 convolution_bitcast_fusion.1
  93.7 2.3 copy.153
  96.0 1.8 maximum_convert_fusion
  97.9 3.5 multiply_convert_fusion.4
  101.4 1.0 fusion.99
  102.4 1.8 reshape_squeeze.16
  104.7 0.9 copy-done.4
  106.4 3.9 fusion.6
  110.3 16.2 %all-gather = bf16[8,4,64,128]{3,2,1,0:T(8,128)(2,1)} all-gather(bf16[2,4,64,128]{3,2,1,0:T(8,128)(2,1)S(1)} %convert_element_type.180), channel_id=2, replica_groups=mesh['grp'=2,'sp'=4,'tp'=4] {'sp'}, dimensions={0}, use_global_device_ids=true | all-gather | bytes 655360 | tf_op jit(solution)/shard_map/all_gather | solution.py:24
  126.5 3.8 reshape_squeeze.19
  130.2 2.1 multiply_convert_fusion
  133.1 1.6 copy-done
  134.7 3.9 fusion.2
  138.6 16.4 %all-gather.1 = bf16[8,4,64,64]{3,2,1,0:T(8,128)(2,1)} all-gather(bf16[2,4,64,64]{3,2,1,0:T(8,128)(2,1)S(1)} %convert_element_type.185), channel_id=3, replica_groups=mesh['grp'=2,'sp'=4,'tp'=4] {'sp'}, dimensions={0}, use_global_device_ids=true | all-gather | bytes 327680 | tf_op jit(solution)/shard_map/all_gather | solution.py:24
  156.5 8.7 %fusion.10 = bf16[12,2,4,64,64]{4,0,3,2,1:T(8,128)(2,1)S(1)} fusion(f32[12,2,4,64,64]{4,3,2,1,0:T(8,128)} %copy-done, f32[2,4,64,64]{3,2,1,0:T(8,128)} %get-tuple-element.65, f32[12,2,4]{0,2,1:T(4,128)S(1)} %copy-done.38, f32[12,2,4]{0,2,1:T(4,128)S(1)} %reduce_window_sum.43, f32[12,2,4]{0,2,1:T(4,128)S(1)} %copy-done.36, ...), kind=kOutput, calls=%fused_computation.16 | convolution fusion | flops 57805056 | bytes 2491664 | tf_op jit(solution)/shard_map/cbgr,bgrpn->cgrpn/dot_general | solution.py:104
  165.3 1.1 fusion.29
  166.5 1.0 fusion.20
  167.5 3.8 copy.192
  171.3 4.6 stack_reshape.7
  175.9 6.4 %fusion.11 = bf16[12,2,4,64,128]{4,0,3,2,1:T(8,128)(2,1)S(1)} fusion(f32[12,2,4,64,128]{4,3,2,1,0:T(8,128)S(1)} %fusion.39, f32[2,4,64,128]{3,2,1,0:T(8,128)S(1)} %get-tuple-element.64, f32[12,2,4]{0,2,1:T(4,128)S(1)} %copy-done.37, f32[12,2,4]{0,2,1:T(4,128)S(1)} %reduce_window_sum.41, f32[12,2,4]{0,2,1:T(4,128)S(1)} %copy-done.35, ...), kind=kOutput, calls=%fused_computation.18 | convolution fusion | flops 115607808 | bytes 4982032 | tf_op jit(solution)/shard_map/cbgr,bgrpn->cgrpn/dot_general | solution.py:104
  182.4 1.1 fusion.28
  183.6 1.0 fusion.21
  184.6 3.8 copy.180
  188.4 3.5 stack_reshape.6
  192.1 1.9 copy.193
  194.1 1.1 copy-done.3
  196.6 3.1 fusion.19
  199.7 5.1 %convolution_convert_fusion.1 = bf16[768,2048]{1,0:T(8,128)(2,1)} fusion(bf16[768,1024]{0,1:T(8,128)(2,1)S(1)} %fusion.19, bf16[1024,2048]{1,0:T(8,128)(2,1)S(1)} %copy-done.59), kind=kOutput, calls=%fused_computation.24 | convolution fusion | flops 3222798336 | bytes 8912896 | tf_op jit(solution)/shard_map/dot_general | solution.py:203
  205.5 45.7 %reduce-scatter.3.cloned.1.call-done = bf16[192,2048]{1,0:T(8,128)(2,1)} async-done(((bf16[768,2048]{1,0:T(8,128)(2,1)}), bf16[192,2048]{1,0:T(8,128)(2,1)}) %reduce-scatter.3.cloned.1.call-update) | async-done | bytes 786448 | tf_op jit(solution)/shard_map/reduce_scatter | solution.py:202
  251.2 1.5 fusion.30
  252.7 2.3 fusion.32
  256.4 22.1 %all-gather.9.cloned.1.call-done = bf16[2048,768]{1,0:T(8,128)(2,1)} async-done(((bf16[512,768]{1,0:T(8,128)(2,1)}), bf16[2048,768]{1,0:T(8,128)(2,1)}) %all-gather.9.cloned.1.call-update) | async-done | bytes 3145744 | tf_op jit(solution)/shard_map/all_gather | solution.py:45
  278.5 28.5 %all-gather.7.cloned.1.call-done = bf16[768,2048]{1,0:T(8,128)(2,1)} async-done(((bf16[192,2048]{1,0:T(8,128)(2,1)}), bf16[768,2048]{1,0:T(8,128)(2,1)}) %all-gather.7.cloned.1.call-update) | async-done | bytes 3145744 | tf_op jit(solution)/shard_map/all_gather | solution.py:216
  307.0 5.4 %fusion.104 = f32[768,768]{1,0:T(8,128)S(1)} fusion(bf16[768,2048]{1,0:T(8,128)(2,1)} %all-gather.7.cloned.1.call-done, bf16[2048,768]{1,0:T(8,128)(2,1)} %all-gather.9.cloned.1.call-done), kind=kOutput, calls=%fused_computation.204 | convolution fusion | flops 2415919104 | bytes 8650752 | tf_op jit(solution)/shard_map/dot_general | solution.py:217
  312.5 59.3 %all-gather.11.cloned.1.call-done = bf16[2048,768]{1,0:T(8,128)(2,1)} async-done(((bf16[512,768]{1,0:T(8,128)(2,1)}), bf16[2048,768]{1,0:T(8,128)(2,1)}) %all-gather.11.cloned.1.call-update) | async-done | bytes 3145744 | tf_op jit(solution)/shard_map/all_gather | solution.py:46
  371.8 63.6 %all-gather.13.cloned.1.call-done = bf16[2048,768]{1,0:T(8,128)(2,1)} async-done(((bf16[512,768]{1,0:T(8,128)(2,1)}), bf16[2048,768]{1,0:T(8,128)(2,1)}) %all-gather.13.cloned.1.call-update) | async-done | bytes 3145744 | tf_op jit(solution)/shard_map/all_gather | solution.py:47
  435.4 11.2 %convolution_convert_fusion = bf16[768,2048]{1,0:T(8,128)(2,1)} fusion(bf16[2048,768]{1,0:T(8,128)(2,1)} %all-gather.13.cloned.1.call-done, f32[768,768]{1,0:T(8,128)S(1)} %fusion.104, bf16[768,2048]{1,0:T(8,128)(2,1)} %all-gather.7.cloned.1.call-done, bf16[2048,768]{1,0:T(8,128)(2,1)} %all-gather.11.cloned.1.call-done), kind=kOutput, calls=%fused_computation.23 | convolution fusion | flops 4836950016 | bytes 14942208 | tf_op jit(solution)/shard_map/dot_general | solution.py:221
  446.6 36.7 %reduce-scatter.5.cloned.1.call-done = bf16[192,2048]{1,0:T(8,128)(2,1)} async-done(((bf16[768,2048]{1,0:T(8,128)(2,1)}), bf16[192,2048]{1,0:T(8,128)(2,1)}) %reduce-scatter.5.cloned.1.call-update) | async-done | bytes 786448 | tf_op jit(solution)/shard_map/reduce_scatter | solution.py:220
  483.3 2.4 fusion.33
  (208 shorter events, 23.5 us)
Async XLA Ops:
  7.4 24.5 %copy-start.60 = (f32[16]{0:T(128)S(1)}, f32[16]{0:T(128)}, u32[]{:S(2)}) copy-start(f32[16]{0:T(128)} %param.32) | copy-start | bytes 196
  7.4 24.5 %copy-start.31 = (f32[768,16]{0,1:T(8,128)S(1)}, f32[768,16]{0,1:T(8,128)}, u32[]{:S(2)}) copy-start(f32[768,16]{0,1:T(8,128)} %param.30) | copy-start | bytes 147460
  7.4 24.5 %copy-start.30 = (f32[768,16]{0,1:T(8,128)S(1)}, f32[768,16]{0,1:T(8,128)}, u32[]{:S(2)}) copy-start(f32[768,16]{0,1:T(8,128)} %param.31) | copy-start | bytes 147460
  7.4 243.8 %reduce-scatter.3.cloned.1.call-start = ((), (), s32[]{:S(2)}) async-start(), calls=%async_computation.2 | async-start | bytes 3932160 | tf_op jit(solution)/shard_map/reduce_scatter | solution.py:202
  9.0 87.0 %collective-permute-start = (bf16[3,1024]{0,1:T(8,128)(2,1)}, bf16[3,1024]{0,1:T(8,128)(2,1)}, u32[]{:S(2)}, u32[]{:S(2)}) collective-permute-start(bf16[3,1024]{0,1:T(8,128)(2,1)} %copy.149), channel_id=1, source_target_pairs={{0,4},{4,8},{8,12},{1,5},{5,9},{9,13},{2,6},{6,10},{10,14},{3,7},{... | collective-permute-start | bytes 18440 | tf_op jit(solution)/shard_map/ppermute | solution.py:18
  15.4 74.8 %collective-permute-start.1 = (bf16[3,256]{1,0:T(4,128)(2,1)S(1)}, bf16[3,256]{1,0:T(4,128)(2,1)S(1)}, u32[]{:S(2)}, u32[]{:S(2)}) collective-permute-start(bf16[3,256]{1,0:T(4,128)(2,1)S(1)} %slice.187), channel_id=1, source_target_pairs={{0,4},{4,8},{8,12},{1,5},{5,9},{9,13},{2,6},{6,10},{10,14},{3,7},{... | collective-permute-start | bytes 4616 | tf_op jit(solution)/shard_map/ppermute | solution.py:18
  18.8 68.7 %collective-permute-start.3 = (bf16[3,128]{1,0:T(4,128)(2,1)S(1)}, bf16[3,128]{1,0:T(4,128)(2,1)S(1)}, u32[]{:S(2)}, u32[]{:S(2)}) collective-permute-start(bf16[3,128]{1,0:T(4,128)(2,1)S(1)} %slice.214), channel_id=1, source_target_pairs={{0,4},{4,8},{8,12},{1,5},{5,9},{9,13},{2,6},{6,10},{10,14},{3,7},{... | collective-permute-start | bytes 2312 | tf_op jit(solution)/shard_map/ppermute | solution.py:18
  23.6 64.4 %collective-permute-start.4 = (bf16[3,128]{1,0:T(4,128)(2,1)}, bf16[3,128]{1,0:T(4,128)(2,1)S(1)}, u32[]{:S(2)}, u32[]{:S(2)}) collective-permute-start(bf16[3,128]{1,0:T(4,128)(2,1)} %slice.223), channel_id=1, source_target_pairs={{0,4},{4,8},{8,12},{1,5},{5,9},{9,13},{2,6},{6,10},{10,14},{3,7},{... | collective-permute-start | bytes 2312 | tf_op jit(solution)/shard_map/ppermute | solution.py:18
  26.8 64.1 %collective-permute-start.2 = (bf16[3,256]{1,0:T(4,128)(2,1)}, bf16[3,256]{1,0:T(4,128)(2,1)}, u32[]{:S(2)}, u32[]{:S(2)}) collective-permute-start(bf16[3,256]{1,0:T(4,128)(2,1)} %slice.196), channel_id=1, source_target_pairs={{0,4},{4,8},{8,12},{1,5},{5,9},{9,13},{2,6},{6,10},{10,14},{3,7},{... | collective-permute-start | bytes 4616 | tf_op jit(solution)/shard_map/ppermute | solution.py:18
  47.9 10.8 %copy-start.32 = (bf16[4,1024]{1,0:T(4,128)(2,1)S(1)}, bf16[4,1024]{1,0:T(4,128)(2,1)}, u32[]{:S(2)}) copy-start(bf16[4,1024]{1,0:T(4,128)(2,1)} %param.33) | copy-start | bytes 24580
  47.9 11.4 %copy-start.45 = (bf16[4,256]{1,0:T(4,128)(2,1)S(1)}, bf16[4,256]{1,0:T(4,128)(2,1)}, u32[]{:S(2)}) copy-start(bf16[4,256]{1,0:T(4,128)(2,1)} %param.34) | copy-start | bytes 6148
  47.9 12.6 %copy-start.48 = (bf16[4,128]{1,0:T(4,128)(2,1)S(1)}, bf16[4,128]{1,0:T(4,128)(2,1)}, u32[]{:S(2)}) copy-start(bf16[4,128]{1,0:T(4,128)(2,1)} %param.36) | copy-start | bytes 3076
  56.6 17.1 %copy-start.49 = (bf16[4,128]{1,0:T(4,128)(2,1)S(1)}, bf16[4,128]{1,0:T(4,128)(2,1)}, u32[]{:S(2)}) copy-start(bf16[4,128]{1,0:T(4,128)(2,1)} %param.37) | copy-start | bytes 3076
  56.6 17.1 %copy-start.46 = (bf16[4,256]{1,0:T(4,128)(2,1)S(1)}, bf16[4,256]{1,0:T(4,128)(2,1)}, u32[]{:S(2)}) copy-start(bf16[4,256]{1,0:T(4,128)(2,1)} %param.35) | copy-start | bytes 6148
  76.1 4.2 copy-start.1
  76.1 2.5 copy-start.11
  78.6 8.4 %copy-start.58 = (bf16[1024]{0:T(1024)(128)(2,1)S(1)}, bf16[1024]{0:T(1024)(128)(2,1)}, u32[]{:S(2)}) copy-start(bf16[1024]{0:T(1024)(128)(2,1)} %param.38) | copy-start | bytes 6148
  78.6 9.0 %copy-start.22 = (bf16[768,128]{1,0:T(8,128)(2,1)S(1)}, bf16[768,128]{1,0:T(8,128)(2,1)}, u32[]{:S(2)}) copy-start(bf16[768,128]{1,0:T(8,128)(2,1)} %param.28) | copy-start | bytes 589828
  80.3 7.8 %copy-start.23 = (bf16[768,128]{1,0:T(8,128)(2,1)S(1)}, bf16[768,128]{1,0:T(8,128)(2,1)}, u32[]{:S(2)}) copy-start(bf16[768,128]{1,0:T(8,128)(2,1)} %param.29) | copy-start | bytes 589828
  88.0 2.1 copy-start.20
  88.1 2.1 copy-start.50
  88.1 2.1 copy-start.51
  88.1 2.1 copy-start.52
  88.1 2.1 copy-start.53
  88.6 2.2 copy-start.12
  90.1 1.8 copy-start.54
  90.1 1.8 copy-start.55
  90.1 1.8 copy-start.56
  90.1 1.8 copy-start.57
  90.9 2.9 copy-start.16
  91.9 4.1 copy-start.9
  92.5 5.3 %copy-start.14 = (bf16[12,64,2,128]{3,2,1,0:T(2,128)(2,1)}, bf16[12,64,2,128]{3,2,1,0:T(2,128)(2,1)S(1)}, u32[]{:S(2)}) copy-start(bf16[12,64,2,128]{3,2,1,0:T(2,128)(2,1)S(1)} %reshape_reshape.13) | copy-start | bytes 1179652
  96.0 1.8 copy-start.40
  96.0 1.8 copy-start.41
  96.0 1.9 copy-start.42
  96.0 1.9 copy-start.43
  104.2 1.4 copy-start.4
  104.2 1.4 copy-start.17
  132.3 2.4 copy-start.33
  133.1 1.6 copy-start
  156.5 8.7 %copy-start.6 = (bf16[12,64,2,4,64]{1,0,4,3,2:T(8,128)(2,1)S(1)}, bf16[12,64,2,4,64]{1,0,4,3,2:T(8,128)(2,1)}, u32[]{:S(2)}) copy-start(bf16[12,64,2,4,64]{1,0,4,3,2:T(8,128)(2,1)} %reshape_squeeze.19) | copy-start | bytes 2359300
  156.5 8.8 %copy-start.18 = (f32[12,64,64,2]{2,1,3,0:T(8,128)S(1)}, f32[12,64,64,2]{2,1,3,0:T(8,128)}, u32[]{:S(2)}) copy-start(f32[12,64,64,2]{2,1,3,0:T(8,128)} %copy.183) | copy-start | bytes 1179652
  156.5 8.8 %copy-start.27 = (f32[12,64,2,4]{1,3,2,0:T(4,128)S(1)}, f32[12,64,2,4]{1,3,2,0:T(4,128)}, u32[]{:S(2)}) copy-start(f32[12,64,2,4]{1,3,2,0:T(4,128)} %copy.184) | copy-start | bytes 73732
  156.5 8.8 %copy-start.29 = (f32[12,64,2,4]{1,3,2,0:T(4,128)S(1)}, f32[12,64,2,4]{1,3,2,0:T(4,128)}, u32[]{:S(2)}) copy-start(f32[12,64,2,4]{1,3,2,0:T(4,128)} %copy.186) | copy-start | bytes 73732
  156.5 8.8 %copy-start.44 = (pred[64,64]{1,0:T(8,128)(4,1)S(1)}, pred[64,64]{1,0:T(8,128)(4,1)}, u32[]{:S(2)}) copy-start(pred[64,64]{1,0:T(8,128)(4,1)} %iota_compare_fusion) | copy-start | bytes 12292
  165.3 1.2 copy-start.13
  171.3 4.6 copy-start.35
  171.3 4.6 copy-start.37
  175.9 6.4 %copy-start.5 = (bf16[12,64,2,4,64]{1,0,4,3,2:T(8,128)(2,1)S(1)}, bf16[12,64,2,4,64]{1,0,4,3,2:T(8,128)(2,1)}, u32[]{:S(2)}) copy-start(bf16[12,64,2,4,64]{1,0,4,3,2:T(8,128)(2,1)} %copy-done.4) | copy-start | bytes 2359300
  175.9 6.4 %copy-start.19 = (f32[12,64,64,2]{2,1,3,0:T(8,128)S(1)}, f32[12,64,64,2]{2,1,3,0:T(8,128)}, u32[]{:S(2)}) copy-start(f32[12,64,64,2]{2,1,3,0:T(8,128)} %copy.153) | copy-start | bytes 1179652
  175.9 6.4 %copy-start.26 = (f32[12,64,2,4]{1,3,2,0:T(4,128)S(1)}, f32[12,64,2,4]{1,3,2,0:T(4,128)}, u32[]{:S(2)}) copy-start(f32[12,64,2,4]{1,3,2,0:T(4,128)} %copy.156) | copy-start | bytes 73732
  175.9 6.4 %copy-start.28 = (f32[12,64,2,4]{1,3,2,0:T(4,128)S(1)}, f32[12,64,2,4]{1,3,2,0:T(4,128)}, u32[]{:S(2)}) copy-start(f32[12,64,2,4]{1,3,2,0:T(4,128)} %copy.159) | copy-start | bytes 73732
  188.4 3.6 copy-start.10
  192.1 3.0 copy-start.3
  195.1 1.4 copy-start.2
  195.1 1.4 copy-start.39
  196.6 3.1 copy-start.59
  204.8 46.4 %copy-start.7 = (bf16[192,2048]{1,0:T(8,128)(2,1)S(1)}, bf16[192,2048]{1,0:T(8,128)(2,1)}, u32[]{:S(2)}) copy-start(bf16[192,2048]{1,0:T(8,128)(2,1)} %param.23) | copy-start | bytes 2359300
  204.9 73.7 %all-gather.9.cloned.1.call-start = ((), (), s32[]{:S(2)}) async-start(), calls=%async_computation.4 | async-start | bytes 3932160 | tf_op jit(solution)/shard_map/all_gather | solution.py:45
  205.4 101.6 %all-gather.7.cloned.1.call-start = ((), (), s32[]{:S(2)}) async-start(), calls=%async_computation.3 | async-start | bytes 3932160 | tf_op jit(solution)/shard_map/all_gather | solution.py:216
  255.0 116.8 %all-gather.11.cloned.1.call-start = ((), (), s32[]{:S(2)}) async-start(), calls=%async_computation.5 | async-start | bytes 3932160 | tf_op jit(solution)/shard_map/all_gather | solution.py:46
  255.6 179.7 %all-gather.13.cloned.1.call-start = ((), (), s32[]{:S(2)}) async-start(), calls=%async_computation.6 | async-start | bytes 3932160 | tf_op jit(solution)/shard_map/all_gather | solution.py:47
  256.4 226.9 %reduce-scatter.5.cloned.1.call-start = ((), (), s32[]{:S(2)}) async-start(), calls=%async_computation.7 | async-start | bytes 3932160 | tf_op jit(solution)/shard_map/reduce_scatter | solution.py:220
  446.6 36.7 %copy-start.8 = (bf16[192,2048]{1,0:T(8,128)(2,1)S(1)}, bf16[192,2048]{1,0:T(8,128)(2,1)}, u32[]{:S(2)}) copy-start(bf16[192,2048]{1,0:T(8,128)(2,1)} %reduce-scatter.3.cloned.1.call-done) | copy-start | bytes 2359300
  (8 other events, 7.3 us)
Sparse Core Ops, SparseCore 0:
  205.0 46.1 reduce-scatter.2
  446.7 36.5 reduce-scatter.4
Sparse Core Ops, SparseCore 1:
  206.9 71.6 all-gather.8
  280.0 27.0 all-gather.6
  308.5 63.3 all-gather.10
  373.4 61.9 all-gather.12
where the time goes:
time: 499 us; the launch traced here: 494 us
  waiting for transfers between devices  258 us (52%)
  local copies, waits for them, and re-layouts  62.3 us (12%)
  matrix products  52 us (10%)
  other arithmetic  48.2 us (10%)
  blocking collectives  40.5 us (8%)
  starting transfers between devices  16.5 us (3%)
  between operations  16.2 us (3%)
    all_gather x1, waiting for transfers between devices, collect_weights(): lax.all_gather(down_matrix, 'sp', axis=0, tiled=True)  63.6 us
    all_gather x1, waiting for transfers between devices, collect_weights(): lax.all_gather(up_matrix, 'sp', axis=0, tiled=True)  59.3 us
    reduce_scatter x1, waiting for transfers between devices, on_device(): lax.psum_scatter(jnp.dot(normed, output_matrix, preferred_element_type=jn...  45.7 us
    all_gather x3, blocking collectives, entering_2(): lax.all_gather(a.astype(kind), axis)  40.5 us
    reduce_scatter x1, waiting for transfers between devices, on_device(): lax.psum_scatter(lax.dot_general(hidden, down_full, (((1,), (1,)), ((), (...  36.7 us
    all_gather x1, waiting for transfers between devices, on_device(): piece = lax.all_gather(x_norm, 'tp', axis=0, tiled=True)  28.5 us
    all_gather x1, waiting for transfers between devices, collect_weights(): lax.all_gather(gate_matrix, 'sp', axis=0, tiled=True)  22.1 us
    ppermute x5, starting transfers between devices, passed_along(): lax.ppermute(value, axis, [(source, source + steps) for source in range(i...  16.3 us
  transfers between devices with their start and end apart: 11, of which 6 were waited for; matrix products, arithmetic and copies ran while one was open for 14% of the time, Pallas kernels for 0%

commit v1 on v0

v1 whole, which is shorter than its diff:
```python
import functools
import jax
import jax.numpy as jnp
from jax import lax
from jax.experimental import pallas as pl
from jax.experimental.pallas import tpu as pltpu
from jax.sharding import PartitionSpec as P


HEAD_DIM = 64
PER_GROUP = 4
GROUP_COLS = HEAD_DIM * PER_GROUP
STATE_WIDE = 128
STATE_NARROW = 64
CHUNK = 128
TAIL = 16
FADE_ROWS = 16
F32 = jnp.float32
BF16 = jnp.bfloat16


def silu(x):
    half = 0.5 * x
    return half + half * jnp.tanh(half)


def spread(values, table):
    high = values.astype(BF16).astype(F32)
    low = values - high
    return jnp.dot(
        jnp.concatenate([high, low], axis=1).astype(BF16), table, preferred_element_type=F32
    )


def head_table(heads, columns):
    head = lax.broadcasted_iota(jnp.int32, (2 * heads, columns), 0)
    head = jnp.where(head >= heads, head - heads, head)
    column = lax.broadcasted_iota(jnp.int32, (2 * heads, columns), 1)
    inside = (column >= head * HEAD_DIM) & (column < (head + 1) * HEAD_DIM)
    return jnp.where(inside, 1.0, 0.0).astype(BF16)


def narrow_mask(place, rows, lanes):
    lane = lax.broadcasted_iota(jnp.int32, (rows, lanes), 1)
    start = place * STATE_NARROW
    return (lane >= start) & (lane < start + STATE_NARROW)


def tails_body(*refs):
    out_ref = refs[-1]
    offset = 0
    for ref in refs[:-1]:
        out_ref[:, offset : offset + ref.shape[1]] = ref[...]
        offset += ref.shape[1]


def tails_call(raw):
    length = raw[0].shape[0]
    width = sum(a.shape[1] for a in raw)
    return pl.pallas_call(
        tails_body,
        grid=(1,),
        in_specs=[
            pl.BlockSpec((TAIL, a.shape[1]), lambda i: (length // TAIL - 1, 0)) for a in raw
        ],
        out_specs=pl.BlockSpec((TAIL, width), lambda i: (0, 0)),
        out_shape=jax.ShapeDtypeStruct((TAIL, width), BF16),
        name="tails",
    )(*raw)


def local_body(
    value_ref,
    kw_ref,
    qw_ref,
    kn_ref,
    qn_ref,
    step_ref,
    extra_ref,
    rate_ref,
    rim_ref,
    value_taps,
    kw_taps,
    qw_taps,
    kn_taps,
    qn_taps,
    y_ref,
    q_ref,
    fade_ref,
    state_ref,
    raw,
    carried,
    before,
):
    turn = pl.program_id(0)
    chunk = value_ref.shape[0]
    heads = step_ref.shape[0]
    columns = value_ref.shape[1]
    table = head_table(heads, columns)

    @pl.when(turn == 0)
    def _():
        raw[0:8, :] = rim_ref[...].astype(F32)[TAIL - 8 :, :]
        carried[...] = jnp.zeros_like(carried)
        before[...] = jnp.zeros_like(before)

    @pl.when(turn > 0)
    def _():
        raw[0:8, :] = raw[chunk : chunk + 8, :]

    starts = []
    offset = 0
    for ref in (value_ref, kw_ref, qw_ref, kn_ref, qn_ref):
        starts.append(offset)
        raw[8 : 8 + chunk, offset : offset + ref.shape[1]] = ref[...].astype(F32)
        offset += ref.shape[1]

    def conv(which, start, width):
        taps_ref = (value_taps, kw_taps, qw_taps, kn_taps, qn_taps)[which]
        weights = taps_ref[:, start : start + width].astype(F32)
        taps = weights.shape[0]
        start = starts[which] + start
        total = None
        for tap in range(taps):
            first = 8 - (taps - 1) + tap
            term = raw[first : first + chunk, start : start + width] * weights[tap : tap + 1]
            total = term if total is None else total + term
        return silu(total).astype(BF16)

    step = jnp.log(1.0 + jnp.exp(step_ref[...].T))
    decay = extra_ref[...].T - jnp.exp(rate_ref[...]) * step
    row = lax.broadcasted_iota(jnp.int32, (chunk, chunk), 0)
    column = lax.broadcasted_iota(jnp.int32, (chunk, chunk), 1)
    lower = row >= column
    first = decay.astype(BF16).astype(F32)
    second = (decay - first).astype(BF16).astype(F32)
    terms = jnp.concatenate([first, second, decay - first - second], axis=1).astype(BF16)
    sums = jnp.dot(
        jnp.where(lower, 1.0, 0.0).astype(BF16), terms, preferred_element_type=F32
    )
    running = sums[:, :heads] + sums[:, heads : 2 * heads] + sums[:, 2 * heads :]
    middle = running[chunk // 2 - 1 : chunk // 2, :]
    total = running[chunk - 1 : chunk, :]
    since = jnp.exp(running)
    fade_ref[...] = jnp.exp(running + before[0:1, :])
    before[...] = before[...] + total
    factors = spread(
        jnp.concatenate(
            [
                jnp.exp(middle - running) * step,
                jnp.exp(running - middle),
                since[chunk // 2 - 8 : chunk // 2],
                since[chunk - 8 : chunk],
            ],
            axis=0,
        ),
        table,
    )
    to_middle = factors[:chunk]
    from_middle = factors[chunk : 2 * chunk]
    at_middle = factors[2 * chunk + 7 : 2 * chunk + 8, :]
    at_end = factors[2 * chunk + 15 : 2 * chunk + 16, :]
    middle_to_end = from_middle[chunk - 1 : chunk, :]

    groups = columns // GROUP_COLS
    for group in range(groups):
        place = group // 2
        lanes = slice(group * GROUP_COLS, (group + 1) * GROUP_COLS)
        values = conv(0, group * GROUP_COLS, GROUP_COLS)
        scaled = (values.astype(F32) * to_middle[:, lanes]).astype(BF16)
        if group % 2 == 0:
            keys = conv(1, place * STATE_WIDE, STATE_WIDE)
            queries = conv(2, place * STATE_WIDE, STATE_WIDE)
            q_ref[:, place * STATE_WIDE : (place + 1) * STATE_WIDE] = queries
        else:
            pair = place // 2
            inner = place % 2
            if inner == 0:
                keys_n = conv(3, pair * STATE_WIDE, STATE_WIDE)
                queries_n = conv(4, pair * STATE_WIDE, STATE_WIDE)
                first = kw_ref.shape[1] + pair * STATE_WIDE
                q_ref[:, first : first + STATE_WIDE] = queries_n
            mask = narrow_mask(inner, chunk, STATE_WIDE)
            keys = jnp.where(mask, keys_n, jnp.zeros_like(keys_n))
            queries = queries_n
        scores = lax.dot_general(
            queries, keys, (((1,), (1,)), ((), ())), preferred_element_type=F32
        )
        scores = jnp.where(lower, scores, 0.0).astype(BF16)
        state = carried[group]
        entering = (state * at_middle[:, lanes]).astype(BF16)
        mixed = jnp.dot(
            jnp.concatenate([scores, queries], axis=1),
            jnp.concatenate([scaled, entering], axis=0),
            preferred_element_type=F32,
        )
        y_ref[:, lanes] = mixed * from_middle[:, lanes]
        gained = lax.dot_general(
            keys, scaled, (((0,), (0,)), ((), ())), preferred_element_type=F32
        )
        carried[group] = state * at_end[:, lanes] + gained * middle_to_end[:, lanes]

    @pl.when(turn == pl.num_programs(0) - 1)
    def _():
        whole = spread(jnp.exp(before[...]), table)
        wide = (groups // 2) * STATE_WIDE
        last = state_ref.shape[0] - FADE_ROWS
        row = lax.broadcasted_iota(jnp.int32, (FADE_ROWS, GROUP_COLS), 0)
        fades = jnp.zeros((FADE_ROWS, GROUP_COLS), F32)
        for group in range(groups):
            place = group // 2
            lanes = slice(group * GROUP_COLS, (group + 1) * GROUP_COLS)
            fades = jnp.where(row == group, whole[0:1, lanes], fades)
            if group % 2 == 0:
                at = place * STATE_WIDE
                state_ref[at : at + STATE_WIDE, :] = carried[group].astype(BF16)
            else:
                inner = (place % 2) * STATE_NARROW
                at = wide + place * STATE_NARROW
                state_ref[at : at + STATE_NARROW, :] = carried[group][
                    inner : inner + STATE_NARROW, :
                ].astype(BF16)
        state_ref[last:, :] = fades.astype(BF16)


def joined(later, earlier):
    last = later.shape[0] - FADE_ROWS
    groups = last // (STATE_WIDE + STATE_NARROW) * 2
    wide = (groups // 2) * STATE_WIDE
    later, earlier = later.astype(F32), earlier.astype(F32)
    parts = []
    for place in range(groups // 2):
        rows = slice(place * STATE_WIDE, (place + 1) * STATE_WIDE)
        fade = later[last + 2 * place : last + 2 * place + 1]
        parts.append(fade * earlier[rows] + later[rows])
    for place in range(groups // 2):
        rows = slice(wide + place * STATE_NARROW, wide + (place + 1) * STATE_NARROW)
        fade = later[last + 2 * place + 1 : last + 2 * place + 2]
        parts.append(fade * earlier[rows] + later[rows])
    parts.append(later[last:] * earlier[last:])
    return jnp.concatenate(parts, axis=0).astype(BF16)


def join_body(later_ref, earlier_ref, out_ref):
    out_ref[...] = joined(later_ref[...], earlier_ref[...])


def join_call(later, earlier):
    return pl.pallas_call(
        join_body, out_shape=jax.ShapeDtypeStruct(later.shape, BF16), name="join_states"
    )(later, earlier)


def final_body(
    ids_ref, y_ref, q_ref, fade_ref, gate_ref, gain_ref, near_ref, far_ref, matrix_ref, out_ref, state, normed, matrix, arrived
):
    rows, columns = y_ref.shape
    heads = fade_ref.shape[1]
    table = head_table(heads, columns)
    turn = pl.program_id(0)
    copy = pltpu.make_async_copy(matrix_ref, matrix, arrived)

    @pl.when(turn == 0)
    def _():
        copy.start()
        state[...] = joined(near_ref[...], far_ref[...])

    fade = spread(fade_ref[...], table)
    groups = columns // GROUP_COLS
    wide = (groups // 2) * STATE_WIDE
    parts = []
    squares = []
    for group in range(groups):
        place = group // 2
        lanes = slice(group * GROUP_COLS, (group + 1) * GROUP_COLS)
        if group % 2 == 0:
            at = place * STATE_WIDE
            queries = q_ref[:, at : at + STATE_WIDE]
        else:
            at = wide + (place // 2) * STATE_WIDE
            queries = q_ref[:, at : at + STATE_WIDE]
            queries = jnp.where(
                narrow_mask(place % 2, rows, STATE_WIDE), queries, jnp.zeros_like(queries)
            )
        outer = jnp.dot(queries, state[at : at + STATE_WIDE, :], preferred_element_type=F32)
        mixed = y_ref[:, lanes] + outer * fade[:, lanes]
        gated = mixed * silu(gate_ref[:, lanes].astype(F32))
        parts.append(gated)
        square = (gated * gated).astype(BF16)
        squares.append(
            lax.dot_general(
                square,
                table[0:heads, lanes],
                (((1,), (1,)), ((), ())),
                preferred_element_type=F32,
            )
        )
    mean = functools.reduce(jnp.add, squares) * (1.0 / HEAD_DIM)
    scale = spread(lax.rsqrt(mean + 1e-06), table)
    at = pl.multiple_of(turn * rows, rows)
    for group in range(groups):
        lanes = slice(group * GROUP_COLS, (group + 1) * GROUP_COLS)
        gain = gain_ref[0:1, lanes].astype(F32)
        normed[pl.ds(at, rows), lanes] = (parts[group] * scale[:, lanes] * gain).astype(BF16)

    @pl.when(turn == pl.num_programs(0) - 1)
    def _():
        copy.wait()
        width = out_ref.shape[1]
        step = 512
        for start in range(0, width, step):
            product = jnp.dot(
                normed[...], matrix[:, start : start + step], preferred_element_type=F32
            )
            out_ref[:, start : start + step] = product.astype(out_ref.dtype)


def local_call(raw, step, extra, rate, rim, taps):
    length, columns = raw[0].shape
    heads = step.shape[0]
    chunk = CHUNK
    groups = columns // GROUP_COLS
    width = rim.shape[1]
    states = raw[1].shape[1] + raw[3].shape[1]

    def rows(array):
        return pl.BlockSpec((chunk, array.shape[1]), lambda i: (i, 0))

    def fixed(shape):
        return pl.BlockSpec(shape, lambda i: tuple(0 for _ in shape))

    turned = pl.BlockSpec((heads, chunk), lambda i: (0, i))
    return pl.pallas_call(
        local_body,
        grid=(length // chunk,),
        in_specs=[rows(a) for a in raw]
        + [turned, turned, fixed(rate.shape), fixed(rim.shape)]
        + [fixed(t.shape) for t in taps],
        out_specs=[
            pl.BlockSpec((chunk, columns), lambda i: (i, 0)),
            pl.BlockSpec((chunk, states), lambda i: (i, 0)),
            pl.BlockSpec((chunk, heads), lambda i: (i, 0)),
            fixed((states + FADE_ROWS, GROUP_COLS)),
        ],
        out_shape=[
            jax.ShapeDtypeStruct((length, columns), F32),
            jax.ShapeDtypeStruct((length, states), BF16),
            jax.ShapeDtypeStruct((length, heads), F32),
            jax.ShapeDtypeStruct((states + FADE_ROWS, GROUP_COLS), BF16),
        ],
        scratch_shapes=[
            pltpu.VMEM((8 + chunk, width), F32),
            pltpu.VMEM((groups, STATE_WIDE, GROUP_COLS), F32),
            pltpu.VMEM((8, heads), F32),
        ],
        compiler_params=pltpu.CompilerParams(dimension_semantics=("arbitrary",)),
        cost_estimate=pl.CostEstimate(
            flops=12_000_000_000, bytes_accessed=10_000_000, transcendentals=0
        ),
        name="mix_local",
    )(*raw, step, extra, rate, rim, *taps)


def final_call(ids, y, q, fade, gate, gain, near, far, matrix, rows_each, kind):
    columns = y.shape[1]
    width = matrix.shape[1]
    count = ids.shape[0]

    def rows(array):
        return pl.BlockSpec((rows_each, array.shape[1]), lambda i, ids: (ids[i], 0))

    def fixed(array):
        return pl.BlockSpec(array.shape, lambda i, ids: (0, 0))

    return pl.pallas_call(
        final_body,
        grid_spec=pltpu.PrefetchScalarGridSpec(
            num_scalar_prefetch=1,
            grid=(count,),
            in_specs=[rows(y), rows(q), rows(fade), rows(gate)]
            + [fixed(a) for a in (gain, near, far)]
            + [pl.BlockSpec(memory_space=pl.ANY)],
            out_specs=pl.BlockSpec((rows_each * count, width), lambda i, ids: (0, 0)),
            scratch_shapes=[
                pltpu.VMEM(near.shape, BF16),
                pltpu.VMEM((rows_each * count, columns), BF16),
                pltpu.VMEM(matrix.shape, BF16),
                pltpu.SemaphoreType.DMA,
            ],
        ),
        out_shape=jax.ShapeDtypeStruct((rows_each * count, width), kind),
        compiler_params=pltpu.CompilerParams(dimension_semantics=("arbitrary",)),
        cost_estimate=pl.CostEstimate(
            flops=6_000_000_000, bytes_accessed=10_000_000, transcendentals=0
        ),
        name="mix_final",
    )(ids, y, q, fade, gate, gain, near, far, matrix)


def settle_body(residual_ref, kept_ref, near_ref, far_ref, gain_ref, after_ref, norm_ref):
    total = kept_ref[...] + near_ref[...].astype(F32) + far_ref[...].astype(F32)
    after = (residual_ref[...].astype(F32) + total).astype(BF16)
    after_ref[...] = after
    wide = after.astype(F32)
    mean = jnp.mean(wide * wide, axis=-1, keepdims=True)
    norm_ref[...] = (wide * lax.rsqrt(mean + 1e-06) * gain_ref[...].astype(F32)).astype(BF16)


def settle_call(residual, kept, near, far, gain):
    rows, width = residual.shape
    top = pl.BlockSpec((rows // 2, width), lambda i: (i, 0))
    return pl.pallas_call(
        settle_body,
        grid=(2,),
        in_specs=[top] * 4 + [pl.BlockSpec(gain.shape, lambda i: (0, 0))],
        out_specs=[top, top],
        out_shape=[jax.ShapeDtypeStruct(residual.shape, BF16)] * 2,
        name="settle",
    )(residual, kept, near, far, gain)


def finish_body(after_ref, kept_ref, came_ref, l1_ref, l2_ref, r1_ref, r2_ref, out_ref):
    half = l1_ref.shape[1]
    share = kept_ref[...].astype(F32) + came_ref[...].astype(F32)
    left = share[:, :half] + l1_ref[...].astype(F32) + l2_ref[...].astype(F32)
    right = share[:, half:] + r1_ref[...].astype(F32) + r2_ref[...].astype(F32)
    out_ref[:, :half] = (after_ref[:, :half].astype(F32) + 0.5 * left).astype(BF16)
    out_ref[:, half:] = (after_ref[:, half:].astype(F32) + 0.5 * right).astype(BF16)


def finish_call(*arrays):
    rows, width = arrays[0].shape
    each = rows // 2
    return pl.pallas_call(
        finish_body,
        grid=(2,),
        in_specs=[pl.BlockSpec((each, a.shape[1]), lambda i: (i, 0)) for a in arrays],
        out_specs=pl.BlockSpec((each, width), lambda i: (i, 0)),
        out_shape=jax.ShapeDtypeStruct((rows, width), BF16),
        name="finish",
    )(*arrays)


def pick_body(part_ref, gate_ref, up_ref, down_ref, out_ref):
    columns = gate_ref.shape[1]
    for k, ref in enumerate((gate_ref, up_ref, down_ref)):
        out_ref[:, k * columns : (k + 1) * columns] = ref[...]


def pick_call(part, parts, weights):
    rows, columns = weights[0].shape
    columns //= parts
    return pl.pallas_call(
        pick_body,
        grid_spec=pltpu.PrefetchScalarGridSpec(
            num_scalar_prefetch=1,
            grid=(1,),
            in_specs=[pl.BlockSpec((rows, columns), lambda i, part: (0, part[0]))] * 3,
            out_specs=pl.BlockSpec((rows, 3 * columns), lambda i, part: (0, 0)),
        ),
        out_shape=jax.ShapeDtypeStruct((rows, 3 * columns), BF16),
        name="pick",
    )(part, *weights)


def feed_body(*refs):
    out_refs = refs[-4:-2]
    total, downs = refs[-2:]
    x_refs, weight_ref = refs[:-5], refs[-5]
    step = pl.program_id(0)
    depth = weight_ref.shape[0]
    columns = weight_ref.shape[1] // 3

    @pl.when(step == 0)
    def _():
        total[...] = jnp.zeros_like(total)

    downs[pl.ds(pl.multiple_of(step * depth, depth), depth), :] = weight_ref[:, 2 * columns :]
    x = jnp.concatenate([x_ref[...] for x_ref in x_refs], axis=0)
    total[...] += jnp.dot(x, weight_ref[:, : 2 * columns], preferred_element_type=F32)

    @pl.when(step == pl.num_programs(0) - 1)
    def _():
        rows, width = out_refs[0].shape
        hidden = (silu(total[:, :columns]) * total[:, columns:]).astype(BF16)
        for start in range(0, width, 512):
            product = lax.dot_general(
                hidden,
                downs[start : start + 512, :],
                (((1,), (1,)), ((), ())),
                preferred_element_type=F32,
            ).astype(BF16)
            out_refs[0][:, start : start + 512] = product[:rows]
            out_refs[1][:, start : start + 512] = product[rows:]


def feed_call(kept, away, weight):
    width = kept[0].shape[1]
    columns = weight.shape[1] // 3
    steps = 4
    depth = width // steps
    rows = sum(a.shape[0] for a in kept)
    outs = jax.ShapeDtypeStruct((rows, width), BF16)
    return pl.pallas_call(
        feed_body,
        grid=(steps,),
        in_specs=[pl.BlockSpec((a.shape[0], depth), lambda k: (0, k)) for a in (*kept, *away)]
        + [pl.BlockSpec((depth, 3 * columns), lambda k: (k, 0))],
        out_specs=[pl.BlockSpec((rows, width), lambda k: (0, 0))] * 2,
        out_shape=[outs, outs],
        scratch_shapes=[
            pltpu.VMEM((2 * rows, 2 * columns), F32),
            pltpu.VMEM((width, columns), BF16),
        ],
        compiler_params=pltpu.CompilerParams(dimension_semantics=("arbitrary",)),
        cost_estimate=pl.CostEstimate(
            flops=12 * rows * width * columns, bytes_accessed=8_000_000, transcendentals=0
        ),
        name="feed",
    )(*kept, *away, weight)


def halves_body(ref, came, left, right):
    half = left.shape[1]
    both = ref[...].astype(F32) + came[...].astype(F32)
    left[...] = both[:, :half].astype(BF16)
    right[...] = both[:, half:].astype(BF16)


def halves_call(*arrays):
    rows, width = arrays[0].shape
    return pl.pallas_call(
        halves_body,
        out_shape=[jax.ShapeDtypeStruct((rows, width // 2), BF16)] * 2,
        name="halves",
    )(*arrays)


def feed_forward(x_norm, after_mixer, weight):
    rows, _ = x_norm.shape
    half = rows // 2

    x1 = x_norm
    x_side = swapped(x1, "tp", 2)
    y_side = swapped(x1, "grp", 1)
    x1_away = swapped(x1, "tp", 1)
    corner_top = swapped(y_side[:half], "tp", 2)
    corner_low = swapped(x_side[half:], "grp", 1)
    x_away = swapped(x_side, "tp", 1)
    y_away = swapped(y_side, "tp", 1)
    top_away = swapped(corner_top, "tp", 1)
    low_away = swapped(corner_low, "tp", 1)

    def feed(kept, away):
        mine, theirs = feed_call(kept, away, weight)
        return mine, swapped(theirs, "tp", 1)

    own, own_came = feed([x1], [x1_away])
    xs, xs_came = feed([x_side], [x_away])
    ys, ys_came = feed([y_side], [y_away])
    corner, corner_came = feed([corner_top, corner_low], [top_away, low_away])
    x_left, x_right = halves_call(xs, xs_came)
    y_left, y_right = halves_call(ys, ys_came)
    l1 = swapped(x_left, "tp", 2)
    r1 = swapped(y_right, "grp", 1)
    c_left, c_right = halves_call(corner, corner_came)
    l2 = swapped(c_left, "tp", 2)
    r2 = swapped(c_right, "grp", 1)
    y_left = (y_left.astype(F32) + l2.astype(F32)).astype(BF16)
    x_right = (x_right.astype(F32) + r2.astype(F32)).astype(BF16)
    l2 = swapped(y_left, "grp", 1)
    r2 = swapped(x_right, "tp", 2)
    return finish_call(after_mixer, own, own_came, l1, l2, r1, r2)


def feed_forward_any(x_norm, after_mixer, weight):
    columns = weight.shape[1] // 3
    x = lax.all_gather(x_norm, ("grp", "tp"), axis=0, tiled=True)
    gates = jnp.dot(x, weight[:, :columns], preferred_element_type=F32)
    ups = jnp.dot(x, weight[:, columns : 2 * columns], preferred_element_type=F32)
    hidden = (silu(gates) * ups).astype(BF16)
    share = lax.dot_general(
        hidden,
        weight[:, 2 * columns :],
        (((1,), (1,)), ((), ())),
        preferred_element_type=F32,
    ).astype(BF16)
    share = lax.psum_scatter(share, ("grp", "tp"), scatter_dimension=0, tiled=True)
    return (after_mixer.astype(F32) + 0.5 * share.astype(F32)).astype(BF16)


def shifted(value, axis, steps):
    count = lax.axis_size(axis)
    return lax.ppermute(value, axis, [(s, s + steps) for s in range(count - steps)])


def swapped(value, axis, bit):
    count = lax.axis_size(axis)
    return lax.ppermute(value, axis, [(s, s ^ bit) for s in range(count)])


def entering_states(packed, axis):
    count = lax.axis_size(axis)
    window, before, got = packed, None, jnp.zeros_like(packed)
    reach = 1
    while reach < count:
        if reach > 1:
            window = join_call(window, got)
            before = got if before is None else join_call(before, got)
        got = shifted(window, axis, reach)
        reach *= 2
    return (got, jnp.zeros_like(got)) if before is None else (before, got)


def on_device(
    residual,
    value_projected,
    gate_projected,
    wide_key_rows,
    wide_query_rows,
    narrow_key_rows,
    narrow_query_rows,
    step_before_softplus,
    extra_log_decay,
    log_decay_rate,
    value_kernel,
    wide_key_kernel,
    wide_query_kernel,
    narrow_key_kernel,
    narrow_query_kernel,
    head_norm_gain,
    output_matrix,
    feedforward_norm_gain,
    gate_matrix,
    up_matrix,
    down_matrix,
):
    members = lax.axis_size("tp")
    place = lax.axis_index("tp")
    part = jnp.reshape(lax.axis_index("grp"), (1,))
    mine = pick_call(part, lax.axis_size("grp"), (gate_matrix, up_matrix, down_matrix))
    raw = (value_projected, wide_key_rows, wide_query_rows, narrow_key_rows, narrow_query_rows)
    tails, mine = lax.optimization_barrier((tails_call(raw), mine))
    rim = shifted(tails, "sp", 1)
    weight = lax.all_gather(mine, "sp", axis=0, tiled=True)

    taps = (
        value_kernel,
        wide_key_kernel,
        wide_query_kernel,
        narrow_key_kernel,
        narrow_query_kernel,
    )
    y, q, fade, packed = local_call(
        raw, step_before_softplus.T, extra_log_decay.T, log_decay_rate[None, :], rim, taps
    )
    near, far = entering_states(packed, "sp")
    rows = y.shape[0] // members
    masks = 2 * jnp.arange(members // 2, dtype=jnp.int32)
    shared = (y, q, fade, gate_projected, head_norm_gain[None, :], near, far, output_matrix, rows)
    away = final_call((place ^ 1) ^ masks, *shared, BF16)
    came = swapped(away, "tp", 1)
    kept = final_call(place ^ masks, *shared, F32)
    bit = members // 2
    total = {m: None for m in range(0, members, 2)}

    def block(array, mask):
        return array[mask // 2 * rows : (mask // 2 + 1) * rows]

    for mask in range(2, members, 2):
        total[mask] = block(kept, mask) + block(came, mask).astype(F32)
    last = None
    while bit > 1:
        for mask in range(0, bit, 2):
            got = swapped(total[mask + bit].astype(BF16), "tp", bit)
            if mask == 0:
                last = got if last is None else last.astype(F32) + got.astype(F32)
            else:
                total[mask] = total[mask] + got.astype(F32)
        bit //= 2
    after_mixer, x_norm = settle_call(residual, kept, came, last, feedforward_norm_gain[None, :])
    if members == 4 and lax.axis_size("grp") == 2:
        return feed_forward(x_norm, after_mixer, weight)
    return feed_forward_any(x_norm, after_mixer, weight)


def solution(mesh):
    in_specs = (
        P(("grp", "sp", "tp"), None),
        P(("grp", "sp"), "tp"),
        P(("grp", "sp"), "tp"),
        P(("grp", "sp"), "tp"),
        P(("grp", "sp"), "tp"),
        P(("grp", "sp"), "tp"),
        P(("grp", "sp"), "tp"),
        P(("grp", "sp"), "tp"),
        P(("grp", "sp"), "tp"),
        P("tp"),
        P(None, "tp"),
        P(None, "tp"),
        P(None, "tp"),
        P(None, "tp"),
        P(None, "tp"),
        P("tp"),
        P("tp", None),
        P(),
        P("sp", "tp"),
        P("sp", "tp"),
        P("sp", "tp"),
    )
    out_specs = P(("grp", "sp", "tp"), None)

    return jax.shard_map(
        on_device, mesh=mesh, in_specs=in_specs, out_specs=out_specs, check_vma=False
    )
```

time: 499 us -> 229 us (0.46)
  the two profiles are of different devices: /device:TPU:0 before, /device:TPU:24 now
where the time goes in v1:
time: 229 us; the launch traced here: 228 us
  waiting for transfers between devices  105 us (46%)
  Pallas kernels  76.1 us (33%)
  starting transfers between devices  20.1 us (9%)
  between operations  13.6 us (6%)
  local copies, waits for them, and re-layouts  8.69 us (4%)
  other arithmetic  4.52 us (2%)
    ppermute x21, waiting for transfers between devices, swapped(): return lax.ppermute(value, axis, [(s, s ^ bit) for s in range(count)])  58.6 us
    ppermute x3, waiting for transfers between devices, shifted(): lax.ppermute(value, axis, [(s, s + steps) for s in range(count - steps)])  46.7 us
    pallas_call x4, Pallas kernels, feed_call(): pl.pallas_call(feed_body, grid=(steps,), in_specs=[pl.BlockSpec((a.shape[...  27.4 us
    ppermute x21, starting transfers between devices, swapped(): return lax.ppermute(value, axis, [(s, s ^ bit) for s in range(count)])  16.1 us
    pallas_call x2, Pallas kernels, final_call(): pl.pallas_call(final_body, grid_spec=pltpu.PrefetchScalarGridSpec(num_sca...  15.4 us
    pallas_call x1, Pallas kernels, local_call(): pl.pallas_call(local_body, grid=(length // chunk,), in_specs=[rows(a) for...  14.3 us
    unnamed x44, local copies, waits for them, and re-layouts  7.44 us
    pallas_call x3, Pallas kernels, halves_call(): pl.pallas_call(halves_body, out_shape=[jax.ShapeDtypeStruct((rows, width...  7.1 us
  transfers between devices with their start and end apart: 25, of which 12 were waited for; matrix products, arithmetic and copies ran while one was open for 3% of the time, Pallas kernels for 30%

profile of v1, /device:TPU:24, one launch (start us, length us, event | category | flops | bytes accessed | tf_op | source)
XLA Modules:
  0.0 228.4 jit_solution(245766161897133520)
XLA Ops:
  6.5 2.3 %pick.1 = bf16[512,1152]{1,0:T(8,128)(2,1)} custom-call(s32[1]{0:T(128)} %bitcast.3.part_ref, bf16[512,768]{1,0:T(8,128)(2,1)} %gate_ref.3, bf16[512,768]{1,0:T(8,128)(2,1)} %up_ref.1, bf16[512,768]{1,0:T(8,128)(2,1)} %down_ref.1), custom_call_target="tpu_custom_call" | custom-call | tf_op jit(solution)/shard_map/pick/pallas_call | solution.py:453
  8.9 1.4 tails.1
  10.3 1.3 collective-permute-start
  11.6 5.0 %collective-permute-done.rim_ref = bf16[16,1792]{1,0:T(8,128)(2,1)S(1)} collective-permute-done((bf16[16,1792]{1,0:T(8,128)(2,1)}, bf16[16,1792]{1,0:T(8,128)(2,1)S(1)}, u32[]{:S(2)}, u32[]{:S(2)}) %collective-permute-start) | collective-permute-done | bytes 57376 | tf_op jit(solution)/shard_map/ppermute | solution.py:594
  16.6 0.6 copy-done.21
  17.2 14.3 %mix_local.1 = (f32[768,1024]{1,0:T(8,128)}, bf16[768,384]{1,0:T(8,128)(2,1)}, f32[768,16]{1,0:T(8,128)}, bf16[400,256]{1,0:T(8,128)(2,1)}) custom-call(bf16[768,1024]{1,0:T(8,128)(2,1)} %value_ref.1, bf16[768,256]{1,0:T(8,128)(2,1)} %kw_ref.1, bf16[768,256]{1,0:T(8,128)(2,1)} %qw_ref.1, bf16[768,128]{1,0:T(8,128)(2,1)} %kn_ref.1, bf16[768,128]{1,0:T(8,128)(2,1)} %qn_ref.1, ...), custom_call_target="tpu_custom_call" | custom-call | flops 12000000000 | bytes 10000000 | tf_op jit(solution)/shard_map/mix_local/pallas_call | solution.py:333
  31.5 1.3 collective-permute-start.1
  32.8 16.8 %collective-permute-done.1.earlier_ref.near_ref = bf16[400,256]{1,0:T(8,128)(2,1)S(1)} collective-permute-done((bf16[400,256]{1,0:T(8,128)(2,1)}, bf16[400,256]{1,0:T(8,128)(2,1)S(1)}, u32[]{:S(2)}, u32[]{:S(2)}) %collective-permute-start.1) | collective-permute-done | bytes 204832 | tf_op jit(solution)/shard_map/ppermute | solution.py:594
  49.6 0.7 copy-done.11
  50.3 1.8 join_states.1
  52.1 1.5 collective-permute-start.2
  53.5 0.6 broadcast_in_dim.10.gain_ref
  54.1 0.6 fusion.1.ids_ref
  54.7 24.9 %collective-permute-done.2.far_ref = bf16[400,256]{1,0:T(8,128)(2,1)S(1)} collective-permute-done((bf16[400,256]{1,0:T(8,128)(2,1)}, bf16[400,256]{1,0:T(8,128)(2,1)S(1)}, u32[]{:S(2)}, u32[]{:S(2)}) %collective-permute-start.2) | collective-permute-done | bytes 204832 | tf_op jit(solution)/shard_map/ppermute | solution.py:594
  79.7 0.7 copy-done.20
  80.3 7.5 %mix_final.3 = bf16[384,2048]{1,0:T(8,128)(2,1)} custom-call(s32[2]{0:T(128)} %fusion.1.ids_ref, f32[768,1024]{1,0:T(8,128)} %get-tuple-element.28.y_ref, bf16[768,384]{1,0:T(8,128)(2,1)} %get-tuple-element.29.q_ref, f32[768,16]{1,0:T(8,128)} %get-tuple-element.30.fade_ref, bf16[768,1024]{1,0:T(8,128)(2,1)} %gate_ref.5, ...), custom_call_target="tpu_custom_call" | custom-call | flops 6000000000 | bytes 10000000 | tf_op jit(solution)/shard_map/mix_final/pallas_call | solution.py:375
  87.8 0.1 collective-permute-start.3
  87.9 0.5 fusion.2.ids_ref
  88.4 7.9 %mix_final.2.kept_ref = f32[384,2048]{1,0:T(8,128)} custom-call(s32[2]{0:T(128)} %fusion.2.ids_ref, f32[768,1024]{1,0:T(8,128)} %get-tuple-element.28.y_ref, bf16[768,384]{1,0:T(8,128)(2,1)} %get-tuple-element.29.q_ref, f32[768,16]{1,0:T(8,128)} %get-tuple-element.30.fade_ref, bf16[768,1024]{1,0:T(8,128)(2,1)} %gate_ref.5, ...), custom_call_target="tpu_custom_call" | custom-call | flops 6000000000 | bytes 10000000 | tf_op jit(solution)/shard_map/mix_final/pallas_call | solution.py:375
  96.4 2.2 fusion
  98.6 1.7 collective-permute-start.4
  100.3 0.6 broadcast_in_dim.11.gain_ref
  100.9 17.7 %collective-permute-done.4.far_ref = bf16[192,2048]{1,0:T(8,128)(2,1)S(1)} collective-permute-done((bf16[192,2048]{1,0:T(8,128)(2,1)S(1)}, bf16[192,2048]{1,0:T(8,128)(2,1)S(1)}, u32[]{:S(2)}, u32[]{:S(2)}) %collective-permute-start.4) | collective-permute-done | bytes 786464 | tf_op jit(solution)/shard_map/ppermute | solution.py:599
  118.6 0.9 copy-done.2
  119.5 3.3 %settle.1 = (bf16[192,2048]{1,0:T(8,128)(2,1)}, bf16[192,2048]{1,0:T(8,128)(2,1)}) custom-call(bf16[192,2048]{1,0:T(8,128)(2,1)} %residual_ref.1, f32[384,2048]{1,0:T(8,128)} %mix_final.2.kept_ref, bf16[384,2048]{1,0:T(8,128)(2,1)} %copy-done, bf16[192,2048]{1,0:T(8,128)(2,1)} %copy-done.2, bf16[1,2048]{1,0:T(2,128)(2,1)} %broadcast_in_dim.11.gain_ref), custom_call_target="tpu_custom_call" | custom-call | tf_op jit(solution)/shard_map/settle/pallas_call | solution.py:412
  122.8 1.6 collective-permute-start.11
  124.4 1.5 collective-permute-start.7
  125.8 16.2 %collective-permute-done.11.refs_0_ = bf16[192,2048]{1,0:T(8,128)(2,1)S(1)} collective-permute-done((bf16[192,2048]{1,0:T(8,128)(2,1)}, bf16[192,2048]{1,0:T(8,128)(2,1)S(1)}, u32[]{:S(2)}, u32[]{:S(2)}) %collective-permute-start.11) | collective-permute-done | bytes 786464 | tf_op jit(solution)/shard_map/ppermute | solution.py:599
  142.1 1.7 collective-permute-start.14
  143.8 1.6 collective-permute-start.15
  145.4 0.5 collective-permute-start.8
  145.9 6.1 %collective-permute-done.14.refs_0_ = bf16[96,2048]{1,0:T(8,128)(2,1)S(1)} collective-permute-done((bf16[96,2048]{1,0:T(8,128)(2,1)S(1)}, bf16[96,2048]{1,0:T(8,128)(2,1)S(1)}, u32[]{:S(2)}, u32[]{:S(2)}) %collective-permute-start.14) | collective-permute-done | bytes 393248 | tf_op jit(solution)/shard_map/ppermute | solution.py:599
  152.0 1.4 collective-permute-done.15.refs_1_
  153.4 0.3 collective-permute-done.16.refs_2_
  153.7 1.5 collective-permute-done.17.refs_3_
  155.3 6.9 %feed.7 = (bf16[192,2048]{1,0:T(8,128)(2,1)}, bf16[192,2048]{1,0:T(8,128)(2,1)}) custom-call(bf16[96,2048]{1,0:T(8,128)(2,1)} %copy-done.17, bf16[96,2048]{1,0:T(8,128)(2,1)} %copy-done.18, bf16[96,2048]{1,0:T(8,128)(2,1)} %copy-done.19, bf16[96,2048]{1,0:T(8,128)(2,1)} %collective-permute-done.17.refs_3_, ...), custom_call_target="tpu_custom_call" | custom-call | flops 1811939328 | bytes 8000000 | tf_op jit(solution)/shard_map/feed/pallas_call | solution.py:504
  162.1 0.2 collective-permute-start.18
  162.3 0.4 collective-permute-start.5
  162.7 0.9 copy-done.16
  163.6 6.9 %feed.6 = (bf16[192,2048]{1,0:T(8,128)(2,1)}, bf16[192,2048]{1,0:T(8,128)(2,1)}) custom-call(bf16[192,2048]{1,0:T(8,128)(2,1)} %copy-done.13, bf16[192,2048]{1,0:T(8,128)(2,1)} %copy-done.16, bf16[2048,1152]{1,0:T(8,128)(2,1)} %all-gather.2.cloned.1.call-done.refs_2_.refs_4_), custom_call_target="tpu_custom_call" | custom-call | flops 1811939328 | bytes 8000000 | tf_op jit(solution)/shard_map/feed/pallas_call | solution.py:504
  170.4 0.1 collective-permute-start.13
  170.6 6.8 %feed.5 = (bf16[192,2048]{1,0:T(8,128)(2,1)}, bf16[192,2048]{1,0:T(8,128)(2,1)}) custom-call(bf16[192,2048]{1,0:T(8,128)(2,1)} %copy-done.12, bf16[192,2048]{1,0:T(8,128)(2,1)} %collective-permute-done.8.refs_1_, bf16[2048,1152]{1,0:T(8,128)(2,1)} %all-gather.2.cloned.1.call-done.refs_2_.refs_4_), custom_call_target="tpu_custom_call" | custom-call | flops 1811939328 | bytes 8000000 | tf_op jit(solution)/shard_map/feed/pallas_call | solution.py:504
  177.4 0.4 collective-permute-start.9
  177.8 0.9 copy-done.5
  178.7 2.4 %halves.5 = (bf16[192,1024]{1,0:T(8,128)(2,1)}, bf16[192,1024]{1,0:T(8,128)(2,1)}) custom-call(bf16[192,2048]{1,0:T(8,128)(2,1)} %get-tuple-element.43.ref, bf16[192,2048]{1,0:T(8,128)(2,1)} %copy-done.5), custom_call_target="tpu_custom_call" | custom-call | tf_op jit(solution)/shard_map/halves/pallas_call | solution.py:532
  181.0 1.5 collective-permute-start.22
  182.5 0.8 collective-permute-start.19
  183.3 6.8 %feed.4 = (bf16[192,2048]{1,0:T(8,128)(2,1)}, bf16[192,2048]{1,0:T(8,128)(2,1)}) custom-call(bf16[192,2048]{1,0:T(8,128)(2,1)} %get-tuple-element.33.refs_0_, bf16[192,2048]{1,0:T(8,128)(2,1)} %collective-permute-done.5.refs_1_, bf16[2048,1152]{1,0:T(8,128)(2,1)} %all-gather.2.cloned.1.call-done.refs_2_.refs_4_), custom_call_target="tpu_custom_call" | custom-call | flops 1811939328 | bytes 8000000 | tf_op jit(solution)/shard_map/feed/pallas_call | solution.py:504
  190.2 1.0 copy-done.4
  191.1 2.4 %halves.4 = (bf16[192,1024]{1,0:T(8,128)(2,1)}, bf16[192,1024]{1,0:T(8,128)(2,1)}) custom-call(bf16[192,2048]{1,0:T(8,128)(2,1)} %get-tuple-element.40.ref, bf16[192,2048]{1,0:T(8,128)(2,1)} %copy-done.4), custom_call_target="tpu_custom_call" | custom-call | tf_op jit(solution)/shard_map/halves/pallas_call | solution.py:532
  193.5 0.9 collective-permute-start.21
  194.4 0.9 copy-done.3
  195.3 2.4 %halves.3 = (bf16[192,1024]{1,0:T(8,128)(2,1)}, bf16[192,1024]{1,0:T(8,128)(2,1)}) custom-call(bf16[192,2048]{1,0:T(8,128)(2,1)} %get-tuple-element.37.ref, bf16[192,2048]{1,0:T(8,128)(2,1)} %copy-done.3), custom_call_target="tpu_custom_call" | custom-call | tf_op jit(solution)/shard_map/halves/pallas_call | solution.py:532
  197.6 0.9 collective-permute-start.10
  198.5 1.1 add_convert_fusion
  199.7 1.2 collective-permute-start.23
  200.9 0.1 add_convert_fusion.1
  201.0 1.2 collective-permute-start.20
  202.2 3.5 %collective-permute-done.21.r1_ref = bf16[192,1024]{1,0:T(8,128)(2,1)S(1)} collective-permute-done((bf16[192,1024]{1,0:T(8,128)(2,1)}, bf16[192,1024]{1,0:T(8,128)(2,1)S(1)}, u32[]{:S(2)}, u32[]{:S(2)}) %collective-permute-start.21) | collective-permute-done | bytes 393248 | tf_op jit(solution)/shard_map/ppermute | solution.py:599
  205.7 4.1 %collective-permute-done.10.l1_ref = bf16[192,1024]{1,0:T(8,128)(2,1)S(1)} collective-permute-done((bf16[192,1024]{1,0:T(8,128)(2,1)}, bf16[192,1024]{1,0:T(8,128)(2,1)S(1)}, u32[]{:S(2)}, u32[]{:S(2)}) %collective-permute-start.10) | collective-permute-done | bytes 393248 | tf_op jit(solution)/shard_map/ppermute | solution.py:599
  209.8 7.7 %collective-permute-done.23.r2_ref = bf16[192,1024]{1,0:T(8,128)(2,1)S(1)} collective-permute-done((bf16[192,1024]{1,0:T(8,128)(2,1)S(1)}, bf16[192,1024]{1,0:T(8,128)(2,1)S(1)}, u32[]{:S(2)}, u32[]{:S(2)}) %collective-permute-start.23) | collective-permute-done | bytes 393248 | tf_op jit(solution)/shard_map/ppermute | solution.py:599
  217.5 0.7 copy-done.8
  218.3 0.2 copy-done.9
  218.4 3.1 %finish.1 = bf16[192,2048]{1,0:T(8,128)(2,1)} custom-call(bf16[192,2048]{1,0:T(8,128)(2,1)} %get-tuple-element.32.after_ref, bf16[192,2048]{1,0:T(8,128)(2,1)} %get-tuple-element.35.kept_ref, bf16[192,2048]{1,0:T(8,128)(2,1)} %copy-done.1, bf16[192,1024]{1,0:T(8,128)(2,1)} %copy-done.7, bf16[192,1024]{1,0:T(8,128)(2,1)} %copy-done.9, ...), custom_call_target="tpu_custom_call" | custom-call | tf_op jit(solution)/shard_map/finish/pallas_call | solution.py:434
  (55 shorter events, 0.2 us)
Async XLA Ops:
  6.5 148.7 %all-gather.2.cloned.1.call-start = ((), (), s32[]{:S(2)}) async-start(), calls=%async_computation | async-start | bytes 5898240 | tf_op jit(solution)/shard_map/all_gather | solution.py:645
  10.3 6.3 %collective-permute-start = (bf16[16,1792]{1,0:T(8,128)(2,1)}, bf16[16,1792]{1,0:T(8,128)(2,1)S(1)}, u32[]{:S(2)}, u32[]{:S(2)}) collective-permute-start(bf16[16,1792]{1,0:T(8,128)(2,1)} %tails.1), channel_id=1, source_target_pairs={{0,4},{4,8},{8,12},{1,5},{5,9},{9,13},{2,6},{6,10},{10,14},{3,7},{... | collective-permute-start | bytes 172040 | tf_op jit(solution)/shard_map/ppermute | solution.py:594
  16.6 0.6 copy-start.21
  17.2 36.3 %copy-start.15 = (bf16[1024]{0:T(1024)(128)(2,1)S(1)}, bf16[1024]{0:T(1024)(128)(2,1)}, u32[]{:S(2)}) copy-start(bf16[1024]{0:T(1024)(128)(2,1)} %param.36) | copy-start | bytes 6148
  31.5 18.1 %collective-permute-start.1 = (bf16[400,256]{1,0:T(8,128)(2,1)}, bf16[400,256]{1,0:T(8,128)(2,1)S(1)}, u32[]{:S(2)}, u32[]{:S(2)}) collective-permute-start(bf16[400,256]{1,0:T(8,128)(2,1)} %get-tuple-element.31.later_ref), channel_id=1, source_target_pairs={{0,4},{4,8},{8,12},{1,5},{5,9},{9,13},{2,6},{6,10},{10,14},{3,7},{... | collective-permute-start | bytes 614408 | tf_op jit(solution)/shard_map/ppermute | solution.py:594
  49.6 0.7 copy-start.11
  52.1 27.6 %collective-permute-start.2 = (bf16[400,256]{1,0:T(8,128)(2,1)}, bf16[400,256]{1,0:T(8,128)(2,1)S(1)}, u32[]{:S(2)}, u32[]{:S(2)}) collective-permute-start(bf16[400,256]{1,0:T(8,128)(2,1)} %join_states.1), channel_id=1, source_target_pairs={{0,8},{4,12},{1,9},{5,13},{2,10},{6,14},{3,11},{7,15},{16,24},{20,... | collective-permute-start | bytes 614408 | tf_op jit(solution)/shard_map/ppermute | solution.py:594
  79.7 0.7 copy-start.20
  87.8 8.6 %collective-permute-start.3 = (bf16[384,2048]{1,0:T(8,128)(2,1)}, bf16[384,2048]{1,0:T(8,128)(2,1)S(1)}, u32[]{:S(2)}, u32[]{:S(2)}) collective-permute-start(bf16[384,2048]{1,0:T(8,128)(2,1)} %mix_final.3), channel_id=1, source_target_pairs={{0,1},{1,0},{2,3},{3,2},{4,5},{5,4},{6,7},{7,6},{8,9},{9,8},{10,11... | collective-permute-start | bytes 4718600 | tf_op jit(solution)/shard_map/ppermute | solution.py:599
  96.4 3.9 %copy-start.14 = (bf16[2048]{0:T(1024)(128)(2,1)S(1)}, bf16[2048]{0:T(1024)(128)(2,1)}, u32[]{:S(2)}) copy-start(bf16[2048]{0:T(1024)(128)(2,1)} %param.38) | copy-start | bytes 12292
  96.4 2.2 copy-start
  98.6 20.0 %collective-permute-start.4 = (bf16[192,2048]{1,0:T(8,128)(2,1)S(1)}, bf16[192,2048]{1,0:T(8,128)(2,1)S(1)}, u32[]{:S(2)}, u32[]{:S(2)}) collective-permute-start(bf16[192,2048]{1,0:T(8,128)(2,1)S(1)} %fusion), channel_id=1, source_target_pairs={{0,2},{1,3},{2,0},{3,1},{4,6},{5,7},{6,4},{7,5},{8,10},{9,11},{10,... | collective-permute-start | bytes 2359304 | tf_op jit(solution)/shard_map/ppermute | solution.py:599
  118.6 0.9 copy-start.2
  122.8 19.3 %collective-permute-start.11 = (bf16[192,2048]{1,0:T(8,128)(2,1)}, bf16[192,2048]{1,0:T(8,128)(2,1)S(1)}, u32[]{:S(2)}, u32[]{:S(2)}) collective-permute-start(bf16[192,2048]{1,0:T(8,128)(2,1)} %get-tuple-element.33.refs_0_), channel_id=1, source_target_pairs={{0,16},{16,0},{1,17},{17,1},{2,18},{18,2},{3,19},{19,3},{4,20},{20... | collective-permute-start | bytes 2359304 | tf_op jit(solution)/shard_map/ppermute | solution.py:599
  124.4 19.4 %collective-permute-start.7 = (bf16[192,2048]{1,0:T(8,128)(2,1)}, bf16[192,2048]{1,0:T(8,128)(2,1)S(1)}, u32[]{:S(2)}, u32[]{:S(2)}) collective-permute-start(bf16[192,2048]{1,0:T(8,128)(2,1)} %get-tuple-element.33.refs_0_), channel_id=1, source_target_pairs={{0,2},{1,3},{2,0},{3,1},{4,6},{5,7},{6,4},{7,5},{8,10},{9,11},{10,... | collective-permute-start | bytes 2359304 | tf_op jit(solution)/shard_map/ppermute | solution.py:599
  142.1 20.1 %copy-start.13 = (bf16[192,2048]{1,0:T(8,128)(2,1)}, bf16[192,2048]{1,0:T(8,128)(2,1)S(1)}, u32[]{:S(2)}) copy-start(bf16[192,2048]{1,0:T(8,128)(2,1)S(1)} %collective-permute-done.11.refs_0_) | copy-start | bytes 2359300
  142.1 9.9 %collective-permute-start.14 = (bf16[96,2048]{1,0:T(8,128)(2,1)S(1)}, bf16[96,2048]{1,0:T(8,128)(2,1)S(1)}, u32[]{:S(2)}, u32[]{:S(2)}) collective-permute-start(bf16[96,2048]{1,0:T(8,128)(2,1)S(1)} %slice.18), channel_id=1, source_target_pairs={{0,2},{1,3},{2,0},{3,1},{4,6},{5,7},{6,4},{7,5},{8,10},{9,11},{10,... | collective-permute-start | bytes 1179656 | tf_op jit(solution)/shard_map/ppermute | solution.py:599
  143.8 18.4 %copy-start.12 = (bf16[192,2048]{1,0:T(8,128)(2,1)}, bf16[192,2048]{1,0:T(8,128)(2,1)S(1)}, u32[]{:S(2)}) copy-start(bf16[192,2048]{1,0:T(8,128)(2,1)S(1)} %collective-permute-done.7.refs_0_) | copy-start | bytes 2359300
  143.8 9.6 %collective-permute-start.15 = (bf16[96,2048]{1,0:T(8,128)(2,1)S(1)}, bf16[96,2048]{1,0:T(8,128)(2,1)S(1)}, u32[]{:S(2)}, u32[]{:S(2)}) collective-permute-start(bf16[96,2048]{1,0:T(8,128)(2,1)S(1)} %slice.19), channel_id=1, source_target_pairs={{0,16},{16,0},{1,17},{17,1},{2,18},{18,2},{3,19},{19,3},{4,20},{20... | collective-permute-start | bytes 1179656 | tf_op jit(solution)/shard_map/ppermute | solution.py:599
  145.4 17.3 %collective-permute-start.12 = (bf16[192,2048]{1,0:T(8,128)(2,1)S(1)}, bf16[192,2048]{1,0:T(8,128)(2,1)S(1)}, u32[]{:S(2)}, u32[]{:S(2)}) collective-permute-start(bf16[192,2048]{1,0:T(8,128)(2,1)S(1)} %collective-permute-done.11.refs_0_), channel_id=1, source_target_pairs={{0,1},{1,0},{2,3},{3,2},{4,5},{5,4},{6,7},{7,6},{8,9},{9,8},{10,11... | collective-permute-start | bytes 2359304 | tf_op jit(solution)/shard_map/ppermute | solution.py:599
  145.4 25.2 %collective-permute-start.8 = (bf16[192,2048]{1,0:T(8,128)(2,1)S(1)}, bf16[192,2048]{1,0:T(8,128)(2,1)}, u32[]{:S(2)}, u32[]{:S(2)}) collective-permute-start(bf16[192,2048]{1,0:T(8,128)(2,1)S(1)} %collective-permute-done.7.refs_0_), channel_id=1, source_target_pairs={{0,1},{1,0},{2,3},{3,2},{4,5},{5,4},{6,7},{7,6},{8,9},{9,8},{10,11... | collective-permute-start | bytes 2359304 | tf_op jit(solution)/shard_map/ppermute | solution.py:599
  152.0 3.3 %copy-start.17 = (bf16[96,2048]{1,0:T(8,128)(2,1)}, bf16[96,2048]{1,0:T(8,128)(2,1)S(1)}, u32[]{:S(2)}) copy-start(bf16[96,2048]{1,0:T(8,128)(2,1)S(1)} %collective-permute-done.14.refs_0_) | copy-start | bytes 1179652
  152.0 1.7 collective-permute-start.16
  153.4 1.9 copy-start.18
  153.4 1.9 collective-permute-start.17
  153.7 1.6 copy-start.19
  162.1 15.7 %collective-permute-start.18 = (bf16[192,2048]{1,0:T(8,128)(2,1)}, bf16[192,2048]{1,0:T(8,128)(2,1)S(1)}, u32[]{:S(2)}, u32[]{:S(2)}) collective-permute-start(bf16[192,2048]{1,0:T(8,128)(2,1)} %get-tuple-element.44), channel_id=1, source_target_pairs={{0,1},{1,0},{2,3},{3,2},{4,5},{5,4},{6,7},{7,6},{8,9},{9,8},{10,11... | collective-permute-start | bytes 2359304 | tf_op jit(solution)/shard_map/ppermute | solution.py:599
  162.3 21.0 %collective-permute-start.5 = (bf16[192,2048]{1,0:T(8,128)(2,1)}, bf16[192,2048]{1,0:T(8,128)(2,1)}, u32[]{:S(2)}, u32[]{:S(2)}) collective-permute-start(bf16[192,2048]{1,0:T(8,128)(2,1)} %get-tuple-element.33.refs_0_), channel_id=1, source_target_pairs={{0,1},{1,0},{2,3},{3,2},{4,5},{5,4},{6,7},{7,6},{8,9},{9,8},{10,11... | collective-permute-start | bytes 2359304 | tf_op jit(solution)/shard_map/ppermute | solution.py:599
  162.7 0.9 copy-start.16
  170.4 19.7 %collective-permute-start.13 = (bf16[192,2048]{1,0:T(8,128)(2,1)}, bf16[192,2048]{1,0:T(8,128)(2,1)S(1)}, u32[]{:S(2)}, u32[]{:S(2)}) collective-permute-start(bf16[192,2048]{1,0:T(8,128)(2,1)} %get-tuple-element.41), channel_id=1, source_target_pairs={{0,1},{1,0},{2,3},{3,2},{4,5},{5,4},{6,7},{7,6},{8,9},{9,8},{10,11... | collective-permute-start | bytes 2359304 | tf_op jit(solution)/shard_map/ppermute | solution.py:599
  177.4 16.9 %collective-permute-start.9 = (bf16[192,2048]{1,0:T(8,128)(2,1)}, bf16[192,2048]{1,0:T(8,128)(2,1)S(1)}, u32[]{:S(2)}, u32[]{:S(2)}) collective-permute-start(bf16[192,2048]{1,0:T(8,128)(2,1)} %get-tuple-element.38), channel_id=1, source_target_pairs={{0,1},{1,0},{2,3},{3,2},{4,5},{5,4},{6,7},{7,6},{8,9},{9,8},{10,11... | collective-permute-start | bytes 2359304 | tf_op jit(solution)/shard_map/ppermute | solution.py:599
  177.8 0.9 copy-start.5
  181.0 17.5 %collective-permute-start.22 = (bf16[192,1024]{1,0:T(8,128)(2,1)}, bf16[192,1024]{1,0:T(8,128)(2,1)S(1)}, u32[]{:S(2)}, u32[]{:S(2)}) collective-permute-start(bf16[192,1024]{1,0:T(8,128)(2,1)} %get-tuple-element.48), channel_id=1, source_target_pairs={{0,16},{16,0},{1,17},{17,1},{2,18},{18,2},{3,19},{19,3},{4,20},{20... | collective-permute-start | bytes 1179656 | tf_op jit(solution)/shard_map/ppermute | solution.py:599
  182.5 18.3 %collective-permute-start.19 = (bf16[192,1024]{1,0:T(8,128)(2,1)}, bf16[192,1024]{1,0:T(8,128)(2,1)S(1)}, u32[]{:S(2)}, u32[]{:S(2)}) collective-permute-start(bf16[192,1024]{1,0:T(8,128)(2,1)} %get-tuple-element.45), channel_id=1, source_target_pairs={{0,2},{1,3},{2,0},{3,1},{4,6},{5,7},{6,4},{7,5},{8,10},{9,11},{10,... | collective-permute-start | bytes 1179656 | tf_op jit(solution)/shard_map/ppermute | solution.py:599
  190.1 12.1 %collective-permute-start.6 = (bf16[192,2048]{1,0:T(8,128)(2,1)}, bf16[192,2048]{1,0:T(8,128)(2,1)S(1)}, u32[]{:S(2)}, u32[]{:S(2)}) collective-permute-start(bf16[192,2048]{1,0:T(8,128)(2,1)} %get-tuple-element.36), channel_id=1, source_target_pairs={{0,1},{1,0},{2,3},{3,2},{4,5},{5,4},{6,7},{7,6},{8,9},{9,8},{10,11... | collective-permute-start | bytes 2359304 | tf_op jit(solution)/shard_map/ppermute | solution.py:599
  190.1 1.0 copy-start.4
  193.5 7.4 %copy-start.10 = (bf16[192,1024]{1,0:T(8,128)(2,1)S(1)}, bf16[192,1024]{1,0:T(8,128)(2,1)}, u32[]{:S(2)}) copy-start(bf16[192,1024]{1,0:T(8,128)(2,1)} %get-tuple-element.42) | copy-start | bytes 1179652
  193.5 12.2 %collective-permute-start.21 = (bf16[192,1024]{1,0:T(8,128)(2,1)}, bf16[192,1024]{1,0:T(8,128)(2,1)S(1)}, u32[]{:S(2)}, u32[]{:S(2)}) collective-permute-start(bf16[192,1024]{1,0:T(8,128)(2,1)} %get-tuple-element.46), channel_id=1, source_target_pairs={{0,16},{16,0},{1,17},{17,1},{2,18},{18,2},{3,19},{19,3},{4,20},{20... | collective-permute-start | bytes 1179656 | tf_op jit(solution)/shard_map/ppermute | solution.py:599
  194.4 0.9 copy-start.3
  197.6 12.2 %collective-permute-start.10 = (bf16[192,1024]{1,0:T(8,128)(2,1)}, bf16[192,1024]{1,0:T(8,128)(2,1)S(1)}, u32[]{:S(2)}, u32[]{:S(2)}) collective-permute-start(bf16[192,1024]{1,0:T(8,128)(2,1)} %get-tuple-element.39), channel_id=1, source_target_pairs={{0,2},{1,3},{2,0},{3,1},{4,6},{5,7},{6,4},{7,5},{8,10},{9,11},{10,... | collective-permute-start | bytes 1179656 | tf_op jit(solution)/shard_map/ppermute | solution.py:599
  199.7 17.8 %collective-permute-start.23 = (bf16[192,1024]{1,0:T(8,128)(2,1)S(1)}, bf16[192,1024]{1,0:T(8,128)(2,1)S(1)}, u32[]{:S(2)}, u32[]{:S(2)}) collective-permute-start(bf16[192,1024]{1,0:T(8,128)(2,1)S(1)} %add_convert_fusion), channel_id=1, source_target_pairs={{0,2},{1,3},{2,0},{3,1},{4,6},{5,7},{6,4},{7,5},{8,10},{9,11},{10,... | collective-permute-start | bytes 1179656 | tf_op jit(solution)/shard_map/ppermute | solution.py:599
  201.0 16.5 %collective-permute-start.20 = (bf16[192,1024]{1,0:T(8,128)(2,1)S(1)}, bf16[192,1024]{1,0:T(8,128)(2,1)S(1)}, u32[]{:S(2)}, u32[]{:S(2)}) collective-permute-start(bf16[192,1024]{1,0:T(8,128)(2,1)S(1)} %add_convert_fusion.1), channel_id=1, source_target_pairs={{0,16},{16,0},{1,17},{17,1},{2,18},{18,2},{3,19},{19,3},{4,20},{20... | collective-permute-start | bytes 1179656 | tf_op jit(solution)/shard_map/ppermute | solution.py:599
  202.2 15.3 %copy-start.1 = (bf16[192,2048]{1,0:T(8,128)(2,1)}, bf16[192,2048]{1,0:T(8,128)(2,1)S(1)}, u32[]{:S(2)}) copy-start(bf16[192,2048]{1,0:T(8,128)(2,1)S(1)} %collective-permute-done.6.came_ref) | copy-start | bytes 2359300
  205.7 11.8 %copy-start.6 = (bf16[192,1024]{1,0:T(8,128)(2,1)}, bf16[192,1024]{1,0:T(8,128)(2,1)S(1)}, u32[]{:S(2)}) copy-start(bf16[192,1024]{1,0:T(8,128)(2,1)S(1)} %collective-permute-done.21.r1_ref) | copy-start | bytes 1179652
  209.8 7.7 %copy-start.7 = (bf16[192,1024]{1,0:T(8,128)(2,1)}, bf16[192,1024]{1,0:T(8,128)(2,1)S(1)}, u32[]{:S(2)}) copy-start(bf16[192,1024]{1,0:T(8,128)(2,1)S(1)} %collective-permute-done.10.l1_ref) | copy-start | bytes 1179652
  217.5 0.7 copy-start.8
  217.5 0.9 copy-start.9
Sparse Core Ops, SparseCore 0:
  10.5 100.5 all-gather.1

commit v2 on v1

--- a/solution.py
+++ b/solution.py
@@ -15,6 +15,7 @@
 CHUNK = 128
 TAIL = 16
 FADE_ROWS = 16
+VMEM_LIMIT = 16 * 1024 * 1024
 F32 = jnp.float32
 BF16 = jnp.bfloat16
 
@@ -47,24 +48,31 @@
 
 
 def tails_body(*refs):
-    out_ref = refs[-1]
+    out_ref, arrived = refs[-2:]
+    copies = []
     offset = 0
-    for ref in refs[:-1]:
-        out_ref[:, offset : offset + ref.shape[1]] = ref[...]
-        offset += ref.shape[1]
+    for k, ref in enumerate(refs[:-2]):
+        rows, columns = ref.shape
+        copies.append(
+            pltpu.make_async_copy(
+                ref.at[rows - TAIL :, :], out_ref.at[:, offset : offset + columns], arrived.at[k]
+            )
+        )
+        offset += columns
+    for copy in copies:
+        copy.start()
+    for copy in copies:
+        copy.wait()
 
 
 def tails_call(raw):
-    length = raw[0].shape[0]
     width = sum(a.shape[1] for a in raw)
     return pl.pallas_call(
         tails_body,
-        grid=(1,),
-        in_specs=[
-            pl.BlockSpec((TAIL, a.shape[1]), lambda i: (length // TAIL - 1, 0)) for a in raw
-        ],
-        out_specs=pl.BlockSpec((TAIL, width), lambda i: (0, 0)),
+        in_specs=[pl.BlockSpec(memory_space=pltpu.HBM)] * len(raw),
+        out_specs=pl.BlockSpec(memory_space=pltpu.VMEM),
         out_shape=jax.ShapeDtypeStruct((TAIL, width), BF16),
+        scratch_shapes=[pltpu.SemaphoreType.DMA((len(raw),))],
         name="tails",
     )(*raw)
 
@@ -247,13 +255,17 @@
 
 def join_call(later, earlier):
     return pl.pallas_call(
-        join_body, out_shape=jax.ShapeDtypeStruct(later.shape, BF16), name="join_states"
+        join_body,
+        out_shape=jax.ShapeDtypeStruct(later.shape, BF16),
+        compiler_params=pltpu.CompilerParams(vmem_limit_bytes=VMEM_LIMIT),
+        name="join_states",
     )(later, earlier)
 
 
 def final_body(
-    ids_ref, y_ref, q_ref, fade_ref, gate_ref, gain_ref, near_ref, far_ref, matrix_ref, out_ref, state, normed, matrix, arrived
+    ids_ref, y_ref, q_ref, fade_ref, gate_ref, gain_ref, near_ref, far_ref, matrix_ref, *rest
 ):
+    out_refs, (state, normed, matrix, arrived) = rest[:-4], rest[-4:]
     rows, columns = y_ref.shape
     heads = fade_ref.shape[1]
     table = head_table(heads, columns)
@@ -306,13 +318,16 @@
     @pl.when(turn == pl.num_programs(0) - 1)
     def _():
         copy.wait()
-        width = out_ref.shape[1]
         step = 512
-        for start in range(0, width, step):
+        for start in range(0, matrix.shape[1], step):
             product = jnp.dot(
                 normed[...], matrix[:, start : start + step], preferred_element_type=F32
             )
-            out_ref[:, start : start + step] = product.astype(out_ref.dtype)
+            at = 0
+            for out_ref in out_refs:
+                size = out_ref.shape[0]
+                out_ref[:, start : start + step] = product[at : at + size].astype(out_ref.dtype)
+                at += size
 
 
 def local_call(raw, step, extra, rate, rim, taps):
@@ -361,7 +376,7 @@
     )(*raw, step, extra, rate, rim, *taps)
 
 
-def final_call(ids, y, q, fade, gate, gain, near, far, matrix, rows_each, kind):
+def final_call(ids, y, q, fade, gate, gain, near, far, matrix, rows_each, outs):
     columns = y.shape[1]
     width = matrix.shape[1]
     count = ids.shape[0]
@@ -380,7 +395,9 @@
             in_specs=[rows(y), rows(q), rows(fade), rows(gate)]
             + [fixed(a) for a in (gain, near, far)]
             + [pl.BlockSpec(memory_space=pl.ANY)],
-            out_specs=pl.BlockSpec((rows_each * count, width), lambda i, ids: (0, 0)),
+            out_specs=[
+                pl.BlockSpec((n * rows_each, width), lambda i, ids: (0, 0)) for n, _ in outs
+            ],
             scratch_shapes=[
                 pltpu.VMEM(near.shape, BF16),
                 pltpu.VMEM((rows_each * count, columns), BF16),
@@ -388,8 +405,8 @@
                 pltpu.SemaphoreType.DMA,
             ],
         ),
-        out_shape=jax.ShapeDtypeStruct((rows_each * count, width), kind),
-        compiler_params=pltpu.CompilerParams(dimension_semantics=("arbitrary",)),
+        out_shape=[jax.ShapeDtypeStruct((n * rows_each, width), kind) for n, kind in outs],
+        compiler_params=pltpu.CompilerParams(vmem_limit_bytes=VMEM_LIMIT),
         cost_estimate=pl.CostEstimate(
             flops=6_000_000_000, bytes_accessed=10_000_000, transcendentals=0
         ),
@@ -415,6 +432,7 @@
         in_specs=[top] * 4 + [pl.BlockSpec(gain.shape, lambda i: (0, 0))],
         out_specs=[top, top],
         out_shape=[jax.ShapeDtypeStruct(residual.shape, BF16)] * 2,
+        compiler_params=pltpu.CompilerParams(vmem_limit_bytes=VMEM_LIMIT),
         name="settle",
     )(residual, kept, near, far, gain)
 
@@ -437,6 +455,7 @@
         in_specs=[pl.BlockSpec((each, a.shape[1]), lambda i: (i, 0)) for a in arrays],
         out_specs=pl.BlockSpec((each, width), lambda i: (i, 0)),
         out_shape=jax.ShapeDtypeStruct((rows, width), BF16),
+        compiler_params=pltpu.CompilerParams(vmem_limit_bytes=VMEM_LIMIT),
         name="finish",
     )(*arrays)
 
@@ -463,82 +482,92 @@
     )(part, *weights)
 
 
-def feed_body(*refs):
-    out_refs = refs[-4:-2]
-    total, downs = refs[-2:]
-    x_refs, weight_ref = refs[:-5], refs[-5]
-    step = pl.program_id(0)
-    depth = weight_ref.shape[0]
-    columns = weight_ref.shape[1] // 3
-
-    @pl.when(step == 0)
-    def _():
-        total[...] = jnp.zeros_like(total)
-
-    downs[pl.ds(pl.multiple_of(step * depth, depth), depth), :] = weight_ref[:, 2 * columns :]
-    x = jnp.concatenate([x_ref[...] for x_ref in x_refs], axis=0)
-    total[...] += jnp.dot(x, weight_ref[:, : 2 * columns], preferred_element_type=F32)
-
-    @pl.when(step == pl.num_programs(0) - 1)
-    def _():
-        rows, width = out_refs[0].shape
-        hidden = (silu(total[:, :columns]) * total[:, columns:]).astype(BF16)
-        for start in range(0, width, 512):
-            product = lax.dot_general(
-                hidden,
-                downs[start : start + 512, :],
-                (((1,), (1,)), ((), ())),
-                preferred_element_type=F32,
-            ).astype(BF16)
-            out_refs[0][:, start : start + 512] = product[:rows]
-            out_refs[1][:, start : start + 512] = product[rows:]
-
-
-def feed_call(kept, away, weight):
+def feed_body(place_ref, *refs, pieces):
+    own_ref, moved = refs[0], refs[1 : 2 * pieces - 1]
+    x_refs = refs[2 * pieces - 1 : -4]
+    out_refs, weights, arrived = refs[-4:-2], refs[-2], refs[-1]
+    place, odd = place_ref[0], place_ref[1]
+    copies = [pltpu.make_async_copy(own_ref, weights.at[0], arrived.at[0])]
+    copies[0].start()
+    for k in range(1, pieces):
+        target = weights.at[k], arrived.at[k]
+        copies.append(pltpu.make_async_copy(own_ref, *target))
+        for ahead in (True, False):
+            steps = k if ahead else pieces - k
+            stream, back = moved[2 * steps - 2 : 2 * steps]
+            side = place + k < pieces if ahead else place + k >= pieces
+
+            @pl.when(side & (odd == int(ahead)))
+            def _(stream=stream, target=target):
+                source = stream if len(stream.shape) == 2 else stream.at[0]
+                pltpu.make_async_copy(source, *target).start()
+
+            @pl.when(side & (odd != int(ahead)))
+            def _(back=back, target=target):
+                pltpu.make_async_copy(back, *target).start()
+
+    depth = weights.shape[1]
+    columns = weights.shape[2] // 3
+    rows = out_refs[0].shape[0]
+
+    def run(k):
+        at = lax.rem(place_ref[0] + k, pieces) if pieces > 1 else 0
+        return pl.ds(pl.multiple_of(at * depth, depth), depth)
+
+    total = None
+    for k, copy in enumerate(copies):
+        copy.wait()
+        x = jnp.concatenate([x_ref[:, run(k)] for x_ref in x_refs], axis=0)
+        term = jnp.dot(x, weights[k, :, : 2 * columns], preferred_element_type=F32)
+        total = term if total is None else total + term
+    hidden = (silu(total[:, :columns]) * total[:, columns:]).astype(BF16)
+    for k in range(pieces):
+        product = lax.dot_general(
+            hidden,
+            weights[k, :, 2 * columns :],
+            (((1,), (1,)), ((), ())),
+            preferred_element_type=F32,
+        ).astype(BF16)
+        out_refs[0][:, run(k)] = product[:rows]
+        out_refs[1][:, run(k)] = product[rows:]
+
+
+def feed_call(place, kept, away, weights):
     width = kept[0].shape[1]
-    columns = weight.shape[1] // 3
-    steps = 4
-    depth = width // steps
+    pieces = (len(weights) + 1) // 2
+    columns = weights[0].shape[1] // 3
     rows = sum(a.shape[0] for a in kept)
     outs = jax.ShapeDtypeStruct((rows, width), BF16)
+    whole = pl.BlockSpec(memory_space=pltpu.VMEM)
     return pl.pallas_call(
-        feed_body,
-        grid=(steps,),
-        in_specs=[pl.BlockSpec((a.shape[0], depth), lambda k: (0, k)) for a in (*kept, *away)]
-        + [pl.BlockSpec((depth, 3 * columns), lambda k: (k, 0))],
-        out_specs=[pl.BlockSpec((rows, width), lambda k: (0, 0))] * 2,
+        functools.partial(feed_body, pieces=pieces),
+        in_specs=[pl.BlockSpec(memory_space=pltpu.SMEM)]
+        + [pl.BlockSpec(memory_space=pltpu.HBM)] * len(weights)
+        + [whole] * (len(kept) + len(away)),
+        out_specs=[whole, whole],
         out_shape=[outs, outs],
         scratch_shapes=[
-            pltpu.VMEM((2 * rows, 2 * columns), F32),
-            pltpu.VMEM((width, columns), BF16),
+            pltpu.VMEM((pieces, *weights[0].shape), BF16),
+            pltpu.SemaphoreType.DMA((pieces,)),
         ],
-        compiler_params=pltpu.CompilerParams(dimension_semantics=("arbitrary",)),
         cost_estimate=pl.CostEstimate(
             flops=12 * rows * width * columns, bytes_accessed=8_000_000, transcendentals=0
         ),
+        compiler_params=pltpu.CompilerParams(vmem_limit_bytes=VMEM_LIMIT),
         name="feed",
-    )(*kept, *away, weight)
-
-
-def halves_body(ref, came, left, right):
-    half = left.shape[1]
-    both = ref[...].astype(F32) + came[...].astype(F32)
-    left[...] = both[:, :half].astype(BF16)
-    right[...] = both[:, half:].astype(BF16)
-
-
-def halves_call(*arrays):
-    rows, width = arrays[0].shape
-    return pl.pallas_call(
-        halves_body,
-        out_shape=[jax.ShapeDtypeStruct((rows, width // 2), BF16)] * 2,
-        name="halves",
-    )(*arrays)
-
-
-def feed_forward(x_norm, after_mixer, weight):
+    )(place, *weights, *kept, *away)
+
+
+def halves(ref, came):
+    both = ref.astype(F32) + came.astype(F32)
+    half = both.shape[1] // 2
+    return both[:, :half].astype(BF16), both[:, half:].astype(BF16)
+
+
+def feed_forward(x_norm, after_mixer, weights):
     rows, _ = x_norm.shape
     half = rows // 2
+    spot = jnp.stack([lax.axis_index("sp"), lax.axis_index("tp") & 1])
 
     x1 = x_norm
     x_side = swapped(x1, "tp", 2)
@@ -552,18 +581,18 @@
     low_away = swapped(corner_low, "tp", 1)
 
     def feed(kept, away):
-        mine, theirs = feed_call(kept, away, weight)
+        mine, theirs = feed_call(spot, kept, away, weights)
         return mine, swapped(theirs, "tp", 1)
 
     own, own_came = feed([x1], [x1_away])
     xs, xs_came = feed([x_side], [x_away])
+    corner, corner_came = feed([corner_top, corner_low], [top_away, low_away])
     ys, ys_came = feed([y_side], [y_away])
-    corner, corner_came = feed([corner_top, corner_low], [top_away, low_away])
-    x_left, x_right = halves_call(xs, xs_came)
-    y_left, y_right = halves_call(ys, ys_came)
+    x_left, x_right = halves(xs, xs_came)
+    y_left, y_right = halves(ys, ys_came)
     l1 = swapped(x_left, "tp", 2)
     r1 = swapped(y_right, "grp", 1)
-    c_left, c_right = halves_call(corner, corner_came)
+    c_left, c_right = halves(corner, corner_came)
     l2 = swapped(c_left, "tp", 2)
     r2 = swapped(c_right, "grp", 1)
     y_left = (y_left.astype(F32) + l2.astype(F32)).astype(BF16)
@@ -573,7 +602,8 @@
     return finish_call(after_mixer, own, own_came, l1, l2, r1, r2)
 
 
-def feed_forward_any(x_norm, after_mixer, weight):
+def feed_forward_any(x_norm, after_mixer, weights):
+    (weight,) = weights
     columns = weight.shape[1] // 3
     x = lax.all_gather(x_norm, ("grp", "tp"), axis=0, tiled=True)
     gates = jnp.dot(x, weight[:, :columns], preferred_element_type=F32)
@@ -592,6 +622,17 @@
 def shifted(value, axis, steps):
     count = lax.axis_size(axis)
     return lax.ppermute(value, axis, [(s, s + steps) for s in range(count - steps)])
+
+
+def either_way(value):
+    count, members = lax.axis_size("sp"), lax.axis_size("tp")
+    pairs = []
+    for s in range(count):
+        for t in range(members):
+            target = s - 1 if t % 2 else s + 1
+            if 0 <= target < count:
+                pairs.append((s * members + t, target * members + t))
+    return lax.ppermute(value, ("sp", "tp"), pairs)
 
 
 def swapped(value, axis, bit):
@@ -640,9 +681,14 @@
     part = jnp.reshape(lax.axis_index("grp"), (1,))
     mine = pick_call(part, lax.axis_size("grp"), (gate_matrix, up_matrix, down_matrix))
     raw = (value_projected, wide_key_rows, wide_query_rows, narrow_key_rows, narrow_query_rows)
-    tails, mine = lax.optimization_barrier((tails_call(raw), mine))
-    rim = shifted(tails, "sp", 1)
-    weight = lax.all_gather(mine, "sp", axis=0, tiled=True)
+    rim = shifted(tails_call(raw), "sp", 1)
+    count = lax.axis_size("sp")
+    direct = members == 4 and lax.axis_size("grp") == 2 and count == 4
+    if direct:
+        mine, rim = lax.optimization_barrier((mine, rim))
+        first = either_way(mine)
+    else:
+        weights = [lax.all_gather(mine, "sp", axis=0, tiled=True)]
 
     taps = (
         value_kernel,
@@ -654,21 +700,40 @@
     y, q, fade, packed = local_call(
         raw, step_before_softplus.T, extra_log_decay.T, log_decay_rate[None, :], rim, taps
     )
+    if direct:
+        mine, packed = lax.optimization_barrier((mine, packed))
     near, far = entering_states(packed, "sp")
+    if direct:
+        pair = jnp.stack([first, swapped(mine, "tp", 1)])
+    if direct:
+        pair, near, far = lax.optimization_barrier((pair, near, far))
+        streams = [first]
+        backs = []
+        for k in range(2, count + 1):
+            pair = either_way(pair if k < count else pair[1])
+            if k < count:
+                streams.append(pair)
+            backs.append(swapped(pair[1] if k < count else pair, "tp", 1))
+        weights = [mine]
+        for stream, back in zip(streams, backs):
+            weights += [stream, back]
+
     rows = y.shape[0] // members
     masks = 2 * jnp.arange(members // 2, dtype=jnp.int32)
     shared = (y, q, fade, gate_projected, head_norm_gain[None, :], near, far, output_matrix, rows)
-    away = final_call((place ^ 1) ^ masks, *shared, BF16)
+    half = members // 2
+    ids = jnp.concatenate([(place ^ 1) ^ masks, place ^ masks[1:]])
+    away, far_kept = final_call(ids, *shared, [(half, BF16), (half - 1, BF16)])
     came = swapped(away, "tp", 1)
-    kept = final_call(place ^ masks, *shared, F32)
+    (kept,) = final_call(place ^ masks[:1], *shared, [(1, F32)])
     bit = members // 2
-    total = {m: None for m in range(0, members, 2)}
-
-    def block(array, mask):
-        return array[mask // 2 * rows : (mask // 2 + 1) * rows]
+    total = {}
+
+    def block(array, index):
+        return array[index * rows : (index + 1) * rows]
 
     for mask in range(2, members, 2):
-        total[mask] = block(kept, mask) + block(came, mask).astype(F32)
+        total[mask] = block(far_kept, mask // 2 - 1).astype(F32) + block(came, mask // 2).astype(F32)
     last = None
     while bit > 1:
         for mask in range(0, bit, 2):
@@ -680,8 +745,8 @@
         bit //= 2
     after_mixer, x_norm = settle_call(residual, kept, came, last, feedforward_norm_gain[None, :])
     if members == 4 and lax.axis_size("grp") == 2:
-        return feed_forward(x_norm, after_mixer, weight)
-    return feed_forward_any(x_norm, after_mixer, weight)
+        return feed_forward(x_norm, after_mixer, weights)
+    return feed_forward_any(x_norm, after_mixer, weights)
 
 
 def solution(mesh):

time: 229 us -> 231 us (level)
  the two profiles are of different devices: /device:TPU:24 before, /device:TPU:0 now
where the time goes in v2:
time: 231 us; the launch traced here: 230 us
  waiting for transfers between devices  100 us (43%)
  starting transfers between devices  50.2 us (22%)
  Pallas kernels  50.1 us (22%)
  local copies, waits for them, and re-layouts  24.6 us (11%)
  other arithmetic  3.26 us (1%)
    ppermute x25, waiting for transfers between devices, swapped(): return lax.ppermute(value, axis, [(s, s ^ bit) for s in range(count)])  49.6 us
    ppermute x4, waiting for transfers between devices, either_way(): return lax.ppermute(value, ('sp', 'tp'), pairs)  32.2 us
    pallas_call x4, Pallas kernels, feed_call(): pl.pallas_call(functools.partial(feed_body, pieces=pieces), in_specs=[pl....  21 us
    unnamed x74, local copies, waits for them, and re-layouts  20.4 us
    ppermute x3, waiting for transfers between devices, shifted(): lax.ppermute(value, axis, [(s, s + steps) for s in range(count - steps)])  18.4 us
    ppermute x4, starting transfers between devices, either_way(): return lax.ppermute(value, ('sp', 'tp'), pairs)  17.6 us
    ppermute x25, starting transfers between devices, swapped(): return lax.ppermute(value, axis, [(s, s ^ bit) for s in range(count)])  16.7 us
    ppermute x3, starting transfers between devices, shifted(): lax.ppermute(value, axis, [(s, s + steps) for s in range(count - steps)])  15.9 us
  transfers between devices with their start and end apart: 32, of which 15 were waited for; matrix products, arithmetic and copies ran while one was open for 3% of the time, Pallas kernels for 14%

profile of v2, /device:TPU:0, one launch (start us, length us, event | category | flops | bytes accessed | tf_op | source)
XLA Modules:
  0.0 230.1 jit_solution(418389922731784155)
XLA Ops:
  0.0 1.4 tails.1
  1.4 5.0 %collective-permute-start = (bf16[16,1792]{1,0:T(8,128)(2,1)}, bf16[16,1792]{1,0:T(8,128)(2,1)S(1)}, u32[]{:S(2)}, u32[]{:S(2)}) collective-permute-start(bf16[16,1792]{1,0:T(8,128)(2,1)} %tails.1), channel_id=1, source_target_pairs={{0,4},{4,8},{8,12},{1,5},{5,9},{9,13},{2,6},{6,10},{10,14},{3,7},{... | collective-permute-start | bytes 172040 | tf_op jit(solution)/shard_map/ppermute | solution.py:624
  6.4 2.4 %pick.1.refs_0_ = bf16[512,1152]{1,0:T(8,128)(2,1)} custom-call(s32[1]{0:T(128)} %bitcast.4.part_ref, bf16[512,768]{1,0:T(8,128)(2,1)} %gate_ref.3, bf16[512,768]{1,0:T(8,128)(2,1)} %up_ref.1, bf16[512,768]{1,0:T(8,128)(2,1)} %down_ref.1), custom_call_target="tpu_custom_call" | custom-call | tf_op jit(solution)/shard_map/pick/pallas_call | solution.py:472
  8.8 0.6 copy-done.36
  9.4 14.3 %mix_local.1 = (f32[768,1024]{1,0:T(8,128)}, bf16[768,384]{1,0:T(8,128)(2,1)}, f32[768,16]{1,0:T(8,128)}, bf16[400,256]{1,0:T(8,128)(2,1)}) custom-call(bf16[768,1024]{1,0:T(8,128)(2,1)} %value_ref.1, bf16[768,256]{1,0:T(8,128)(2,1)} %kw_ref.1, bf16[768,256]{1,0:T(8,128)(2,1)} %qw_ref.1, bf16[768,128]{1,0:T(8,128)(2,1)} %kn_ref.1, bf16[768,128]{1,0:T(8,128)(2,1)} %qn_ref.1, ...), custom_call_target="tpu_custom_call" | custom-call | flops 12000000000 | bytes 10000000 | tf_op jit(solution)/shard_map/mix_local/pallas_call | solution.py:348
  23.8 4.0 %collective-permute-start.1 = (bf16[512,1152]{1,0:T(8,128)(2,1)S(1)}, bf16[512,1152]{1,0:T(8,128)(2,1)S(1)}, u32[]{:S(2)}, u32[]{:S(2)}) collective-permute-start(bf16[512,1152]{1,0:T(8,128)(2,1)S(1)} %copy-done.3), channel_id=1, source_target_pairs={{0,4},{2,6},{4,8},{5,1},{6,10},{7,3},{8,12},{9,5},{10,14},{11,7},{... | collective-permute-start | bytes 3538952 | tf_op jit(solution)/shard_map/ppermute | solution.py:635
  27.8 3.4 %collective-permute-start.3 = (bf16[400,256]{1,0:T(8,128)(2,1)}, bf16[400,256]{1,0:T(8,128)(2,1)S(1)}, u32[]{:S(2)}, u32[]{:S(2)}) collective-permute-start(bf16[400,256]{1,0:T(8,128)(2,1)} %get-tuple-element.35.later_ref), channel_id=1, source_target_pairs={{0,4},{4,8},{8,12},{1,5},{5,9},{9,13},{2,6},{6,10},{10,14},{3,7},{... | collective-permute-start | bytes 614408 | tf_op jit(solution)/shard_map/ppermute | solution.py:624
  31.2 16.9 %collective-permute-done.3.earlier_ref.near_ref = bf16[400,256]{1,0:T(8,128)(2,1)S(1)} collective-permute-done((bf16[400,256]{1,0:T(8,128)(2,1)}, bf16[400,256]{1,0:T(8,128)(2,1)S(1)}, u32[]{:S(2)}, u32[]{:S(2)}) %collective-permute-start.3) | collective-permute-done | bytes 204832 | tf_op jit(solution)/shard_map/ppermute | solution.py:624
  48.1 0.9 copy-done.22
  49.1 7.5 %collective-permute-start.4 = (bf16[400,256]{1,0:T(8,128)(2,1)S(1)}, bf16[400,256]{1,0:T(8,128)(2,1)S(1)}, u32[]{:S(2)}, u32[]{:S(2)}) collective-permute-start(bf16[400,256]{1,0:T(8,128)(2,1)S(1)} %join_states.1), channel_id=1, source_target_pairs={{0,8},{4,12},{1,9},{5,13},{2,10},{6,14},{3,11},{7,15},{16,24},{20,... | collective-permute-start | bytes 614408 | tf_op jit(solution)/shard_map/ppermute | solution.py:624
  56.6 1.8 pad_maximum_fusion
  58.4 1.5 collective-permute-done.4.far_ref
  59.9 0.7 copy-done.27
  60.6 1.5 collective-permute-start.7
  63.4 25.2 %collective-permute-done.7.refs_3_ = bf16[2,512,1152]{2,1,0:T(8,128)(2,1)S(1)} collective-permute-done((bf16[2,512,1152]{2,1,0:T(8,128)(2,1)}, bf16[2,512,1152]{2,1,0:T(8,128)(2,1)S(1)}, u32[]{:S(2)}, u32[]{:S(2)}) %collective-permute-start.7) | collective-permute-done | bytes 2359328 | tf_op jit(solution)/shard_map/ppermute | solution.py:635
  88.6 6.6 %collective-permute-start.9 = (bf16[2,512,1152]{2,1,0:T(8,128)(2,1)S(1)}, bf16[2,512,1152]{2,1,0:T(8,128)(2,1)S(1)}, u32[]{:S(2)}, u32[]{:S(2)}) collective-permute-start(bf16[2,512,1152]{2,1,0:T(8,128)(2,1)S(1)} %collective-permute-done.7.refs_3_), channel_id=1, source_target_pairs={{0,4},{2,6},{4,8},{5,1},{6,10},{7,3},{8,12},{9,5},{10,14},{11,7},{... | collective-permute-start | bytes 7077896 | tf_op jit(solution)/shard_map/ppermute | solution.py:635
  95.2 0.9 copy-done.20
  96.1 2.2 copy-done.23
  98.3 1.4 copy-done.25
  99.7 0.9 copy-done.28
  100.7 1.9 copy-done.29
  102.5 1.1 copy-done.31
  103.6 1.0 copy-done.33
  104.6 6.6 %mix_final.3 = (bf16[384,2048]{1,0:T(8,128)(2,1)S(1)}, bf16[192,2048]{1,0:T(8,128)(2,1)S(1)}) custom-call(s32[3]{0:T(128)S(1)} %pad_add_fusion.ids_ref, f32[768,1024]{1,0:T(8,128)S(1)} %copy-done.29, bf16[768,384]{1,0:T(8,128)(2,1)S(1)} %copy-done.31, f32[768,16]{1,0:T(8,128)S(1)} %copy-done.33, bf16[768,1024]{1,0:T(8,128)(2,1)S(1)} %copy-done.25, ...), custom_call_target="tpu_custom_call" | custom-call | flops 6000000000 | bytes 10000000 | tf_op jit(solution)/shard_map/mix_final/pallas_call | solution.py:390
  111.9 2.8 %collective-permute-done.5.near_ref = bf16[384,2048]{1,0:T(8,128)(2,1)S(1)} collective-permute-done((bf16[384,2048]{1,0:T(8,128)(2,1)S(1)}, bf16[384,2048]{1,0:T(8,128)(2,1)S(1)}, u32[]{:S(2)}, u32[]{:S(2)}) %collective-permute-start.5) | collective-permute-done | bytes 1572896 | tf_op jit(solution)/shard_map/ppermute | solution.py:640
  114.9 1.5 collective-permute-start.6
  116.5 4.9 %collective-permute-done.9.refs_5_ = bf16[2,512,1152]{2,1,0:T(8,128)(2,1)S(1)} collective-permute-done((bf16[2,512,1152]{2,1,0:T(8,128)(2,1)S(1)}, bf16[2,512,1152]{2,1,0:T(8,128)(2,1)S(1)}, u32[]{:S(2)}, u32[]{:S(2)}) %collective-permute-start.9) | collective-permute-done | bytes 2359328 | tf_op jit(solution)/shard_map/ppermute | solution.py:635
  121.4 1.3 slice_bitcast_fusion
  122.7 5.5 %collective-permute-start.11 = (bf16[512,1152]{1,0:T(8,128)(2,1)}, bf16[512,1152]{1,0:T(8,128)(2,1)}, u32[]{:S(2)}, u32[]{:S(2)}) collective-permute-start(bf16[512,1152]{1,0:T(8,128)(2,1)} %slice_bitcast_fusion), channel_id=1, source_target_pairs={{0,4},{2,6},{4,8},{5,1},{6,10},{7,3},{8,12},{9,5},{10,14},{11,7},{... | collective-permute-start | bytes 3538952 | tf_op jit(solution)/shard_map/ppermute | solution.py:635
  128.3 2.3 %mix_final.2.kept_ref = f32[192,2048]{1,0:T(8,128)S(1)} custom-call(s32[1]{0:T(128)S(6)} %xor.20.ids_ref, f32[768,1024]{1,0:T(8,128)S(1)} %copy-done.30, bf16[768,384]{1,0:T(8,128)(2,1)S(1)} %copy-done.32, f32[768,16]{1,0:T(8,128)S(1)} %copy-done.33, bf16[768,1024]{1,0:T(8,128)(2,1)S(1)} %copy-done.26, bf16[1,1024]{1,0:T(2,128)(2,1)S(1)} %broadcast_in_dim.10.gain_ref, ...), custom_call_target="tpu_custom_call" | custom-call | flops 6000000000 | bytes 10000000 | tf_op jit(solution)/shard_map/mix_final/pallas_call | solution.py:390
  130.6 4.0 %collective-permute-done.6.far_ref = bf16[192,2048]{1,0:T(8,128)(2,1)S(1)} collective-permute-done((bf16[192,2048]{1,0:T(8,128)(2,1)S(1)}, bf16[192,2048]{1,0:T(8,128)(2,1)S(1)}, u32[]{:S(2)}, u32[]{:S(2)}) %collective-permute-start.6) | collective-permute-done | bytes 786464 | tf_op jit(solution)/shard_map/ppermute | solution.py:640
  134.6 0.8 settle.1
  135.4 1.5 collective-permute-start.19
  136.9 1.5 collective-permute-start.15
  139.1 2.1 collective-permute-done.11
  141.2 13.0 %collective-permute-done.19.refs_7_ = bf16[192,2048]{1,0:T(8,128)(2,1)} collective-permute-done((bf16[192,2048]{1,0:T(8,128)(2,1)S(1)}, bf16[192,2048]{1,0:T(8,128)(2,1)}, u32[]{:S(2)}, u32[]{:S(2)}) %collective-permute-start.19) | collective-permute-done | bytes 786464 | tf_op jit(solution)/shard_map/ppermute | solution.py:640
  154.3 1.0 slice.64
  155.3 1.5 collective-permute-start.22
  156.9 1.0 slice.65
  157.9 1.6 collective-permute-start.23
  159.5 5.3 %collective-permute-done.22.refs_7_ = bf16[96,2048]{1,0:T(8,128)(2,1)S(1)} collective-permute-done((bf16[96,2048]{1,0:T(8,128)(2,1)S(1)}, bf16[96,2048]{1,0:T(8,128)(2,1)S(1)}, u32[]{:S(2)}, u32[]{:S(2)}) %collective-permute-start.22) | collective-permute-done | bytes 393248 | tf_op jit(solution)/shard_map/ppermute | solution.py:640
  164.9 0.8 copy-done.15
  165.6 1.6 collective-permute-done.23.refs_8_
  167.2 1.0 copy-done.7
  168.8 0.7 copy-done.17
  170.1 1.7 copy-done.1
  171.8 1.3 copy-done.5
  173.1 1.3 copy-done.8
  174.3 1.0 copy-done.16
  175.3 1.0 copy-done.18
  176.3 5.2 %feed.7 = (bf16[192,2048]{1,0:T(8,128)(2,1)S(1)}, bf16[192,2048]{1,0:T(8,128)(2,1)S(1)}) custom-call(s32[2]{0:T(128)S(1)} %pad_add_fusion.1.place_ref, bf16[512,1152]{1,0:T(8,128)(2,1)S(1)} %copy-done.3, bf16[512,1152]{1,0:T(8,128)(2,1)S(1)} %copy-done.5, bf16[512,1152]{1,0:T(8,128)(2,1)S(1)} %copy-done.8, ...), custom_call_target="tpu_custom_call" | custom-call | flops 1811939328 | bytes 8000000 | tf_op jit(solution)/shard_map/feed/pallas_call | solution.py:542
  182.0 5.5 %feed.5 = (bf16[192,2048]{1,0:T(8,128)(2,1)S(1)}, bf16[192,2048]{1,0:T(8,128)(2,1)S(1)}) custom-call(s32[2]{0:T(128)S(1)} %pad_add_fusion.1.place_ref, bf16[512,1152]{1,0:T(8,128)(2,1)S(1)} %copy-done.3, bf16[512,1152]{1,0:T(8,128)(2,1)S(1)} %copy-done.5, bf16[512,1152]{1,0:T(8,128)(2,1)S(1)} %copy-done.8, ...), custom_call_target="tpu_custom_call" | custom-call | flops 1811939328 | bytes 8000000 | tf_op jit(solution)/shard_map/feed/pallas_call | solution.py:542
  187.9 5.7 %feed.6 = (bf16[192,2048]{1,0:T(8,128)(2,1)S(1)}, bf16[192,2048]{1,0:T(8,128)(2,1)S(1)}) custom-call(s32[2]{0:T(128)S(1)} %pad_add_fusion.1.place_ref, bf16[512,1152]{1,0:T(8,128)(2,1)S(1)} %copy-done.3, bf16[512,1152]{1,0:T(8,128)(2,1)S(1)} %copy-done.5, bf16[512,1152]{1,0:T(8,128)(2,1)S(1)} %copy-done.8, ...), custom_call_target="tpu_custom_call" | custom-call | flops 1811939328 | bytes 8000000 | tf_op jit(solution)/shard_map/feed/pallas_call | solution.py:542
  194.0 4.7 %feed.4 = (bf16[192,2048]{1,0:T(8,128)(2,1)S(1)}, bf16[192,2048]{1,0:T(8,128)(2,1)S(1)}) custom-call(s32[2]{0:T(128)S(1)} %pad_add_fusion.1.place_ref, bf16[512,1152]{1,0:T(8,128)(2,1)S(1)} %copy-done.3, bf16[512,1152]{1,0:T(8,128)(2,1)S(1)} %copy-done.6, bf16[512,1152]{1,0:T(8,128)(2,1)S(1)} %copy-done.9, ...), custom_call_target="tpu_custom_call" | custom-call | flops 1811939328 | bytes 8000000 | tf_op jit(solution)/shard_map/feed/pallas_call | solution.py:542
  199.4 1.6 collective-permute-start.30
  202.7 1.5 collective-permute-start.18
  204.3 7.2 %collective-permute-done.30 = bf16[192,1024]{1,0:T(8,128)(2,1)S(1)} collective-permute-done((bf16[192,1024]{1,0:T(8,128)(2,1)S(1)}, bf16[192,1024]{1,0:T(8,128)(2,1)S(1)}, u32[]{:S(2)}, u32[]{:S(2)}) %collective-permute-start.30) | collective-permute-done | bytes 393248 | tf_op jit(solution)/shard_map/ppermute | solution.py:640
  211.6 0.6 collective-permute-start.31
  212.2 0.8 collective-permute-done.27
  213.1 0.8 collective-permute-start.28
  213.9 6.0 %collective-permute-done.29.r1_ref = bf16[192,1024]{1,0:T(8,128)(2,1)S(1)} collective-permute-done((bf16[192,1024]{1,0:T(8,128)(2,1)S(1)}, bf16[192,1024]{1,0:T(8,128)(2,1)S(1)}, u32[]{:S(2)}, u32[]{:S(2)}) %collective-permute-start.29) | collective-permute-done | bytes 393248 | tf_op jit(solution)/shard_map/ppermute | solution.py:640
  219.9 1.5 collective-permute-done.18.l1_ref
  221.4 7.3 %collective-permute-done.31.r2_ref = bf16[192,1024]{1,0:T(8,128)(2,1)S(1)} collective-permute-done((bf16[192,1024]{1,0:T(8,128)(2,1)S(1)}, bf16[192,1024]{1,0:T(8,128)(2,1)S(1)}, u32[]{:S(2)}, u32[]{:S(2)}) %collective-permute-start.31) | collective-permute-done | bytes 393248 | tf_op jit(solution)/shard_map/ppermute | solution.py:640
  228.8 1.3 finish.1
  (107 shorter events, 7.0 us)
Async XLA Ops:
  1.4 7.3 %collective-permute-start = (bf16[16,1792]{1,0:T(8,128)(2,1)}, bf16[16,1792]{1,0:T(8,128)(2,1)S(1)}, u32[]{:S(2)}, u32[]{:S(2)}) collective-permute-start(bf16[16,1792]{1,0:T(8,128)(2,1)} %tails.1), channel_id=1, source_target_pairs={{0,4},{4,8},{8,12},{1,5},{5,9},{9,13},{2,6},{6,10},{10,14},{3,7},{... | collective-permute-start | bytes 172040 | tf_op jit(solution)/shard_map/ppermute | solution.py:624
  9.4 14.3 %copy-start.3 = (bf16[512,1152]{1,0:T(8,128)(2,1)S(1)}, bf16[512,1152]{1,0:T(8,128)(2,1)}, u32[]{:S(2)}) copy-start(bf16[512,1152]{1,0:T(8,128)(2,1)} %pick.1.refs_0_) | copy-start | bytes 3538948
  23.7 32.9 %collective-permute-start.2 = (bf16[512,1152]{1,0:T(8,128)(2,1)S(1)}, bf16[512,1152]{1,0:T(8,128)(2,1)S(1)}, u32[]{:S(2)}, u32[]{:S(2)}) collective-permute-start(bf16[512,1152]{1,0:T(8,128)(2,1)S(1)} %copy-done.3), channel_id=1, source_target_pairs={{0,1},{1,0},{2,3},{3,2},{4,5},{5,4},{6,7},{7,6},{8,9},{9,8},{10,11... | collective-permute-start | bytes 3538952 | tf_op jit(solution)/shard_map/ppermute | solution.py:640
  23.8 32.8 %collective-permute-start.1 = (bf16[512,1152]{1,0:T(8,128)(2,1)S(1)}, bf16[512,1152]{1,0:T(8,128)(2,1)S(1)}, u32[]{:S(2)}, u32[]{:S(2)}) collective-permute-start(bf16[512,1152]{1,0:T(8,128)(2,1)S(1)} %copy-done.3), channel_id=1, source_target_pairs={{0,4},{2,6},{4,8},{5,1},{6,10},{7,3},{8,12},{9,5},{10,14},{11,7},{... | collective-permute-start | bytes 3538952 | tf_op jit(solution)/shard_map/ppermute | solution.py:635
  27.8 20.3 %collective-permute-start.3 = (bf16[400,256]{1,0:T(8,128)(2,1)}, bf16[400,256]{1,0:T(8,128)(2,1)S(1)}, u32[]{:S(2)}, u32[]{:S(2)}) collective-permute-start(bf16[400,256]{1,0:T(8,128)(2,1)} %get-tuple-element.35.later_ref), channel_id=1, source_target_pairs={{0,4},{4,8},{8,12},{1,5},{5,9},{9,13},{2,6},{6,10},{10,14},{3,7},{... | collective-permute-start | bytes 614408 | tf_op jit(solution)/shard_map/ppermute | solution.py:624
  48.1 0.9 copy-start.22
  49.0 7.6 %copy-start.19 = (bf16[400,256]{1,0:T(8,128)(2,1)}, bf16[400,256]{1,0:T(8,128)(2,1)S(1)}, u32[]{:S(2)}) copy-start(bf16[400,256]{1,0:T(8,128)(2,1)S(1)} %collective-permute-done.3.earlier_ref.near_ref) | copy-start | bytes 614404
  49.1 10.8 %collective-permute-start.4 = (bf16[400,256]{1,0:T(8,128)(2,1)S(1)}, bf16[400,256]{1,0:T(8,128)(2,1)S(1)}, u32[]{:S(2)}, u32[]{:S(2)}) collective-permute-start(bf16[400,256]{1,0:T(8,128)(2,1)S(1)} %join_states.1), channel_id=1, source_target_pairs={{0,8},{4,12},{1,9},{5,13},{2,10},{6,14},{3,11},{7,15},{16,24},{20,... | collective-permute-start | bytes 614408 | tf_op jit(solution)/shard_map/ppermute | solution.py:624
  56.6 1.8 copy-start.4
  56.6 5.4 %copy-start.35 = (bf16[1024]{0:T(1024)(128)(2,1)S(1)}, bf16[1024]{0:T(1024)(128)(2,1)}, u32[]{:S(2)}) copy-start(bf16[1024]{0:T(1024)(128)(2,1)} %param.36) | copy-start | bytes 6148
  60.6 28.0 %collective-permute-start.7 = (bf16[2,512,1152]{2,1,0:T(8,128)(2,1)}, bf16[2,512,1152]{2,1,0:T(8,128)(2,1)S(1)}, u32[]{:S(2)}, u32[]{:S(2)}) collective-permute-start(bf16[2,512,1152]{2,1,0:T(8,128)(2,1)} %pad_maximum_fusion), channel_id=1, source_target_pairs={{0,4},{2,6},{4,8},{5,1},{6,10},{7,3},{8,12},{9,5},{10,14},{11,7},{... | collective-permute-start | bytes 7077896 | tf_op jit(solution)/shard_map/ppermute | solution.py:635
  88.6 32.8 %collective-permute-start.9 = (bf16[2,512,1152]{2,1,0:T(8,128)(2,1)S(1)}, bf16[2,512,1152]{2,1,0:T(8,128)(2,1)S(1)}, u32[]{:S(2)}, u32[]{:S(2)}) collective-permute-start(bf16[2,512,1152]{2,1,0:T(8,128)(2,1)S(1)} %collective-permute-done.7.refs_3_), channel_id=1, source_target_pairs={{0,4},{2,6},{4,8},{5,1},{6,10},{7,3},{8,12},{9,5},{10,14},{11,7},{... | collective-permute-start | bytes 7077896 | tf_op jit(solution)/shard_map/ppermute | solution.py:635
  95.2 0.9 copy-start.20
  96.1 2.2 copy-start.23
  98.3 1.4 copy-start.25
  100.6 1.9 copy-start.29
  102.5 1.1 copy-start.31
  103.6 1.0 copy-start.33
  104.6 7.3 %copy-start.34 = (bf16[2048]{0:T(1024)(128)(2,1)S(1)}, bf16[2048]{0:T(1024)(128)(2,1)}, u32[]{:S(2)}) copy-start(bf16[2048]{0:T(1024)(128)(2,1)} %param.38) | copy-start | bytes 12292
  104.6 23.6 %copy-start.26 = (bf16[768,1024]{1,0:T(8,128)(2,1)S(1)}, bf16[768,1024]{1,0:T(8,128)(2,1)}, u32[]{:S(2)}) copy-start(bf16[768,1024]{1,0:T(8,128)(2,1)} %gate_ref.5) | copy-start | bytes 4718596
  104.6 23.6 %copy-start.30 = (f32[768,1024]{1,0:T(8,128)S(1)}, f32[768,1024]{1,0:T(8,128)}, u32[]{:S(2)}) copy-start(f32[768,1024]{1,0:T(8,128)} %get-tuple-element.29.y_ref) | copy-start | bytes 9437188
  104.6 23.6 %copy-start.32 = (bf16[768,384]{1,0:T(8,128)(2,1)S(1)}, bf16[768,384]{1,0:T(8,128)(2,1)}, u32[]{:S(2)}) copy-start(bf16[768,384]{1,0:T(8,128)(2,1)} %get-tuple-element.30.q_ref) | copy-start | bytes 1769476
  111.2 3.5 %collective-permute-start.5 = (bf16[384,2048]{1,0:T(8,128)(2,1)S(1)}, bf16[384,2048]{1,0:T(8,128)(2,1)S(1)}, u32[]{:S(2)}, u32[]{:S(2)}) collective-permute-start(bf16[384,2048]{1,0:T(8,128)(2,1)S(1)} %get-tuple-element.38), channel_id=1, source_target_pairs={{0,1},{1,0},{2,3},{3,2},{4,5},{5,4},{6,7},{7,6},{8,9},{9,8},{10,11... | collective-permute-start | bytes 4718600 | tf_op jit(solution)/shard_map/ppermute | solution.py:640
  114.6 13.6 %copy-start.24 = (bf16[1024,2048]{1,0:T(8,128)(2,1)S(1)}, bf16[1024,2048]{1,0:T(8,128)(2,1)}, u32[]{:S(2)}) copy-start(bf16[1024,2048]{1,0:T(8,128)(2,1)} %matrix_ref.3) | copy-start | bytes 12582916
  114.9 13.3 %copy-start.21 = (bf16[400,256]{1,0:T(8,128)(2,1)S(1)}, bf16[400,256]{1,0:T(8,128)(2,1)}, u32[]{:S(2)}) copy-start(bf16[400,256]{1,0:T(8,128)(2,1)} %copy-done.19) | copy-start | bytes 614404
  114.9 19.6 %collective-permute-start.6 = (bf16[192,2048]{1,0:T(8,128)(2,1)S(1)}, bf16[192,2048]{1,0:T(8,128)(2,1)S(1)}, u32[]{:S(2)}, u32[]{:S(2)}) collective-permute-start(bf16[192,2048]{1,0:T(8,128)(2,1)S(1)} %add_convert_fusion.3), channel_id=1, source_target_pairs={{0,2},{1,3},{2,0},{3,1},{4,6},{5,7},{6,4},{7,5},{8,10},{9,11},{10,... | collective-permute-start | bytes 2359304 | tf_op jit(solution)/shard_map/ppermute | solution.py:640
  121.4 9.2 %copy-start = (bf16[2,512,1152]{2,1,0:T(8,128)(2,1)}, bf16[2,512,1152]{2,1,0:T(8,128)(2,1)S(1)}, u32[]{:S(2)}) copy-start(bf16[2,512,1152]{2,1,0:T(8,128)(2,1)S(1)} %collective-permute-done.9.refs_5_) | copy-start | bytes 7077892
  122.7 11.9 %copy-start.10 = (bf16[192,2048]{1,0:T(8,128)(2,1)S(1)}, bf16[192,2048]{1,0:T(8,128)(2,1)}, u32[]{:S(2)}) copy-start(bf16[192,2048]{1,0:T(8,128)(2,1)} %residual_ref.1) | copy-start | bytes 2359300
  122.7 18.5 %collective-permute-start.11 = (bf16[512,1152]{1,0:T(8,128)(2,1)}, bf16[512,1152]{1,0:T(8,128)(2,1)}, u32[]{:S(2)}, u32[]{:S(2)}) collective-permute-start(bf16[512,1152]{1,0:T(8,128)(2,1)} %slice_bitcast_fusion), channel_id=1, source_target_pairs={{0,4},{2,6},{4,8},{5,1},{6,10},{7,3},{8,12},{9,5},{10,14},{11,7},{... | collective-permute-start | bytes 3538952 | tf_op jit(solution)/shard_map/ppermute | solution.py:635
  135.4 19.9 %copy-start.11 = (bf16[192,2048]{1,0:T(8,128)(2,1)}, bf16[192,2048]{1,0:T(8,128)(2,1)S(1)}, u32[]{:S(2)}) copy-start(bf16[192,2048]{1,0:T(8,128)(2,1)S(1)} %get-tuple-element.40.after_ref) | copy-start | bytes 2359300
  135.4 19.9 %copy-start.13 = (bf16[192,2048]{1,0:T(8,128)(2,1)}, bf16[192,2048]{1,0:T(8,128)(2,1)S(1)}, u32[]{:S(2)}) copy-start(bf16[192,2048]{1,0:T(8,128)(2,1)S(1)} %get-tuple-element.42.refs_7_) | copy-start | bytes 2359300
  135.4 18.9 %collective-permute-start.19 = (bf16[192,2048]{1,0:T(8,128)(2,1)S(1)}, bf16[192,2048]{1,0:T(8,128)(2,1)}, u32[]{:S(2)}, u32[]{:S(2)}) collective-permute-start(bf16[192,2048]{1,0:T(8,128)(2,1)S(1)} %get-tuple-element.42.refs_7_), channel_id=1, source_target_pairs={{0,16},{16,0},{1,17},{17,1},{2,18},{18,2},{3,19},{19,3},{4,20},{20... | collective-permute-start | bytes 2359304 | tf_op jit(solution)/shard_map/ppermute | solution.py:640
  136.9 19.9 %collective-permute-start.15 = (bf16[192,2048]{1,0:T(8,128)(2,1)S(1)}, bf16[192,2048]{1,0:T(8,128)(2,1)}, u32[]{:S(2)}, u32[]{:S(2)}) collective-permute-start(bf16[192,2048]{1,0:T(8,128)(2,1)S(1)} %get-tuple-element.42.refs_7_), channel_id=1, source_target_pairs={{0,2},{1,3},{2,0},{3,1},{4,6},{5,7},{6,4},{7,5},{8,10},{9,11},{10,... | collective-permute-start | bytes 2359304 | tf_op jit(solution)/shard_map/ppermute | solution.py:640
  138.6 28.7 %collective-permute-start.8 = (bf16[512,1152]{1,0:T(8,128)(2,1)S(1)}, bf16[512,1152]{1,0:T(8,128)(2,1)S(1)}, u32[]{:S(2)}, u32[]{:S(2)}) collective-permute-start(bf16[512,1152]{1,0:T(8,128)(2,1)S(1)} %slice_bitcast_fusion.1), channel_id=1, source_target_pairs={{0,1},{1,0},{2,3},{3,2},{4,5},{5,4},{6,7},{7,6},{8,9},{9,8},{10,11... | collective-permute-start | bytes 3538952 | tf_op jit(solution)/shard_map/ppermute | solution.py:640
  138.6 31.5 %collective-permute-start.10 = (bf16[512,1152]{1,0:T(8,128)(2,1)}, bf16[512,1152]{1,0:T(8,128)(2,1)}, u32[]{:S(2)}, u32[]{:S(2)}) collective-permute-start(bf16[512,1152]{1,0:T(8,128)(2,1)} %slice_bitcast_fusion), channel_id=1, source_target_pairs={{0,1},{1,0},{2,3},{3,2},{4,5},{5,4},{6,7},{7,6},{8,9},{9,8},{10,11... | collective-permute-start | bytes 3538952 | tf_op jit(solution)/shard_map/ppermute | solution.py:640
  141.2 28.9 %collective-permute-start.12 = (bf16[512,1152]{1,0:T(8,128)(2,1)}, bf16[512,1152]{1,0:T(8,128)(2,1)}, u32[]{:S(2)}, u32[]{:S(2)}) collective-permute-start(bf16[512,1152]{1,0:T(8,128)(2,1)} %collective-permute-done.11), channel_id=1, source_target_pairs={{0,1},{1,0},{2,3},{3,2},{4,5},{5,4},{6,7},{7,6},{8,9},{9,8},{10,11... | collective-permute-start | bytes 3538952 | tf_op jit(solution)/shard_map/ppermute | solution.py:640
  155.3 9.5 %collective-permute-start.22 = (bf16[96,2048]{1,0:T(8,128)(2,1)S(1)}, bf16[96,2048]{1,0:T(8,128)(2,1)S(1)}, u32[]{:S(2)}, u32[]{:S(2)}) collective-permute-start(bf16[96,2048]{1,0:T(8,128)(2,1)S(1)} %slice.64), channel_id=1, source_target_pairs={{0,2},{1,3},{2,0},{3,1},{4,6},{5,7},{6,4},{7,5},{8,10},{9,11},{10,... | collective-permute-start | bytes 1179656 | tf_op jit(solution)/shard_map/ppermute | solution.py:640
  157.9 9.3 %collective-permute-start.23 = (bf16[96,2048]{1,0:T(8,128)(2,1)S(1)}, bf16[96,2048]{1,0:T(8,128)(2,1)}, u32[]{:S(2)}, u32[]{:S(2)}) collective-permute-start(bf16[96,2048]{1,0:T(8,128)(2,1)S(1)} %slice.65), channel_id=1, source_target_pairs={{0,16},{16,0},{1,17},{17,1},{2,18},{18,2},{3,19},{19,3},{4,20},{20... | collective-permute-start | bytes 1179656 | tf_op jit(solution)/shard_map/ppermute | solution.py:640
  164.9 3.9 %collective-permute-start.24 = (bf16[96,2048]{1,0:T(8,128)(2,1)S(1)}, bf16[96,2048]{1,0:T(8,128)(2,1)S(1)}, u32[]{:S(2)}, u32[]{:S(2)}) collective-permute-start(bf16[96,2048]{1,0:T(8,128)(2,1)S(1)} %collective-permute-done.22.refs_7_), channel_id=1, source_target_pairs={{0,1},{1,0},{2,3},{3,2},{4,5},{5,4},{6,7},{7,6},{8,9},{9,8},{10,11... | collective-permute-start | bytes 1179656 | tf_op jit(solution)/shard_map/ppermute | solution.py:640
  167.2 2.4 %collective-permute-start.25 = (bf16[96,2048]{1,0:T(8,128)(2,1)}, bf16[96,2048]{1,0:T(8,128)(2,1)}, u32[]{:S(2)}, u32[]{:S(2)}) collective-permute-start(bf16[96,2048]{1,0:T(8,128)(2,1)} %collective-permute-done.23.refs_8_), channel_id=1, source_target_pairs={{0,1},{1,0},{2,3},{3,2},{4,5},{5,4},{6,7},{7,6},{8,9},{9,8},{10,11... | collective-permute-start | bytes 1179656 | tf_op jit(solution)/shard_map/ppermute | solution.py:640
  167.2 1.0 copy-start.7
  168.3 13.7 %collective-permute-start.16 = (bf16[192,2048]{1,0:T(8,128)(2,1)}, bf16[192,2048]{1,0:T(8,128)(2,1)}, u32[]{:S(2)}, u32[]{:S(2)}) collective-permute-start(bf16[192,2048]{1,0:T(8,128)(2,1)} %collective-permute-done.15.refs_7_), channel_id=1, source_target_pairs={{0,1},{1,0},{2,3},{3,2},{4,5},{5,4},{6,7},{7,6},{8,9},{9,8},{10,11... | collective-permute-start | bytes 2359304 | tf_op jit(solution)/shard_map/ppermute | solution.py:640
  169.5 18.4 %collective-permute-start.20 = (bf16[192,2048]{1,0:T(8,128)(2,1)}, bf16[192,2048]{1,0:T(8,128)(2,1)}, u32[]{:S(2)}, u32[]{:S(2)}) collective-permute-start(bf16[192,2048]{1,0:T(8,128)(2,1)} %collective-permute-done.19.refs_7_), channel_id=1, source_target_pairs={{0,1},{1,0},{2,3},{3,2},{4,5},{5,4},{6,7},{7,6},{8,9},{9,8},{10,11... | collective-permute-start | bytes 2359304 | tf_op jit(solution)/shard_map/ppermute | solution.py:640
  169.6 24.4 %collective-permute-start.13 = (bf16[192,2048]{1,0:T(8,128)(2,1)}, bf16[192,2048]{1,0:T(8,128)(2,1)S(1)}, u32[]{:S(2)}, u32[]{:S(2)}) collective-permute-start(bf16[192,2048]{1,0:T(8,128)(2,1)} %copy-done.13), channel_id=1, source_target_pairs={{0,1},{1,0},{2,3},{3,2},{4,5},{5,4},{6,7},{7,6},{8,9},{9,8},{10,11... | collective-permute-start | bytes 2359304 | tf_op jit(solution)/shard_map/ppermute | solution.py:640
  170.1 1.7 copy-start.1
  171.8 1.3 copy-start.5
  173.1 1.3 copy-start.8
  174.3 1.0 copy-start.16
  175.3 1.0 copy-start.18
  181.5 17.5 %collective-permute-start.26 = (bf16[192,2048]{1,0:T(8,128)(2,1)S(1)}, bf16[192,2048]{1,0:T(8,128)(2,1)S(1)}, u32[]{:S(2)}, u32[]{:S(2)}) collective-permute-start(bf16[192,2048]{1,0:T(8,128)(2,1)S(1)} %get-tuple-element.50), channel_id=1, source_target_pairs={{0,1},{1,0},{2,3},{3,2},{4,5},{5,4},{6,7},{7,6},{8,9},{9,8},{10,11... | collective-permute-start | bytes 2359304 | tf_op jit(solution)/shard_map/ppermute | solution.py:640
  187.5 6.5 %copy-start.6 = (bf16[512,1152]{1,0:T(8,128)(2,1)S(1)}, bf16[512,1152]{1,0:T(8,128)(2,1)}, u32[]{:S(2)}) copy-start(bf16[512,1152]{1,0:T(8,128)(2,1)} %copy-done.4) | copy-start | bytes 3538948
  187.5 6.5 %copy-start.9 = (bf16[512,1152]{1,0:T(8,128)(2,1)S(1)}, bf16[512,1152]{1,0:T(8,128)(2,1)}, u32[]{:S(2)}) copy-start(bf16[512,1152]{1,0:T(8,128)(2,1)} %copy-done.7) | copy-start | bytes 3538948
  187.5 6.5 %copy-start.14 = (bf16[192,2048]{1,0:T(8,128)(2,1)S(1)}, bf16[192,2048]{1,0:T(8,128)(2,1)}, u32[]{:S(2)}) copy-start(bf16[192,2048]{1,0:T(8,128)(2,1)} %copy-done.13) | copy-start | bytes 2359300
  187.5 14.9 %collective-permute-start.17 = (bf16[192,2048]{1,0:T(8,128)(2,1)S(1)}, bf16[192,2048]{1,0:T(8,128)(2,1)S(1)}, u32[]{:S(2)}, u32[]{:S(2)}) collective-permute-start(bf16[192,2048]{1,0:T(8,128)(2,1)S(1)} %get-tuple-element.46), channel_id=1, source_target_pairs={{0,1},{1,0},{2,3},{3,2},{4,5},{5,4},{6,7},{7,6},{8,9},{9,8},{10,11... | collective-permute-start | bytes 2359304 | tf_op jit(solution)/shard_map/ppermute | solution.py:640
  187.9 6.1 %copy-start.2 = (bf16[2,512,1152]{2,1,0:T(8,128)(2,1)S(1)}, bf16[2,512,1152]{2,1,0:T(8,128)(2,1)}, u32[]{:S(2)}) copy-start(bf16[2,512,1152]{2,1,0:T(8,128)(2,1)} %copy-done) | copy-start | bytes 7077892
  193.6 7.9 %collective-permute-start.21 = (bf16[192,2048]{1,0:T(8,128)(2,1)S(1)}, bf16[192,2048]{1,0:T(8,128)(2,1)S(1)}, u32[]{:S(2)}, u32[]{:S(2)}) collective-permute-start(bf16[192,2048]{1,0:T(8,128)(2,1)S(1)} %get-tuple-element.48), channel_id=1, source_target_pairs={{0,1},{1,0},{2,3},{3,2},{4,5},{5,4},{6,7},{7,6},{8,9},{9,8},{10,11... | collective-permute-start | bytes 2359304 | tf_op jit(solution)/shard_map/ppermute | solution.py:640
  198.6 15.3 %collective-permute-start.14 = (bf16[192,2048]{1,0:T(8,128)(2,1)S(1)}, bf16[192,2048]{1,0:T(8,128)(2,1)S(1)}, u32[]{:S(2)}, u32[]{:S(2)}) collective-permute-start(bf16[192,2048]{1,0:T(8,128)(2,1)S(1)} %get-tuple-element.44), channel_id=1, source_target_pairs={{0,1},{1,0},{2,3},{3,2},{4,5},{5,4},{6,7},{7,6},{8,9},{9,8},{10,11... | collective-permute-start | bytes 2359304 | tf_op jit(solution)/shard_map/ppermute | solution.py:640
  199.4 12.1 %collective-permute-start.30 = (bf16[192,1024]{1,0:T(8,128)(2,1)S(1)}, bf16[192,1024]{1,0:T(8,128)(2,1)S(1)}, u32[]{:S(2)}, u32[]{:S(2)}) collective-permute-start(bf16[192,1024]{1,0:T(8,128)(2,1)S(1)} %get-tuple-element.51), channel_id=1, source_target_pairs={{0,16},{16,0},{1,17},{17,1},{2,18},{18,2},{3,19},{19,3},{4,20},{20... | collective-permute-start | bytes 1179656 | tf_op jit(solution)/shard_map/ppermute | solution.py:640
  201.0 12.0 %collective-permute-start.27 = (bf16[192,1024]{1,0:T(8,128)(2,1)S(1)}, bf16[192,1024]{1,0:T(8,128)(2,1)S(1)}, u32[]{:S(2)}, u32[]{:S(2)}) collective-permute-start(bf16[192,1024]{1,0:T(8,128)(2,1)S(1)} %get-tuple-element.52), channel_id=1, source_target_pairs={{0,2},{1,3},{2,0},{3,1},{4,6},{5,7},{6,4},{7,5},{8,10},{9,11},{10,... | collective-permute-start | bytes 1179656 | tf_op jit(solution)/shard_map/ppermute | solution.py:640
  201.8 18.1 %collective-permute-start.29 = (bf16[192,1024]{1,0:T(8,128)(2,1)S(1)}, bf16[192,1024]{1,0:T(8,128)(2,1)S(1)}, u32[]{:S(2)}, u32[]{:S(2)}) collective-permute-start(bf16[192,1024]{1,0:T(8,128)(2,1)S(1)} %slice.67), channel_id=1, source_target_pairs={{0,16},{16,0},{1,17},{17,1},{2,18},{18,2},{3,19},{19,3},{4,20},{20... | collective-permute-start | bytes 1179656 | tf_op jit(solution)/shard_map/ppermute | solution.py:640
  202.7 26.1 %copy-start.12 = (bf16[192,2048]{1,0:T(8,128)(2,1)S(1)}, bf16[192,2048]{1,0:T(8,128)(2,1)}, u32[]{:S(2)}) copy-start(bf16[192,2048]{1,0:T(8,128)(2,1)} %copy-done.11) | copy-start | bytes 2359300
  202.7 18.7 %collective-permute-start.18 = (bf16[192,1024]{1,0:T(8,128)(2,1)S(1)}, bf16[192,1024]{1,0:T(8,128)(2,1)S(1)}, u32[]{:S(2)}, u32[]{:S(2)}) collective-permute-start(bf16[192,1024]{1,0:T(8,128)(2,1)S(1)} %slice.62), channel_id=1, source_target_pairs={{0,2},{1,3},{2,0},{3,1},{4,6},{5,7},{6,4},{7,5},{8,10},{9,11},{10,... | collective-permute-start | bytes 1179656 | tf_op jit(solution)/shard_map/ppermute | solution.py:640
  211.6 17.2 %collective-permute-start.31 = (bf16[192,1024]{1,0:T(8,128)(2,1)S(1)}, bf16[192,1024]{1,0:T(8,128)(2,1)S(1)}, u32[]{:S(2)}, u32[]{:S(2)}) collective-permute-start(bf16[192,1024]{1,0:T(8,128)(2,1)S(1)} %add_convert_fusion.4), channel_id=1, source_target_pairs={{0,2},{1,3},{2,0},{3,1},{4,6},{5,7},{6,4},{7,5},{8,10},{9,11},{10,... | collective-permute-start | bytes 1179656 | tf_op jit(solution)/shard_map/ppermute | solution.py:640
  213.1 15.6 %collective-permute-start.28 = (bf16[192,1024]{1,0:T(8,128)(2,1)S(1)}, bf16[192,1024]{1,0:T(8,128)(2,1)S(1)}, u32[]{:S(2)}, u32[]{:S(2)}) collective-permute-start(bf16[192,1024]{1,0:T(8,128)(2,1)S(1)} %add_convert_fusion.5), channel_id=1, source_target_pairs={{0,16},{16,0},{1,17},{17,1},{2,18},{18,2},{3,19},{19,3},{4,20},{20... | collective-permute-start | bytes 1179656 | tf_op jit(solution)/shard_map/ppermute | solution.py:640
  (5 other events, 3.8 us)

commit v3 on v2

--- a/solution.py
+++ b/solution.py
@@ -202,7 +202,7 @@
             jnp.concatenate([scaled, entering], axis=0),
             preferred_element_type=F32,
         )
-        y_ref[:, lanes] = mixed * from_middle[:, lanes]
+        y_ref[:, lanes] = (mixed * from_middle[:, lanes]).astype(BF16)
         gained = lax.dot_general(
             keys, scaled, (((0,), (0,)), ((), ())), preferred_element_type=F32
         )
@@ -295,7 +295,7 @@
                 narrow_mask(place % 2, rows, STATE_WIDE), queries, jnp.zeros_like(queries)
             )
         outer = jnp.dot(queries, state[at : at + STATE_WIDE, :], preferred_element_type=F32)
-        mixed = y_ref[:, lanes] + outer * fade[:, lanes]
+        mixed = y_ref[:, lanes].astype(F32) + outer * fade[:, lanes]
         gated = mixed * silu(gate_ref[:, lanes].astype(F32))
         parts.append(gated)
         square = (gated * gated).astype(BF16)
@@ -358,7 +358,7 @@
             fixed((states + FADE_ROWS, GROUP_COLS)),
         ],
         out_shape=[
-            jax.ShapeDtypeStruct((length, columns), F32),
+            jax.ShapeDtypeStruct((length, columns), BF16),
             jax.ShapeDtypeStruct((length, states), BF16),
             jax.ShapeDtypeStruct((length, heads), F32),
             jax.ShapeDtypeStruct((states + FADE_ROWS, GROUP_COLS), BF16),
@@ -553,7 +553,7 @@
         cost_estimate=pl.CostEstimate(
             flops=12 * rows * width * columns, bytes_accessed=8_000_000, transcendentals=0
         ),
-        compiler_params=pltpu.CompilerParams(vmem_limit_bytes=VMEM_LIMIT),
+        compiler_params=pltpu.CompilerParams(vmem_limit_bytes=3 * VMEM_LIMIT),
         name="feed",
     )(place, *weights, *kept, *away)
 

time: 231 us -> 221 us (0.957)
  local copies, waits for them, and re-layouts: 24.6 us -> 14.3 us
    unnamed x74 -> x42, local copies, waits for them, and re-layouts: 20.4 us -> 9.94 us
    ppermute x25, waiting for transfers between devices: 49.6 us -> 43.1 us  [swapped(): return lax.ppermute(value, axis, [(s, s ^ bit) for s in range(count)])]
    ppermute x4, waiting for transfers between devices: 32.2 us -> 36.8 us  [either_way(): return lax.ppermute(value, ('sp', 'tp'), pairs)]
  transfers between devices with their start and end apart: 32 -> 32, of which waited for: 15 -> 15; matrix products, arithmetic and copies ran while one was open for 3% -> 3% of each run, Pallas kernels for 14% -> 16%
where the time goes in v3:
time: 221 us; the launch traced here: 220 us
  waiting for transfers between devices  98.2 us (44%)
  Pallas kernels  52.1 us (24%)
  starting transfers between devices  50.7 us (23%)
  local copies, waits for them, and re-layouts  14.3 us (6%)
  other arithmetic  3.19 us (1%)
    ppermute x25, waiting for transfers between devices, swapped(): return lax.ppermute(value, axis, [(s, s ^ bit) for s in range(count)])  43.1 us
    ppermute x4, waiting for transfers between devices, either_way(): return lax.ppermute(value, ('sp', 'tp'), pairs)  36.8 us
    pallas_call x4, Pallas kernels, feed_call(): pl.pallas_call(functools.partial(feed_body, pieces=pieces), in_specs=[pl....  23 us
    ppermute x4, starting transfers between devices, either_way(): return lax.ppermute(value, ('sp', 'tp'), pairs)  18.8 us
    ppermute x3, waiting for transfers between devices, shifted(): lax.ppermute(value, axis, [(s, s + steps) for s in range(count - steps)])  18.4 us
    ppermute x25, starting transfers between devices, swapped(): return lax.ppermute(value, axis, [(s, s ^ bit) for s in range(count)])  16.1 us
    ppermute x3, starting transfers between devices, shifted(): lax.ppermute(value, axis, [(s, s + steps) for s in range(count - steps)])  15.9 us
    pallas_call x1, Pallas kernels, local_call(): pl.pallas_call(local_body, grid=(length // chunk,), in_specs=[rows(a) for...  14.2 us
  transfers between devices with their start and end apart: 32, of which 15 were waited for; matrix products, arithmetic and copies ran while one was open for 3% of the time, Pallas kernels for 16%

profile of v3, /device:TPU:0, one launch (start us, length us, event | category | flops | bytes accessed | tf_op | source)
XLA Modules:
  0.0 220.3 jit_solution(5240983830163388528)
XLA Ops:
  0.0 1.4 tails.1
  1.4 5.0 %collective-permute-start = (bf16[16,1792]{1,0:T(8,128)(2,1)}, bf16[16,1792]{1,0:T(8,128)(2,1)S(1)}, u32[]{:S(2)}, u32[]{:S(2)}) collective-permute-start(bf16[16,1792]{1,0:T(8,128)(2,1)} %tails.1), channel_id=1, source_target_pairs={{0,4},{4,8},{8,12},{1,5},{5,9},{9,13},{2,6},{6,10},{10,14},{3,7},{... | collective-permute-start | bytes 172040 | tf_op jit(solution)/shard_map/ppermute | solution.py:624
  6.4 2.4 %pick.1.refs_0_ = bf16[512,1152]{1,0:T(8,128)(2,1)} custom-call(s32[1]{0:T(128)} %bitcast.4.part_ref, bf16[512,768]{1,0:T(8,128)(2,1)} %gate_ref.3, bf16[512,768]{1,0:T(8,128)(2,1)} %up_ref.1, bf16[512,768]{1,0:T(8,128)(2,1)} %down_ref.1), custom_call_target="tpu_custom_call" | custom-call | tf_op jit(solution)/shard_map/pick/pallas_call | solution.py:472
  8.8 0.6 copy-done.20
  9.4 14.2 %mix_local.1 = (bf16[768,1024]{1,0:T(8,128)(2,1)}, bf16[768,384]{1,0:T(8,128)(2,1)}, f32[768,16]{1,0:T(8,128)}, bf16[400,256]{1,0:T(8,128)(2,1)}) custom-call(bf16[768,1024]{1,0:T(8,128)(2,1)} %value_ref.1, bf16[768,256]{1,0:T(8,128)(2,1)} %kw_ref.1, bf16[768,256]{1,0:T(8,128)(2,1)} %qw_ref.1, bf16[768,128]{1,0:T(8,128)(2,1)} %kn_ref.1, ...), custom_call_target="tpu_custom_call" | custom-call | flops 12000000000 | bytes 10000000 | tf_op jit(solution)/shard_map/mix_local/pallas_call | solution.py:348
  23.7 3.9 %collective-permute-start.1 = (bf16[512,1152]{1,0:T(8,128)(2,1)S(1)}, bf16[512,1152]{1,0:T(8,128)(2,1)S(1)}, u32[]{:S(2)}, u32[]{:S(2)}) collective-permute-start(bf16[512,1152]{1,0:T(8,128)(2,1)S(1)} %copy-done), channel_id=1, source_target_pairs={{0,4},{2,6},{4,8},{5,1},{6,10},{7,3},{8,12},{9,5},{10,14},{11,7},{... | collective-permute-start | bytes 3538952 | tf_op jit(solution)/shard_map/ppermute | solution.py:635
  27.7 3.4 %collective-permute-start.3 = (bf16[400,256]{1,0:T(8,128)(2,1)}, bf16[400,256]{1,0:T(8,128)(2,1)S(1)}, u32[]{:S(2)}, u32[]{:S(2)}) collective-permute-start(bf16[400,256]{1,0:T(8,128)(2,1)} %get-tuple-element.35.later_ref), channel_id=1, source_target_pairs={{0,4},{4,8},{8,12},{1,5},{5,9},{9,13},{2,6},{6,10},{10,14},{3,7},{... | collective-permute-start | bytes 614408 | tf_op jit(solution)/shard_map/ppermute | solution.py:624
  31.1 16.9 %collective-permute-done.3.earlier_ref.near_ref = bf16[400,256]{1,0:T(8,128)(2,1)S(1)} collective-permute-done((bf16[400,256]{1,0:T(8,128)(2,1)}, bf16[400,256]{1,0:T(8,128)(2,1)S(1)}, u32[]{:S(2)}, u32[]{:S(2)}) %collective-permute-start.3) | collective-permute-done | bytes 204832 | tf_op jit(solution)/shard_map/ppermute | solution.py:624
  48.0 0.9 copy-done.8
  49.0 7.5 %collective-permute-start.4 = (bf16[400,256]{1,0:T(8,128)(2,1)S(1)}, bf16[400,256]{1,0:T(8,128)(2,1)S(1)}, u32[]{:S(2)}, u32[]{:S(2)}) collective-permute-start(bf16[400,256]{1,0:T(8,128)(2,1)S(1)} %join_states.1), channel_id=1, source_target_pairs={{0,8},{4,12},{1,9},{5,13},{2,10},{6,14},{3,11},{7,15},{16,24},{20,... | collective-permute-start | bytes 614408 | tf_op jit(solution)/shard_map/ppermute | solution.py:624
  56.6 1.7 pad_maximum_fusion
  58.3 1.5 collective-permute-done.4.far_ref
  59.8 2.7 %collective-permute-start.7 = (bf16[2,512,1152]{2,1,0:T(8,128)(2,1)}, bf16[2,512,1152]{2,1,0:T(8,128)(2,1)}, u32[]{:S(2)}, u32[]{:S(2)}) collective-permute-start(bf16[2,512,1152]{2,1,0:T(8,128)(2,1)} %pad_maximum_fusion), channel_id=1, source_target_pairs={{0,4},{2,6},{4,8},{5,1},{6,10},{7,3},{8,12},{9,5},{10,14},{11,7},{... | collective-permute-start | bytes 7077896 | tf_op jit(solution)/shard_map/ppermute | solution.py:635
  62.5 0.7 fusion.1
  63.9 23.8 %collective-permute-done.7.refs_3_ = bf16[2,512,1152]{2,1,0:T(8,128)(2,1)} collective-permute-done((bf16[2,512,1152]{2,1,0:T(8,128)(2,1)}, bf16[2,512,1152]{2,1,0:T(8,128)(2,1)}, u32[]{:S(2)}, u32[]{:S(2)}) %collective-permute-start.7) | collective-permute-done | bytes 2359328 | tf_op jit(solution)/shard_map/ppermute | solution.py:635
  87.7 6.7 %collective-permute-start.9 = (bf16[2,512,1152]{2,1,0:T(8,128)(2,1)}, bf16[2,512,1152]{2,1,0:T(8,128)(2,1)S(1)}, u32[]{:S(2)}, u32[]{:S(2)}) collective-permute-start(bf16[2,512,1152]{2,1,0:T(8,128)(2,1)} %collective-permute-done.7.refs_3_), channel_id=1, source_target_pairs={{0,4},{2,6},{4,8},{5,1},{6,10},{7,3},{8,12},{9,5},{10,14},{11,7},{... | collective-permute-start | bytes 7077896 | tf_op jit(solution)/shard_map/ppermute | solution.py:635
  94.4 2.2 copy-done.9
  96.6 1.4 copy-done.11
  98.0 1.4 copy-done.12
  99.4 1.0 copy-done.15
  100.4 6.6 %mix_final.3 = (bf16[384,2048]{1,0:T(8,128)(2,1)S(1)}, bf16[192,2048]{1,0:T(8,128)(2,1)S(1)}) custom-call(s32[3]{0:T(128)S(1)} %pad_add_fusion.ids_ref, bf16[768,1024]{1,0:T(8,128)(2,1)S(1)} %copy-done.12, bf16[768,384]{1,0:T(8,128)(2,1)S(1)} %copy-done.14, f32[768,16]{1,0:T(8,128)S(1)} %copy-done.15, bf16[768,1024]{1,0:T(8,128)(2,1)S(1)} %copy-done.11, ...), custom_call_target="tpu_custom_call" | custom-call | flops 6000000000 | bytes 10000000 | tf_op jit(solution)/shard_map/mix_final/pallas_call | solution.py:390
  107.7 2.8 %collective-permute-done.5.near_ref = bf16[384,2048]{1,0:T(8,128)(2,1)S(1)} collective-permute-done((bf16[384,2048]{1,0:T(8,128)(2,1)S(1)}, bf16[384,2048]{1,0:T(8,128)(2,1)S(1)}, u32[]{:S(2)}, u32[]{:S(2)}) %collective-permute-start.5) | collective-permute-done | bytes 1572896 | tf_op jit(solution)/shard_map/ppermute | solution.py:640
  110.5 0.3 add_convert_fusion.3
  110.8 1.6 collective-permute-start.6
  112.3 8.6 %collective-permute-done.9.refs_5_ = bf16[2,512,1152]{2,1,0:T(8,128)(2,1)S(1)} collective-permute-done((bf16[2,512,1152]{2,1,0:T(8,128)(2,1)}, bf16[2,512,1152]{2,1,0:T(8,128)(2,1)S(1)}, u32[]{:S(2)}, u32[]{:S(2)}) %collective-permute-start.9) | collective-permute-done | bytes 2359328 | tf_op jit(solution)/shard_map/ppermute | solution.py:635
  120.9 1.2 slice_bitcast_fusion
  122.1 5.5 %collective-permute-start.11 = (bf16[512,1152]{1,0:T(8,128)(2,1)}, bf16[512,1152]{1,0:T(8,128)(2,1)}, u32[]{:S(2)}, u32[]{:S(2)}) collective-permute-start(bf16[512,1152]{1,0:T(8,128)(2,1)} %slice_bitcast_fusion), channel_id=1, source_target_pairs={{0,4},{2,6},{4,8},{5,1},{6,10},{7,3},{8,12},{9,5},{10,14},{11,7},{... | collective-permute-start | bytes 3538952 | tf_op jit(solution)/shard_map/ppermute | solution.py:635
  127.6 2.3 %mix_final.2.kept_ref = f32[192,2048]{1,0:T(8,128)S(1)} custom-call(s32[1]{0:T(128)S(6)} %xor.20.ids_ref, bf16[768,1024]{1,0:T(8,128)(2,1)S(1)} %copy-done.13, bf16[768,384]{1,0:T(8,128)(2,1)S(1)} %copy-done.14, f32[768,16]{1,0:T(8,128)S(1)} %copy-done.15, bf16[768,1024]{1,0:T(8,128)(2,1)S(1)} %copy-done.11, bf16[1,1024]{1,0:T(2,128)(2,1)S(1)} %broadcast_in_dim.10.gain_ref, ...), custom_call_target="tpu_custom_call" | custom-call | flops 6000000000 | bytes 10000000 | tf_op jit(solution)/shard_map/mix_final/pallas_call | solution.py:390
  130.0 0.5 collective-permute-done.6.far_ref
  130.4 0.8 settle.1
  131.2 1.6 collective-permute-start.19
  132.8 1.5 collective-permute-start.15
  134.3 1.4 slice_bitcast_fusion.1
  135.7 0.5 collective-permute-start.10
  136.2 4.4 %collective-permute-done.11 = bf16[512,1152]{1,0:T(8,128)(2,1)} collective-permute-done((bf16[512,1152]{1,0:T(8,128)(2,1)}, bf16[512,1152]{1,0:T(8,128)(2,1)}, u32[]{:S(2)}, u32[]{:S(2)}) %collective-permute-start.11) | collective-permute-done | bytes 1179680 | tf_op jit(solution)/shard_map/ppermute | solution.py:635
  140.6 9.4 %collective-permute-done.19.refs_7_ = bf16[192,2048]{1,0:T(8,128)(2,1)S(1)} collective-permute-done((bf16[192,2048]{1,0:T(8,128)(2,1)S(1)}, bf16[192,2048]{1,0:T(8,128)(2,1)S(1)}, u32[]{:S(2)}, u32[]{:S(2)}) %collective-permute-start.19) | collective-permute-done | bytes 786464 | tf_op jit(solution)/shard_map/ppermute | solution.py:640
  150.1 1.6 collective-permute-start.22
  151.6 1.0 slice.65
  152.7 1.6 collective-permute-start.23
  154.2 5.4 %collective-permute-done.22.refs_7_ = bf16[96,2048]{1,0:T(8,128)(2,1)S(1)} collective-permute-done((bf16[96,2048]{1,0:T(8,128)(2,1)S(1)}, bf16[96,2048]{1,0:T(8,128)(2,1)S(1)}, u32[]{:S(2)}, u32[]{:S(2)}) %collective-permute-start.22) | collective-permute-done | bytes 393248 | tf_op jit(solution)/shard_map/ppermute | solution.py:640
  159.7 2.4 %collective-permute-done.23.refs_8_ = bf16[96,2048]{1,0:T(8,128)(2,1)} collective-permute-done((bf16[96,2048]{1,0:T(8,128)(2,1)S(1)}, bf16[96,2048]{1,0:T(8,128)(2,1)}, u32[]{:S(2)}, u32[]{:S(2)}) %collective-permute-start.23) | collective-permute-done | bytes 393248 | tf_op jit(solution)/shard_map/ppermute | solution.py:640
  162.1 0.5 collective-permute-start.16
  162.6 0.6 copy-done.17
  163.2 0.8 copy-done.6
  164.0 0.5 collective-permute-start.20
  164.6 1.0 copy-done.7
  165.6 5.8 %feed.7 = (bf16[192,2048]{1,0:T(8,128)(2,1)S(1)}, bf16[192,2048]{1,0:T(8,128)(2,1)S(1)}) custom-call(s32[2]{0:T(128)S(1)} %pad_add_fusion.1.place_ref, bf16[512,1152]{1,0:T(8,128)(2,1)S(1)} %copy-done, bf16[512,1152]{1,0:T(8,128)(2,1)S(1)} %collective-permute-done.1.refs_1_, bf16[512,1152]{1,0:T(8,128)(2,1)} %copy-done.17, ...), custom_call_target="tpu_custom_call" | custom-call | flops 1811939328 | bytes 8000000 | tf_op jit(solution)/shard_map/feed/pallas_call | solution.py:542
  171.5 6.1 %feed.5 = (bf16[192,2048]{1,0:T(8,128)(2,1)S(1)}, bf16[192,2048]{1,0:T(8,128)(2,1)S(1)}) custom-call(s32[2]{0:T(128)S(1)} %pad_add_fusion.1.place_ref, bf16[512,1152]{1,0:T(8,128)(2,1)S(1)} %copy-done, bf16[512,1152]{1,0:T(8,128)(2,1)S(1)} %collective-permute-done.1.refs_1_, bf16[512,1152]{1,0:T(8,128)(2,1)} %copy-done.17, ...), custom_call_target="tpu_custom_call" | custom-call | flops 1811939328 | bytes 8000000 | tf_op jit(solution)/shard_map/feed/pallas_call | solution.py:542
  177.7 5.9 %feed.6 = (bf16[192,2048]{1,0:T(8,128)(2,1)S(1)}, bf16[192,2048]{1,0:T(8,128)(2,1)S(1)}) custom-call(s32[2]{0:T(128)S(1)} %pad_add_fusion.1.place_ref, bf16[512,1152]{1,0:T(8,128)(2,1)S(1)} %copy-done, bf16[512,1152]{1,0:T(8,128)(2,1)S(1)} %collective-permute-done.1.refs_1_, bf16[512,1152]{1,0:T(8,128)(2,1)} %copy-done.17, ...), custom_call_target="tpu_custom_call" | custom-call | flops 1811939328 | bytes 8000000 | tf_op jit(solution)/shard_map/feed/pallas_call | solution.py:542
  183.7 5.2 %feed.4 = (bf16[192,2048]{1,0:T(8,128)(2,1)S(1)}, bf16[192,2048]{1,0:T(8,128)(2,1)S(1)}) custom-call(s32[2]{0:T(128)S(1)} %pad_add_fusion.1.place_ref, bf16[512,1152]{1,0:T(8,128)(2,1)S(1)} %copy-done, bf16[512,1152]{1,0:T(8,128)(2,1)S(1)} %collective-permute-done.1.refs_1_, bf16[512,1152]{1,0:T(8,128)(2,1)} %copy-done.17, ...), custom_call_target="tpu_custom_call" | custom-call | flops 1811939328 | bytes 8000000 | tf_op jit(solution)/shard_map/feed/pallas_call | solution.py:542
  189.0 0.3 add_convert_fusion
  189.4 1.6 collective-permute-start.30
  190.9 0.5 collective-permute-start.27
  191.5 0.3 add_convert_fusion.1
  191.8 1.1 collective-permute-start.29
  192.9 0.3 add_convert_fusion.2
  193.3 1.0 collective-permute-start.18
  194.2 7.2 %collective-permute-done.30 = bf16[192,1024]{1,0:T(8,128)(2,1)S(1)} collective-permute-done((bf16[192,1024]{1,0:T(8,128)(2,1)S(1)}, bf16[192,1024]{1,0:T(8,128)(2,1)S(1)}, u32[]{:S(2)}, u32[]{:S(2)}) %collective-permute-start.30) | collective-permute-done | bytes 393248 | tf_op jit(solution)/shard_map/ppermute | solution.py:640
  201.5 1.2 collective-permute-start.31
  203.1 0.8 collective-permute-start.28
  203.9 6.0 %collective-permute-done.29.r1_ref = bf16[192,1024]{1,0:T(8,128)(2,1)S(1)} collective-permute-done((bf16[192,1024]{1,0:T(8,128)(2,1)S(1)}, bf16[192,1024]{1,0:T(8,128)(2,1)S(1)}, u32[]{:S(2)}, u32[]{:S(2)}) %collective-permute-start.29) | collective-permute-done | bytes 393248 | tf_op jit(solution)/shard_map/ppermute | solution.py:640
  209.8 1.5 collective-permute-done.18.l1_ref
  211.4 7.7 %collective-permute-done.31.r2_ref = bf16[192,1024]{1,0:T(8,128)(2,1)S(1)} collective-permute-done((bf16[192,1024]{1,0:T(8,128)(2,1)S(1)}, bf16[192,1024]{1,0:T(8,128)(2,1)S(1)}, u32[]{:S(2)}, u32[]{:S(2)}) %collective-permute-start.31) | collective-permute-done | bytes 393248 | tf_op jit(solution)/shard_map/ppermute | solution.py:640
  219.0 1.3 finish.1
  (75 shorter events, 1.5 us)
Async XLA Ops:
  1.4 7.4 %collective-permute-start = (bf16[16,1792]{1,0:T(8,128)(2,1)}, bf16[16,1792]{1,0:T(8,128)(2,1)S(1)}, u32[]{:S(2)}, u32[]{:S(2)}) collective-permute-start(bf16[16,1792]{1,0:T(8,128)(2,1)} %tails.1), channel_id=1, source_target_pairs={{0,4},{4,8},{8,12},{1,5},{5,9},{9,13},{2,6},{6,10},{10,14},{3,7},{... | collective-permute-start | bytes 172040 | tf_op jit(solution)/shard_map/ppermute | solution.py:624
  8.8 0.6 copy-start.20
  9.4 14.2 %copy-start = (bf16[512,1152]{1,0:T(8,128)(2,1)S(1)}, bf16[512,1152]{1,0:T(8,128)(2,1)}, u32[]{:S(2)}) copy-start(bf16[512,1152]{1,0:T(8,128)(2,1)} %pick.1.refs_0_) | copy-start | bytes 3538948
  23.7 32.9 %collective-permute-start.2 = (bf16[512,1152]{1,0:T(8,128)(2,1)S(1)}, bf16[512,1152]{1,0:T(8,128)(2,1)S(1)}, u32[]{:S(2)}, u32[]{:S(2)}) collective-permute-start(bf16[512,1152]{1,0:T(8,128)(2,1)S(1)} %copy-done), channel_id=1, source_target_pairs={{0,1},{1,0},{2,3},{3,2},{4,5},{5,4},{6,7},{7,6},{8,9},{9,8},{10,11... | collective-permute-start | bytes 3538952 | tf_op jit(solution)/shard_map/ppermute | solution.py:640
  23.7 32.8 %collective-permute-start.1 = (bf16[512,1152]{1,0:T(8,128)(2,1)S(1)}, bf16[512,1152]{1,0:T(8,128)(2,1)S(1)}, u32[]{:S(2)}, u32[]{:S(2)}) collective-permute-start(bf16[512,1152]{1,0:T(8,128)(2,1)S(1)} %copy-done), channel_id=1, source_target_pairs={{0,4},{2,6},{4,8},{5,1},{6,10},{7,3},{8,12},{9,5},{10,14},{11,7},{... | collective-permute-start | bytes 3538952 | tf_op jit(solution)/shard_map/ppermute | solution.py:635
  27.7 20.3 %collective-permute-start.3 = (bf16[400,256]{1,0:T(8,128)(2,1)}, bf16[400,256]{1,0:T(8,128)(2,1)S(1)}, u32[]{:S(2)}, u32[]{:S(2)}) collective-permute-start(bf16[400,256]{1,0:T(8,128)(2,1)} %get-tuple-element.35.later_ref), channel_id=1, source_target_pairs={{0,4},{4,8},{8,12},{1,5},{5,9},{9,13},{2,6},{6,10},{10,14},{3,7},{... | collective-permute-start | bytes 614408 | tf_op jit(solution)/shard_map/ppermute | solution.py:624
  48.0 0.9 copy-start.8
  49.0 10.8 %collective-permute-start.4 = (bf16[400,256]{1,0:T(8,128)(2,1)S(1)}, bf16[400,256]{1,0:T(8,128)(2,1)S(1)}, u32[]{:S(2)}, u32[]{:S(2)}) collective-permute-start(bf16[400,256]{1,0:T(8,128)(2,1)S(1)} %join_states.1), channel_id=1, source_target_pairs={{0,8},{4,12},{1,9},{5,13},{2,10},{6,14},{3,11},{7,15},{16,24},{20,... | collective-permute-start | bytes 614408 | tf_op jit(solution)/shard_map/ppermute | solution.py:624
  56.5 5.9 %copy-start.19 = (bf16[1024]{0:T(1024)(128)(2,1)S(1)}, bf16[1024]{0:T(1024)(128)(2,1)}, u32[]{:S(2)}) copy-start(bf16[1024]{0:T(1024)(128)(2,1)} %param.36) | copy-start | bytes 6148
  56.5 37.8 %copy-start.14 = (bf16[768,384]{1,0:T(8,128)(2,1)S(1)}, bf16[768,384]{1,0:T(8,128)(2,1)}, u32[]{:S(2)}) copy-start(bf16[768,384]{1,0:T(8,128)(2,1)} %get-tuple-element.30.q_ref) | copy-start | bytes 1769476
  59.8 27.9 %collective-permute-start.7 = (bf16[2,512,1152]{2,1,0:T(8,128)(2,1)}, bf16[2,512,1152]{2,1,0:T(8,128)(2,1)}, u32[]{:S(2)}, u32[]{:S(2)}) collective-permute-start(bf16[2,512,1152]{2,1,0:T(8,128)(2,1)} %pad_maximum_fusion), channel_id=1, source_target_pairs={{0,4},{2,6},{4,8},{5,1},{6,10},{7,3},{8,12},{9,5},{10,14},{11,7},{... | collective-permute-start | bytes 7077896 | tf_op jit(solution)/shard_map/ppermute | solution.py:635
  87.7 33.2 %collective-permute-start.9 = (bf16[2,512,1152]{2,1,0:T(8,128)(2,1)}, bf16[2,512,1152]{2,1,0:T(8,128)(2,1)S(1)}, u32[]{:S(2)}, u32[]{:S(2)}) collective-permute-start(bf16[2,512,1152]{2,1,0:T(8,128)(2,1)} %collective-permute-done.7.refs_3_), channel_id=1, source_target_pairs={{0,4},{2,6},{4,8},{5,1},{6,10},{7,3},{8,12},{9,5},{10,14},{11,7},{... | collective-permute-start | bytes 7077896 | tf_op jit(solution)/shard_map/ppermute | solution.py:635
  94.4 2.2 copy-start.9
  96.6 1.4 copy-start.11
  98.0 1.4 copy-start.12
  99.4 1.0 copy-start.15
  100.4 7.3 %copy-start.18 = (bf16[2048]{0:T(1024)(128)(2,1)S(1)}, bf16[2048]{0:T(1024)(128)(2,1)}, u32[]{:S(2)}) copy-start(bf16[2048]{0:T(1024)(128)(2,1)} %param.38) | copy-start | bytes 12292
  100.4 27.2 %copy-start.13 = (bf16[768,1024]{1,0:T(8,128)(2,1)S(1)}, bf16[768,1024]{1,0:T(8,128)(2,1)}, u32[]{:S(2)}) copy-start(bf16[768,1024]{1,0:T(8,128)(2,1)} %get-tuple-element.29.y_ref) | copy-start | bytes 4718596
  107.0 3.5 %collective-permute-start.5 = (bf16[384,2048]{1,0:T(8,128)(2,1)S(1)}, bf16[384,2048]{1,0:T(8,128)(2,1)S(1)}, u32[]{:S(2)}, u32[]{:S(2)}) collective-permute-start(bf16[384,2048]{1,0:T(8,128)(2,1)S(1)} %get-tuple-element.38), channel_id=1, source_target_pairs={{0,1},{1,0},{2,3},{3,2},{4,5},{5,4},{6,7},{7,6},{8,9},{9,8},{10,11... | collective-permute-start | bytes 4718600 | tf_op jit(solution)/shard_map/ppermute | solution.py:640
  110.5 17.1 %copy-start.10 = (bf16[1024,2048]{1,0:T(8,128)(2,1)S(1)}, bf16[1024,2048]{1,0:T(8,128)(2,1)}, u32[]{:S(2)}) copy-start(bf16[1024,2048]{1,0:T(8,128)(2,1)} %matrix_ref.3) | copy-start | bytes 12582916
  110.8 19.6 %collective-permute-start.6 = (bf16[192,2048]{1,0:T(8,128)(2,1)S(1)}, bf16[192,2048]{1,0:T(8,128)(2,1)S(1)}, u32[]{:S(2)}, u32[]{:S(2)}) collective-permute-start(bf16[192,2048]{1,0:T(8,128)(2,1)S(1)} %add_convert_fusion.3), channel_id=1, source_target_pairs={{0,2},{1,3},{2,0},{3,1},{4,6},{5,7},{6,4},{7,5},{8,10},{9,11},{10,... | collective-permute-start | bytes 2359304 | tf_op jit(solution)/shard_map/ppermute | solution.py:640
  120.9 9.1 %copy-start.16 = (bf16[2,512,1152]{2,1,0:T(8,128)(2,1)}, bf16[2,512,1152]{2,1,0:T(8,128)(2,1)S(1)}, u32[]{:S(2)}) copy-start(bf16[2,512,1152]{2,1,0:T(8,128)(2,1)S(1)} %collective-permute-done.9.refs_5_) | copy-start | bytes 7077892
  122.1 8.3 %copy-start.1 = (bf16[192,2048]{1,0:T(8,128)(2,1)S(1)}, bf16[192,2048]{1,0:T(8,128)(2,1)}, u32[]{:S(2)}) copy-start(bf16[192,2048]{1,0:T(8,128)(2,1)} %residual_ref.1) | copy-start | bytes 2359300
  122.1 18.5 %collective-permute-start.11 = (bf16[512,1152]{1,0:T(8,128)(2,1)}, bf16[512,1152]{1,0:T(8,128)(2,1)}, u32[]{:S(2)}, u32[]{:S(2)}) collective-permute-start(bf16[512,1152]{1,0:T(8,128)(2,1)} %slice_bitcast_fusion), channel_id=1, source_target_pairs={{0,4},{2,6},{4,8},{5,1},{6,10},{7,3},{8,12},{9,5},{10,14},{11,7},{... | collective-permute-start | bytes 3538952 | tf_op jit(solution)/shard_map/ppermute | solution.py:635
  131.2 18.8 %copy-start.2 = (bf16[192,2048]{1,0:T(8,128)(2,1)}, bf16[192,2048]{1,0:T(8,128)(2,1)S(1)}, u32[]{:S(2)}) copy-start(bf16[192,2048]{1,0:T(8,128)(2,1)S(1)} %get-tuple-element.40.after_ref) | copy-start | bytes 2359300
  131.2 18.8 %copy-start.4 = (bf16[192,2048]{1,0:T(8,128)(2,1)}, bf16[192,2048]{1,0:T(8,128)(2,1)S(1)}, u32[]{:S(2)}) copy-start(bf16[192,2048]{1,0:T(8,128)(2,1)S(1)} %get-tuple-element.42.refs_7_) | copy-start | bytes 2359300
  131.2 18.8 %collective-permute-start.19 = (bf16[192,2048]{1,0:T(8,128)(2,1)S(1)}, bf16[192,2048]{1,0:T(8,128)(2,1)S(1)}, u32[]{:S(2)}, u32[]{:S(2)}) collective-permute-start(bf16[192,2048]{1,0:T(8,128)(2,1)S(1)} %get-tuple-element.42.refs_7_), channel_id=1, source_target_pairs={{0,16},{16,0},{1,17},{17,1},{2,18},{18,2},{3,19},{19,3},{4,20},{20... | collective-permute-start | bytes 2359304 | tf_op jit(solution)/shard_map/ppermute | solution.py:640
  132.8 18.8 %collective-permute-start.15 = (bf16[192,2048]{1,0:T(8,128)(2,1)S(1)}, bf16[192,2048]{1,0:T(8,128)(2,1)}, u32[]{:S(2)}, u32[]{:S(2)}) collective-permute-start(bf16[192,2048]{1,0:T(8,128)(2,1)S(1)} %get-tuple-element.42.refs_7_), channel_id=1, source_target_pairs={{0,2},{1,3},{2,0},{3,1},{4,6},{5,7},{6,4},{7,5},{8,10},{9,11},{10,... | collective-permute-start | bytes 2359304 | tf_op jit(solution)/shard_map/ppermute | solution.py:640
  135.7 26.4 %collective-permute-start.8 = (bf16[512,1152]{1,0:T(8,128)(2,1)S(1)}, bf16[512,1152]{1,0:T(8,128)(2,1)S(1)}, u32[]{:S(2)}, u32[]{:S(2)}) collective-permute-start(bf16[512,1152]{1,0:T(8,128)(2,1)S(1)} %slice_bitcast_fusion.1), channel_id=1, source_target_pairs={{0,1},{1,0},{2,3},{3,2},{4,5},{5,4},{6,7},{7,6},{8,9},{9,8},{10,11... | collective-permute-start | bytes 3538952 | tf_op jit(solution)/shard_map/ppermute | solution.py:640
  135.7 28.8 %collective-permute-start.10 = (bf16[512,1152]{1,0:T(8,128)(2,1)}, bf16[512,1152]{1,0:T(8,128)(2,1)}, u32[]{:S(2)}, u32[]{:S(2)}) collective-permute-start(bf16[512,1152]{1,0:T(8,128)(2,1)} %slice_bitcast_fusion), channel_id=1, source_target_pairs={{0,1},{1,0},{2,3},{3,2},{4,5},{5,4},{6,7},{7,6},{8,9},{9,8},{10,11... | collective-permute-start | bytes 3538952 | tf_op jit(solution)/shard_map/ppermute | solution.py:640
  140.6 24.0 %collective-permute-start.12 = (bf16[512,1152]{1,0:T(8,128)(2,1)}, bf16[512,1152]{1,0:T(8,128)(2,1)}, u32[]{:S(2)}, u32[]{:S(2)}) collective-permute-start(bf16[512,1152]{1,0:T(8,128)(2,1)} %collective-permute-done.11), channel_id=1, source_target_pairs={{0,1},{1,0},{2,3},{3,2},{4,5},{5,4},{6,7},{7,6},{8,9},{9,8},{10,11... | collective-permute-start | bytes 3538952 | tf_op jit(solution)/shard_map/ppermute | solution.py:640
  150.1 9.6 %collective-permute-start.22 = (bf16[96,2048]{1,0:T(8,128)(2,1)S(1)}, bf16[96,2048]{1,0:T(8,128)(2,1)S(1)}, u32[]{:S(2)}, u32[]{:S(2)}) collective-permute-start(bf16[96,2048]{1,0:T(8,128)(2,1)S(1)} %slice.64), channel_id=1, source_target_pairs={{0,2},{1,3},{2,0},{3,1},{4,6},{5,7},{6,4},{7,5},{8,10},{9,11},{10,... | collective-permute-start | bytes 1179656 | tf_op jit(solution)/shard_map/ppermute | solution.py:640
  152.7 9.4 %collective-permute-start.23 = (bf16[96,2048]{1,0:T(8,128)(2,1)S(1)}, bf16[96,2048]{1,0:T(8,128)(2,1)}, u32[]{:S(2)}, u32[]{:S(2)}) collective-permute-start(bf16[96,2048]{1,0:T(8,128)(2,1)S(1)} %slice.65), channel_id=1, source_target_pairs={{0,16},{16,0},{1,17},{17,1},{2,18},{18,2},{3,19},{19,3},{4,20},{20... | collective-permute-start | bytes 1179656 | tf_op jit(solution)/shard_map/ppermute | solution.py:640
  159.7 2.9 %collective-permute-start.24 = (bf16[96,2048]{1,0:T(8,128)(2,1)S(1)}, bf16[96,2048]{1,0:T(8,128)(2,1)S(1)}, u32[]{:S(2)}, u32[]{:S(2)}) collective-permute-start(bf16[96,2048]{1,0:T(8,128)(2,1)S(1)} %collective-permute-done.22.refs_7_), channel_id=1, source_target_pairs={{0,1},{1,0},{2,3},{3,2},{4,5},{5,4},{6,7},{7,6},{8,9},{9,8},{10,11... | collective-permute-start | bytes 1179656 | tf_op jit(solution)/shard_map/ppermute | solution.py:640
  162.1 2.5 %collective-permute-start.25 = (bf16[96,2048]{1,0:T(8,128)(2,1)}, bf16[96,2048]{1,0:T(8,128)(2,1)}, u32[]{:S(2)}, u32[]{:S(2)}) collective-permute-start(bf16[96,2048]{1,0:T(8,128)(2,1)} %collective-permute-done.23.refs_8_), channel_id=1, source_target_pairs={{0,1},{1,0},{2,3},{3,2},{4,5},{5,4},{6,7},{7,6},{8,9},{9,8},{10,11... | collective-permute-start | bytes 1179656 | tf_op jit(solution)/shard_map/ppermute | solution.py:640
  162.1 1.1 copy-start.17
  162.1 9.4 %collective-permute-start.16 = (bf16[192,2048]{1,0:T(8,128)(2,1)}, bf16[192,2048]{1,0:T(8,128)(2,1)}, u32[]{:S(2)}, u32[]{:S(2)}) collective-permute-start(bf16[192,2048]{1,0:T(8,128)(2,1)} %collective-permute-done.15.refs_7_), channel_id=1, source_target_pairs={{0,1},{1,0},{2,3},{3,2},{4,5},{5,4},{6,7},{7,6},{8,9},{9,8},{10,11... | collective-permute-start | bytes 2359304 | tf_op jit(solution)/shard_map/ppermute | solution.py:640
  163.2 0.8 copy-start.6
  164.0 13.7 %collective-permute-start.20 = (bf16[192,2048]{1,0:T(8,128)(2,1)S(1)}, bf16[192,2048]{1,0:T(8,128)(2,1)}, u32[]{:S(2)}, u32[]{:S(2)}) collective-permute-start(bf16[192,2048]{1,0:T(8,128)(2,1)S(1)} %collective-permute-done.19.refs_7_), channel_id=1, source_target_pairs={{0,1},{1,0},{2,3},{3,2},{4,5},{5,4},{6,7},{7,6},{8,9},{9,8},{10,11... | collective-permute-start | bytes 2359304 | tf_op jit(solution)/shard_map/ppermute | solution.py:640
  164.6 19.1 %collective-permute-start.13 = (bf16[192,2048]{1,0:T(8,128)(2,1)}, bf16[192,2048]{1,0:T(8,128)(2,1)S(1)}, u32[]{:S(2)}, u32[]{:S(2)}) collective-permute-start(bf16[192,2048]{1,0:T(8,128)(2,1)} %copy-done.4), channel_id=1, source_target_pairs={{0,1},{1,0},{2,3},{3,2},{4,5},{5,4},{6,7},{7,6},{8,9},{9,8},{10,11... | collective-permute-start | bytes 2359304 | tf_op jit(solution)/shard_map/ppermute | solution.py:640
  164.6 1.0 copy-start.7
  171.4 17.6 %collective-permute-start.26 = (bf16[192,2048]{1,0:T(8,128)(2,1)S(1)}, bf16[192,2048]{1,0:T(8,128)(2,1)S(1)}, u32[]{:S(2)}, u32[]{:S(2)}) collective-permute-start(bf16[192,2048]{1,0:T(8,128)(2,1)S(1)} %get-tuple-element.50), channel_id=1, source_target_pairs={{0,1},{1,0},{2,3},{3,2},{4,5},{5,4},{6,7},{7,6},{8,9},{9,8},{10,11... | collective-permute-start | bytes 2359304 | tf_op jit(solution)/shard_map/ppermute | solution.py:640
  177.6 6.1 %copy-start.5 = (bf16[192,2048]{1,0:T(8,128)(2,1)S(1)}, bf16[192,2048]{1,0:T(8,128)(2,1)}, u32[]{:S(2)}) copy-start(bf16[192,2048]{1,0:T(8,128)(2,1)} %copy-done.4) | copy-start | bytes 2359300
  177.6 15.4 %collective-permute-start.17 = (bf16[192,2048]{1,0:T(8,128)(2,1)S(1)}, bf16[192,2048]{1,0:T(8,128)(2,1)S(1)}, u32[]{:S(2)}, u32[]{:S(2)}) collective-permute-start(bf16[192,2048]{1,0:T(8,128)(2,1)S(1)} %get-tuple-element.46), channel_id=1, source_target_pairs={{0,1},{1,0},{2,3},{3,2},{4,5},{5,4},{6,7},{7,6},{8,9},{9,8},{10,11... | collective-permute-start | bytes 2359304 | tf_op jit(solution)/shard_map/ppermute | solution.py:640
  183.6 7.9 %collective-permute-start.21 = (bf16[192,2048]{1,0:T(8,128)(2,1)S(1)}, bf16[192,2048]{1,0:T(8,128)(2,1)S(1)}, u32[]{:S(2)}, u32[]{:S(2)}) collective-permute-start(bf16[192,2048]{1,0:T(8,128)(2,1)S(1)} %get-tuple-element.48), channel_id=1, source_target_pairs={{0,1},{1,0},{2,3},{3,2},{4,5},{5,4},{6,7},{7,6},{8,9},{9,8},{10,11... | collective-permute-start | bytes 2359304 | tf_op jit(solution)/shard_map/ppermute | solution.py:640
  188.9 14.9 %collective-permute-start.14 = (bf16[192,2048]{1,0:T(8,128)(2,1)S(1)}, bf16[192,2048]{1,0:T(8,128)(2,1)S(1)}, u32[]{:S(2)}, u32[]{:S(2)}) collective-permute-start(bf16[192,2048]{1,0:T(8,128)(2,1)S(1)} %get-tuple-element.44), channel_id=1, source_target_pairs={{0,1},{1,0},{2,3},{3,2},{4,5},{5,4},{6,7},{7,6},{8,9},{9,8},{10,11... | collective-permute-start | bytes 2359304 | tf_op jit(solution)/shard_map/ppermute | solution.py:640
  189.4 12.1 %collective-permute-start.30 = (bf16[192,1024]{1,0:T(8,128)(2,1)S(1)}, bf16[192,1024]{1,0:T(8,128)(2,1)S(1)}, u32[]{:S(2)}, u32[]{:S(2)}) collective-permute-start(bf16[192,1024]{1,0:T(8,128)(2,1)S(1)} %get-tuple-element.51), channel_id=1, source_target_pairs={{0,16},{16,0},{1,17},{17,1},{2,18},{18,2},{3,19},{19,3},{4,20},{20... | collective-permute-start | bytes 1179656 | tf_op jit(solution)/shard_map/ppermute | solution.py:640
  190.9 12.0 %collective-permute-start.27 = (bf16[192,1024]{1,0:T(8,128)(2,1)S(1)}, bf16[192,1024]{1,0:T(8,128)(2,1)S(1)}, u32[]{:S(2)}, u32[]{:S(2)}) collective-permute-start(bf16[192,1024]{1,0:T(8,128)(2,1)S(1)} %get-tuple-element.52), channel_id=1, source_target_pairs={{0,2},{1,3},{2,0},{3,1},{4,6},{5,7},{6,4},{7,5},{8,10},{9,11},{10,... | collective-permute-start | bytes 1179656 | tf_op jit(solution)/shard_map/ppermute | solution.py:640
  191.8 18.0 %collective-permute-start.29 = (bf16[192,1024]{1,0:T(8,128)(2,1)S(1)}, bf16[192,1024]{1,0:T(8,128)(2,1)S(1)}, u32[]{:S(2)}, u32[]{:S(2)}) collective-permute-start(bf16[192,1024]{1,0:T(8,128)(2,1)S(1)} %slice.67), channel_id=1, source_target_pairs={{0,16},{16,0},{1,17},{17,1},{2,18},{18,2},{3,19},{19,3},{4,20},{20... | collective-permute-start | bytes 1179656 | tf_op jit(solution)/shard_map/ppermute | solution.py:640
  193.2 25.8 %copy-start.3 = (bf16[192,2048]{1,0:T(8,128)(2,1)S(1)}, bf16[192,2048]{1,0:T(8,128)(2,1)}, u32[]{:S(2)}) copy-start(bf16[192,2048]{1,0:T(8,128)(2,1)} %copy-done.2) | copy-start | bytes 2359300
  193.3 18.1 %collective-permute-start.18 = (bf16[192,1024]{1,0:T(8,128)(2,1)S(1)}, bf16[192,1024]{1,0:T(8,128)(2,1)S(1)}, u32[]{:S(2)}, u32[]{:S(2)}) collective-permute-start(bf16[192,1024]{1,0:T(8,128)(2,1)S(1)} %slice.62), channel_id=1, source_target_pairs={{0,2},{1,3},{2,0},{3,1},{4,6},{5,7},{6,4},{7,5},{8,10},{9,11},{10,... | collective-permute-start | bytes 1179656 | tf_op jit(solution)/shard_map/ppermute | solution.py:640
  201.5 17.5 %collective-permute-start.31 = (bf16[192,1024]{1,0:T(8,128)(2,1)S(1)}, bf16[192,1024]{1,0:T(8,128)(2,1)S(1)}, u32[]{:S(2)}, u32[]{:S(2)}) collective-permute-start(bf16[192,1024]{1,0:T(8,128)(2,1)S(1)} %add_convert_fusion.4), channel_id=1, source_target_pairs={{0,2},{1,3},{2,0},{3,1},{4,6},{5,7},{6,4},{7,5},{8,10},{9,11},{10,... | collective-permute-start | bytes 1179656 | tf_op jit(solution)/shard_map/ppermute | solution.py:640
  203.1 16.0 %collective-permute-start.28 = (bf16[192,1024]{1,0:T(8,128)(2,1)S(1)}, bf16[192,1024]{1,0:T(8,128)(2,1)S(1)}, u32[]{:S(2)}, u32[]{:S(2)}) collective-permute-start(bf16[192,1024]{1,0:T(8,128)(2,1)S(1)} %add_convert_fusion.5), channel_id=1, source_target_pairs={{0,16},{16,0},{1,17},{17,1},{2,18},{18,2},{3,19},{19,3},{4,20},{20... | collective-permute-start | bytes 1179656 | tf_op jit(solution)/shard_map/ppermute | solution.py:640
